TPU v7x, 32 devices: a whole 2x2x4 slice. The times are simulated.
32 devices in a mesh: ep: 8 (over z, x), tp: 4 (over y, core).
Axes of the slice: x: 2, y: 2, z: 4, core: 2. Of those that a mesh axis runs over, the one named last changes fastest.
Arguments:
- queries: bfloat16 [8192, 2048], P('ep', 'tp'), may hold values from -128 to 128
- key_heads: bfloat16 [8192, 1024], P('ep', 'tp'), may hold values from -6 to 6
- value_heads: bfloat16 [8192, 1024], P('ep', 'tp'), may hold values from -6 to 6
- sink_logits: float32 [32], P('tp'), may hold values from 1 to 5
- mix_weight: bfloat16 [2048, 2048], replicated, may hold values from -1 to 1
- expert_input: bfloat16 [4096, 2048], P(('ep', 'tp')), may hold values from -6 to 6
- norm_gain: float32 [2048], replicated, may hold values from 0.1 to 1.9
- routes: int32 [4096, 4], P(('ep', 'tp')), may hold values from 0 to 31, all different within a row; in each aligned block of 128 rows (0 to 127, 128 to 255, ...) at most 32 rows name the same one
- route_weights: float32 [4096, 4], P(('ep', 'tp')), may hold values from 0.1 to 1
- gate_weight: bfloat16 [32, 2048, 1024], P(('ep', 'tp')), may hold values from -0.375 to 0.375
- up_weight: bfloat16 [32, 2048, 1024], P(('ep', 'tp')), may hold values from -0.375 to 0.375
- down_weight: bfloat16 [32, 1024, 2048], P(('ep', 'tp')), may hold values from -0.046875 to 0.046875
Outputs:
- mixer_out: bfloat16 [8192, 2048], P(('ep', 'tp'))
- experts_out: bfloat16 [4096, 2048], P(('ep', 'tp'))
Inputs may be any that keep to these rules, and one draw needn't show every extreme that they name: `routes`: each row names 4 different experts; within the 128 rows of one device no expert is named more than 32 times, and in some devices' rows some expert is named exactly 32 times.
All inputs are finite; a program needn't handle non-finite values.
Results may differ from a plain program's by a relative error of at most 0.012.
The roundings to bfloat16 on the way count: a program that leaves them out, or rounds other values in their place, can miss the bound.
Values may be sent and summed in bfloat16 or wider, within the bound.
No kernel may reach another device: no remote copies, remote signals or barrier semaphores. Data moves between devices by JAX's collectives and lax.ppermute only.
A program may use at most 128 MiB of HBM per device.

v0:
```python
import functools
import math

import jax
import jax.numpy as jnp
from jax import lax
from jax.experimental import pallas as pl
from jax.experimental.pallas import tpu as pltpu
from jax.sharding import Mesh
from jax.sharding import PartitionSpec as P


HEAD_DIM = 64
WINDOW = 128
GRID_W = 64
ROPE_BASE = 10000.0
CLAMP_LIMIT = 7.0
GATE_SLOPE = 1.702
NORM_EPS = 1e-05
LANES = 128
MASKED = -1e30

VMEM = pl.BlockSpec(memory_space=pltpu.VMEM)
SMEM = pl.BlockSpec(memory_space=pltpu.SMEM)
ANY = pl.BlockSpec(memory_space=pl.ANY)
HBM = pl.BlockSpec(memory_space=pltpu.HBM)
BF16 = jnp.bfloat16
F32 = jnp.float32


def cost(flops):
    return pl.CostEstimate(flops=int(flops), transcendentals=0, bytes_accessed=1 << 20)


def params(mebibytes):
    return pltpu.CompilerParams(vmem_limit_bytes=mebibytes << 20)


def iota(shape, dim):
    return lax.broadcasted_iota(jnp.int32, shape, dim)


def fetch(pairs, sems):
    copies = [pltpu.make_async_copy(s, t, sems.at[i]) for i, (s, t) in enumerate(pairs)]
    for copy in copies:
        copy.start()
    for copy in copies:
        copy.wait()


def norm_kernel(x_hbm, gain_hbm, route_hbm, weight_hbm, out_ref, *scratch):
    x_ref, gain_ref, route_ref, weight_ref, sems = scratch
    fetch(
        ((x_hbm, x_ref), (gain_hbm, gain_ref), (route_hbm, route_ref), (weight_hbm, weight_ref)),
        sems,
    )
    tokens, width = x_ref.shape
    top = route_ref.shape[0]
    values = x_ref[...].astype(F32)
    center = jnp.mean(values, axis=-1, keepdims=True)
    shifted = values - center
    spread = jnp.mean(jnp.square(shifted), axis=-1, keepdims=True)
    normed = shifted * lax.rsqrt(spread + NORM_EPS) * gain_ref[...]
    out_ref[:, :width] = normed.astype(BF16)
    line = iota((LANES, 1), 0)
    names = route_ref[...].astype(F32)
    high = weight_ref[...].astype(BF16).astype(F32)
    low = weight_ref[...] - high
    extra = jnp.zeros((LANES, tokens), F32)
    for i, part in enumerate((names, high, low)):
        for k in range(top):
            extra = jnp.where(line == i * top + k, part[k : k + 1, :], extra)
    out_ref[:, width:] = jnp.transpose(extra).astype(BF16)


def make_payload(x, gain, routes, weights):
    tokens, width = x.shape
    operands = [
        pltpu.with_memory_space_constraint(o, pltpu.HBM)
        for o in (x, gain.reshape(1, width), routes.T, weights.T)
    ]
    return pl.pallas_call(
        norm_kernel,
        out_shape=jax.ShapeDtypeStruct((tokens, width + LANES), BF16),
        in_specs=[HBM] * 4,
        out_specs=VMEM,
        scratch_shapes=[pltpu.VMEM(o.shape, o.dtype) for o in operands]
        + [pltpu.SemaphoreType.DMA((4,))],
        compiler_params=params(6),
        cost_estimate=cost(1e9),
        name="norm",
    )(*operands)


def slot_match(extra, where_ref, plan, weighted):
    tokens = extra.shape[0]
    top, cap, plane, xor = plan
    lane = iota((1, LANES), 1)
    piece = (2 * lane) ^ where_ref[1] if xor else lane
    target = jnp.where(lane < plane, where_ref[0] + piece, -1).astype(F32)
    named = jnp.zeros((tokens, LANES), F32)
    high = jnp.zeros((tokens, LANES), F32)
    low = jnp.zeros((tokens, LANES), F32)
    for k in range(top):
        hit = extra[:, k : k + 1] == target
        named = jnp.where(hit, 1.0, named)
        if weighted:
            high = jnp.where(hit, extra[:, top + k : top + k + 1], high)
            low = jnp.where(hit, extra[:, 2 * top + k : 2 * top + k + 1], low)
    earlier = (iota((tokens, tokens), 1) < iota((tokens, tokens), 0)).astype(F32).astype(BF16)
    slot = jnp.dot(earlier, named.astype(BF16), preferred_element_type=F32)
    slot = jnp.where(named > 0.5, slot, -1.0)
    columns = plane * cap
    spread = (iota((LANES, columns), 1) // cap == iota((LANES, columns), 0)).astype(F32).astype(BF16)
    place = (iota((1, columns), 1) % cap).astype(F32)
    slot = jnp.dot(slot.astype(BF16), spread, preferred_element_type=F32)
    match = slot == place
    if not weighted:
        return jnp.where(match, 1.0, 0.0)
    high = jnp.dot(high.astype(BF16), spread, preferred_element_type=F32)
    low = jnp.dot(low.astype(BF16), spread, preferred_element_type=F32)
    zero = jnp.zeros_like(high)
    return jnp.where(match, high, zero).astype(BF16), jnp.where(match, low, zero).astype(BF16)


def dispatch_kernel(plan, pieces, count, where_ref, *refs):
    payload_refs, out_refs = refs[:count], refs[-pieces:]
    width = payload_refs[0].shape[1] - LANES
    step = math.gcd(width, 512)
    for j, payload_ref in enumerate(payload_refs):
        extra = payload_ref[:, width:].astype(F32)
        match = slot_match(extra, where_ref, plan, False)
        turned = jnp.transpose(match).astype(BF16)
        rows = turned.shape[0] // pieces
        for left in range(0, width, step):
            block = jnp.dot(turned, payload_ref[:, left : left + step], preferred_element_type=F32)
            block = block.astype(BF16)
            for i in range(pieces):
                out_refs[i][j * rows : (j + 1) * rows, left : left + step] = block[
                    i * rows : (i + 1) * rows
                ]


def dispatch(plan, pieces, where, payloads, after):
    width = payloads[0].shape[1] - LANES
    rows = plan[1] * plan[2] // pieces * len(payloads)
    return pl.pallas_call(
        functools.partial(dispatch_kernel, plan, pieces, len(payloads)),
        out_shape=[jax.ShapeDtypeStruct((rows, width), BF16)] * pieces,
        in_specs=[SMEM] + [VMEM] * len(payloads) + [ANY] * len(after),
        out_specs=[VMEM] * pieces,
        compiler_params=params(8),
        cost_estimate=cost(2e9),
        name="dispatch",
    )(where, *payloads, *after)


def combine_kernel(plan, pieces, count, where_ref, *refs):
    payload_refs, back_refs = refs[:count], refs[count : count + pieces]
    out_refs = refs[-count:]
    width = out_refs[0].shape[1]
    step = math.gcd(width, 512)
    rows = plan[1] * plan[2] // pieces
    for j, payload_ref in enumerate(payload_refs):
        high, low = slot_match(payload_ref[:, width:].astype(F32), where_ref, plan, True)
        spot = slice(j * rows, (j + 1) * rows)
        for left in range(0, width, step):
            cut = slice(left, left + step)
            back = jnp.concatenate([r[spot, cut] for r in back_refs], axis=0)
            total = jnp.dot(high, back, preferred_element_type=F32)
            total = total + jnp.dot(low, back, preferred_element_type=F32)
            out_refs[j][:, cut] = total.astype(out_refs[j].dtype)


def combine(plan, where, payloads, back, after):
    tokens, wide = payloads[0].shape
    width = wide - LANES
    count = len(payloads)
    return pl.pallas_call(
        functools.partial(combine_kernel, plan, len(back), count),
        out_shape=[jax.ShapeDtypeStruct((tokens, width), d) for d in (F32, BF16)[:count]],
        in_specs=[SMEM] + [VMEM] * (count + len(back)) + [ANY] * len(after),
        out_specs=[VMEM] * count,
        compiler_params=params(10),
        cost_estimate=cost(2e9),
        name="combine",
    )(where, *payloads, *back, *after)


def expert_kernel(pieces, gate_ref, up_ref, down_ref, *refs):
    in_refs, out_refs = refs[:pieces], refs[-pieces - 2 : -2]
    x_ref, act_ref = refs[-2:]
    rows = in_refs[0].shape[0]
    hidden = gate_ref.shape[2]
    width = down_ref.shape[2]
    for i in range(pieces):
        x_ref[i * rows : (i + 1) * rows, :] = in_refs[i][...]
    tile = math.gcd(hidden, 256)
    for left in range(0, hidden, tile):
        cut = slice(left, left + tile)
        gate = jnp.dot(x_ref[...], gate_ref[0, :, cut], preferred_element_type=F32)
        lift = jnp.dot(x_ref[...], up_ref[0, :, cut], preferred_element_type=F32)
        gate = jnp.minimum(gate, CLAMP_LIMIT)
        lift = jnp.clip(lift, -CLAMP_LIMIT, CLAMP_LIMIT)
        act = (lift + 1.0) * gate * jax.nn.sigmoid(GATE_SLOPE * gate)
        act_ref[:, cut] = act.astype(BF16)
    wide = math.gcd(width, 512)
    for left in range(0, width, wide):
        cut = slice(left, left + wide)
        done = jnp.dot(act_ref[...], down_ref[0, :, cut], preferred_element_type=F32).astype(BF16)
        for i in range(pieces):
            out_refs[i][:, cut] = done[i * rows : (i + 1) * rows]


def experts(parts, weights, after):
    pieces = len(parts)
    rows, width = parts[0].shape
    hidden = weights[0].shape[2]
    return pl.pallas_call(
        functools.partial(expert_kernel, pieces),
        in_specs=[VMEM] * (3 + pieces) + [ANY] * len(after),
        out_specs=[VMEM] * pieces,
        out_shape=[jax.ShapeDtypeStruct((rows, width), BF16)] * pieces,
        scratch_shapes=[
            pltpu.VMEM((pieces * rows, width), BF16),
            pltpu.VMEM((pieces * rows, hidden), BF16),
        ],
        cost_estimate=pl.CostEstimate(
            flops=6 * pieces * rows * width * hidden,
            transcendentals=0,
            bytes_accessed=4 * pieces * rows * width,
        ),
        compiler_params=params(16),
        name="experts",
    )(*weights, *parts, *after)


def rope_block(x, cos, sin):
    lane = iota((1, LANES), 1)
    quarter = HEAD_DIM // 4
    ahead = pltpu.roll(x, LANES - quarter, axis=1)
    behind = pltpu.roll(x, quarter, axis=1)
    mate = jnp.where(lane % (2 * quarter) < quarter, ahead, behind)
    return x * cos + mate * sin


def attention_kernel(
    first, count, info_ref, sink_ref, table_ref, q_hbm, k_hbm, v_hbm, left_ref, right_ref, after_ref, out_ref,
    k_all, v_all, band_ref, score_ref, chance_ref, q_ref, k_ref, sems,
):
    q_block = WINDOW
    rows = k_hbm.shape[0]
    blocks = rows // q_block
    low, high = max(first, 1), min(first + count + 2, blocks + 1)
    near = slice((low - 1) * q_block, (high - 1) * q_block)
    inside = slice((low - first) * q_block, (high - first) * q_block)
    fetch(
        (
            (k_hbm.at[near, :], k_ref.at[inside, :]),
            (v_hbm.at[near, :], v_all.at[inside, :]),
            (q_hbm.at[first * q_block : (first + count) * q_block, :], q_ref),
        ),
        sems,
    )
    kv_width = k_ref.shape[1]
    pairs = kv_width // LANES
    group = q_ref.shape[1] // kv_width
    span = q_block + 2 * WINDOW
    grid_rows = (rows + 2 * WINDOW) // GRID_W
    per_block = q_block // GRID_W
    lane = iota((1, LANES), 1)
    by_row = lane % HEAD_DIM < HEAD_DIM // 2
    half = lane < HEAD_DIM
    cols = grid_rows
    total = grid_rows + GRID_W
    col_cos = table_ref[cols : cols + GRID_W, :]
    col_sin = table_ref[total + cols : total + cols + GRID_W, :]

    def tables(first, count):
        cos, sin = [], []
        for i in range(count // GRID_W):
            r = first + i
            cos.append(jnp.where(by_row, table_ref[pl.ds(r, 1), :], col_cos))
            sin.append(jnp.where(by_row, table_ref[pl.ds(total + r, 1), :], col_sin))
        return jnp.concatenate(cos, axis=0), jnp.concatenate(sin, axis=0)

    def turn_keys(source, source_row, target_row, count, grid_row):
        cos, sin = tables(grid_row, count)
        for p in range(pairs):
            part = source[pl.ds(source_row, count), p * LANES : (p + 1) * LANES].astype(F32)
            k_all[pl.ds(target_row, count), p * LANES : (p + 1) * LANES] = rope_block(
                part, cos, sin
            ).astype(BF16)

    if first == 0:
        turn_keys(left_ref, 0, 0, q_block, 0)
        v_all[0:q_block, :] = left_ref[:, kv_width:]
    if first + count == blocks:
        slot = (count + 1) * q_block
        turn_keys(right_ref, 0, slot, q_block, (blocks + 1) * per_block)
        v_all[slot : slot + q_block, :] = right_ref[:, kv_width:]

    def keys_step(w, carry):
        at = pl.multiple_of((w - first) * q_block, q_block)
        turn_keys(k_ref, at, at, q_block, w * per_block)
        return carry

    lax.fori_loop(low, high, keys_step, 0)
    gap = iota((q_block, span), 1) - iota((q_block, span), 0)
    band_ref[...] = jnp.where((gap >= 0) & (gap <= 2 * WINDOW), 0.0, MASKED)

    def block_step(b, carry):
        at = pl.multiple_of(b * q_block, q_block)
        block = b + first
        cos, sin = tables((block + 1) * per_block, q_block)
        place = info_ref[0] + block * q_block - WINDOW + iota((1, span), 1)
        bias = band_ref[...] + jnp.where((place >= 0) & (place < info_ref[1]), 0.0, MASKED)
        for p in range(pairs):
            heads = []
            for c in range(group):
                left = (p * group + c) * LANES
                x = q_ref[pl.ds(at, q_block), left : left + LANES].astype(F32)
                x = rope_block(x, cos, sin).astype(BF16).astype(F32) * HEAD_DIM**-0.5
                swapped = pltpu.roll(x, HEAD_DIM, axis=1)
                low_side = c < group // 2
                for one in (x, swapped) if low_side else (swapped, x):
                    keep = half if low_side else jnp.logical_not(half)
                    heads.append(jnp.where(keep, one, 0.0).astype(BF16))
            keys = k_all[pl.ds(at, span), p * LANES : (p + 1) * LANES]
            values = v_all[pl.ds(at, span), p * LANES : (p + 1) * LANES]
            score_ref[p] = lax.dot_general(
                jnp.concatenate(heads, axis=0), keys, (((1,), (1,)), ((), ())),
                preferred_element_type=F32,
            )
            for h in range(2 * group):
                scores = score_ref[p, h * q_block : (h + 1) * q_block, :] + bias
                sink = sink_ref[p * 2 * group + h]
                peak = jnp.maximum(jnp.max(scores, axis=-1, keepdims=True), sink)
                exps = jnp.exp(scores - peak)
                bottom = jnp.sum(exps, axis=-1, keepdims=True) + jnp.exp(sink - peak)
                chance_ref[p, h * q_block : (h + 1) * q_block, :] = (exps * (1.0 / bottom)).astype(
                    BF16
                )
            blended = jnp.dot(chance_ref[p], values, preferred_element_type=F32)
            done = [blended[h * q_block : (h + 1) * q_block] for h in range(2 * group)]
            for c in range(group):
                one, two = done[2 * c], done[2 * c + 1]
                if c < group // 2:
                    two = pltpu.roll(two, HEAD_DIM, axis=1)
                else:
                    one = pltpu.roll(one, HEAD_DIM, axis=1)
                left = (p * group + c) * LANES
                out_ref[pl.ds(at, q_block), left : left + LANES] = jnp.where(
                    half, one, two
                ).astype(BF16)
        return carry

    lax.fori_loop(0, count, block_step, 0)


def rope_table(rows, first_global):
    grid_rows = (rows + 2 * WINDOW) // GRID_W
    quarter = HEAD_DIM // 4
    freqs = ROPE_BASE ** (-jnp.arange(0, HEAD_DIM // 2, 2, dtype=F32) / (HEAD_DIM // 2))
    lane_freq = jnp.tile(freqs, LANES // quarter)
    row_at = (first_global - WINDOW) // GRID_W + jnp.arange(grid_rows, dtype=jnp.int32)
    spots = jnp.concatenate([row_at, jnp.arange(GRID_W, dtype=jnp.int32)]).astype(F32)
    angles = spots[:, None] * lane_freq[None, :]
    sign = jnp.where(jnp.arange(LANES) % (2 * quarter) < quarter, -1.0, 1.0)
    return jnp.concatenate([jnp.cos(angles), jnp.sin(angles) * sign[None, :]], axis=0)


def attention(q, k, v, left, right, sink, table, info, first, count, after):
    rows = q.shape[0]
    kv_width = k.shape[1]
    group = q.shape[1] // kv_width
    assert kv_width % LANES == 0 and group == 2 and rows % WINDOW == 0
    assert rows % GRID_W == 0 and WINDOW % GRID_W == 0
    q_block = WINDOW
    span = q_block + 2 * WINDOW
    heads = q.shape[1] // HEAD_DIM
    done = count * q_block
    return pl.pallas_call(
        functools.partial(attention_kernel, first, count),
        out_shape=jax.ShapeDtypeStruct((done, q.shape[1]), BF16),
        in_specs=[SMEM, SMEM, VMEM] + [HBM] * 3 + [VMEM] * 2 + [ANY],
        out_specs=VMEM,
        scratch_shapes=[
            pltpu.VMEM((done + 2 * WINDOW, kv_width), BF16),
            pltpu.VMEM((done + 2 * WINDOW, kv_width), BF16),
            pltpu.VMEM((q_block, span), F32),
            pltpu.VMEM((kv_width // LANES, 2 * group * q_block, span), F32),
            pltpu.VMEM((kv_width // LANES, 2 * group * q_block, span), BF16),
            pltpu.VMEM((done, q.shape[1]), BF16),
            pltpu.VMEM((done + 2 * WINDOW, kv_width), BF16),
            pltpu.SemaphoreType.DMA((3,)),
        ],
        cost_estimate=pl.CostEstimate(
            flops=24 * done * span * heads * HEAD_DIM,
            transcendentals=done * span * heads,
            bytes_accessed=8 * rows * kv_width * 2,
        ),
        compiler_params=params(16),
        name="attention",
    )(info, sink, table, q, k, v, left, right, after)


def mixer_kernel(rows_ref, weight_hbm, out_ref, weight_ref, total_ref, sems):
    parts, _, part = rows_ref.shape
    width = out_ref.shape[1]
    step = math.gcd(width, 512)
    spots = [slice(i * part, (i + 1) * part) for i in range(parts)]
    loads = [
        pltpu.make_async_copy(weight_hbm.at[spot, :], weight_ref.at[spot, :], sems.at[i])
        for i, spot in enumerate(spots)
    ]
    for load in loads:
        load.start()
    for i, spot in enumerate(spots):
        loads[i].wait()
        for left in range(0, width, step):
            cut = slice(left, left + step)
            total = jnp.dot(rows_ref[i], weight_ref[spot, cut], preferred_element_type=F32)
            if i:
                total = total + total_ref[:, cut]
            if i < parts - 1:
                total_ref[:, cut] = total
            else:
                out_ref[:, cut] = total.astype(BF16)


def mix(rows, weight):
    parts, tokens, _ = rows.shape
    width = weight.shape[1]
    return pl.pallas_call(
        mixer_kernel,
        out_shape=jax.ShapeDtypeStruct((tokens, width), BF16),
        in_specs=[VMEM, HBM],
        out_specs=VMEM,
        scratch_shapes=[
            pltpu.VMEM(weight.shape, BF16),
            pltpu.VMEM((tokens, width), F32),
            pltpu.SemaphoreType.DMA((parts,)),
        ],
        compiler_params=params(18),
        cost_estimate=cost(3e9),
        name="mixer",
    )(rows, pltpu.with_memory_space_constraint(weight, pltpu.HBM))


def relay(x, axis):
    return lax.ppermute(x, axis, [(0, 1), (1, 0)])


def layer(
    queries,
    key_heads,
    value_heads,
    sink_logits,
    mix_weight,
    expert_input,
    norm_gain,
    routes,
    route_weights,
    gate_weight,
    up_weight,
    down_weight,
):
    ring = ("zh", "zl", "xx")
    inner = ("xx", "tp")
    ring_size = lax.axis_size(ring)
    tp_size = lax.axis_size("tp")
    plane = lax.axis_size(inner)
    experts_all = ring_size * tp_size
    tok_local, top = routes.shape
    cap = 2 * tok_local * top // experts_all
    xor = plane <= 8 and plane & (plane - 1) == 0 and plane > 1
    pieces = plane // 2 if xor else 1
    plan = (top, cap, pieces if xor else plane, xor)
    position = lax.axis_index(inner)
    base = lax.axis_index(("zh", "zl")) * plane
    where = jnp.stack([base, position]).astype(jnp.int32)

    def mate(x, step):
        return lax.ppermute(x, inner, [(i, i ^ step) for i in range(plane)])

    def both(x):
        return [x, mate(x, 1)] if xor else [x]

    def exchange(parts):
        if not xor:
            block = parts[0].reshape(-1, plane, cap, parts[0].shape[1]).swapaxes(0, 1)
            turned = lax.all_to_all(block, inner, 0, 0, tiled=True)
            return [turned.swapaxes(0, 1).reshape(parts[0].shape)]
        return [parts[0]] + [mate(parts[p], 2 * p) for p in range(1, pieces)]

    own = make_payload(expert_input, norm_gain, routes, route_weights)
    near = relay(own, "zl")
    far = relay(own, "zh")
    far_near = relay(far, "zl")

    rows_here = queries.shape[0]
    first_global = lax.axis_index(ring) * rows_here
    tail = jnp.concatenate([key_heads[-WINDOW:], value_heads[-WINDOW:]], axis=1)
    head = jnp.concatenate([key_heads[:WINDOW], value_heads[:WINDOW]], axis=1)
    ends = ring_size - 1
    left = lax.ppermute(tail, ring, [(i, i + 1) for i in range(ends)])
    right = lax.ppermute(head, ring, [(i + 1, i) for i in range(ends)])
    table = rope_table(rows_here, first_global)
    info = jnp.stack([first_global, jnp.int32(rows_here * ring_size)]).astype(jnp.int32)
    blocks = rows_here // WINDOW

    def attend(i, after):
        return attention(
            queries, key_heads, value_heads, right if i else left, left if not i else right,
            sink_logits, table, info,
            i * (blocks // 2), blocks // 2, after,
        )

    chunks = [both(x) for x in (own, near, far, far_near)]

    def send(i, after):
        parts = dispatch(plan, pieces, where, chunks[i], after)
        return exchange(parts), parts[0]

    held = [
        pltpu.with_memory_space_constraint(w, pltpu.VMEM)
        for w in (gate_weight, up_weight, down_weight)
    ]

    def work(i, after):
        return experts(arrived[i], held, after)

    arrived, made = {}, {}
    arrived[0], sent = send(0, [])
    arrived[1], sent = send(1, [sent])
    arrived[2], sent = send(2, [sent])
    made[0] = work(0, [sent])
    arrived[3], sent = send(3, [made[0][0]])
    made[1] = work(1, [sent])
    made[2] = work(2, [made[1][0]])
    upper = attend(0, made[2][0])
    made[3] = work(3, [upper])
    lower = attend(1, made[3][0])
    attended = jnp.concatenate([upper, lower], axis=0)

    back = {i: exchange(made[i]) for i in (3, 2, 1, 0)}
    tp_blocks = attended.reshape(tp_size, rows_here // tp_size, attended.shape[1])
    token_rows = lax.all_to_all(tp_blocks, "tp", split_axis=0, concat_axis=0, tiled=True)
    mixer_out = mix(token_rows, mix_weight)

    def gather(i, after):
        own_part, *other = combine(plan, where, chunks[i], back[i], after)
        return [own_part] + [mate(x, 1) for x in other], own_part

    def total(parts):
        return sum(x.astype(F32) for x in parts).astype(BF16)

    parts, done = gather(3, [])
    last = total(parts)
    parts, done = gather(2, [last])
    mid = total(parts + [relay(last, "zl")])
    parts, done = gather(1, [done])
    side = total(parts)
    parts, _ = gather(0, [done])
    summed = total(parts + [relay(side, "zl"), relay(mid, "zh")])
    return (mixer_out, summed)


def solution(mesh):
    n_ep, n_tp = mesh.shape["ep"], mesh.shape["tp"]
    assert n_ep % 4 == 0
    fine = Mesh(mesh.devices.reshape(2, 2, n_ep // 4, n_tp), ("zh", "zl", "xx", "tp"))
    ring = ("zh", "zl", "xx")
    every = ring + ("tp",)
    return jax.shard_map(
        layer,
        mesh=fine,
        in_specs=(
            P(ring, "tp"),
            P(ring, "tp"),
            P(ring, "tp"),
            P("tp"),
            P(),
            P(every, None),
            P(),
            P(every, None),
            P(every, None),
            P(every, None, None),
            P(every, None, None),
            P(every, None, None),
        ),
        out_specs=(P(every, None), P(every, None)),
        check_vma=False,
    )
```

profile of v0, /device:TPU:0, one launch (start us, length us, event | category | flops | bytes accessed | tf_op | source)
XLA Modules:
  0.0 199.8 jit_solution(503741188890258291)
XLA Ops:
  0.6 1.4 norm.1.refs_0_
  2.6 2.6 %collective-permute-start.3 = (bf16[128,2176]{1,0:T(8,128)(2,1)S(1)}, bf16[128,2176]{1,0:T(8,128)(2,1)S(1)}, u32[]{:S(2)}, u32[]{:S(2)}) collective-permute-start(bf16[128,2176]{1,0:T(8,128)(2,1)S(1)} %norm.1.refs_0_), channel_id=1, source_target_pairs={{0,8},{8,0},{1,9},{9,1},{2,10},{10,2},{3,11},{11,3},{4,12},{12,4},... | collective-permute-start | bytes 1671176 | tf_op jit(solution)/shard_map/ppermute | solution.py:452
  5.3 2.6 %collective-permute-start.1 = (bf16[128,2176]{1,0:T(8,128)(2,1)S(1)}, bf16[128,2176]{1,0:T(8,128)(2,1)S(1)}, u32[]{:S(2)}, u32[]{:S(2)}) collective-permute-start(bf16[128,2176]{1,0:T(8,128)(2,1)S(1)} %norm.1.refs_0_), channel_id=1, source_target_pairs={{0,16},{16,0},{1,17},{17,1},{2,18},{18,2},{3,19},{19,3},{4,20},{20... | collective-permute-start | bytes 1671176 | tf_op jit(solution)/shard_map/ppermute | solution.py:452
  9.3 21.0 %collective-permute-done.3.refs_0_ = bf16[128,2176]{1,0:T(8,128)(2,1)S(1)} collective-permute-done((bf16[128,2176]{1,0:T(8,128)(2,1)S(1)}, bf16[128,2176]{1,0:T(8,128)(2,1)S(1)}, u32[]{:S(2)}, u32[]{:S(2)}) %collective-permute-start.3) | collective-permute-done | bytes 557088 | tf_op jit(solution)/shard_map/ppermute | solution.py:452
  30.3 2.5 %collective-permute-done.1.refs_0_ = bf16[128,2176]{1,0:T(8,128)(2,1)S(1)} collective-permute-done((bf16[128,2176]{1,0:T(8,128)(2,1)S(1)}, bf16[128,2176]{1,0:T(8,128)(2,1)S(1)}, u32[]{:S(2)}, u32[]{:S(2)}) %collective-permute-start.1) | collective-permute-done | bytes 557088 | tf_op jit(solution)/shard_map/ppermute | solution.py:452
  33.6 1.7 dispatch.4
  35.3 1.6 collective-permute-start.14
  36.9 1.5 collective-permute-start.15
  38.9 6.7 %collective-permute-done.12.refs_0_ = bf16[128,2176]{1,0:T(8,128)(2,1)S(1)} collective-permute-done((bf16[128,2176]{1,0:T(8,128)(2,1)S(1)}, bf16[128,2176]{1,0:T(8,128)(2,1)S(1)}, u32[]{:S(2)}, u32[]{:S(2)}) %collective-permute-start.12) | collective-permute-done | bytes 557088 | tf_op jit(solution)/shard_map/ppermute | solution.py:452
  45.6 1.7 dispatch.5
  47.3 3.8 %collective-permute-start = (bf16[128,512]{1,0:T(8,128)(2,1)S(1)}, bf16[128,512]{1,0:T(8,128)(2,1)S(1)}, u32[]{:S(2)}, u32[]{:S(2)}) collective-permute-start(bf16[128,512]{1,0:T(8,128)(2,1)S(1)} %pad_maximum_fusion.1), channel_id=1, source_target_pairs={{0,4},{4,8},{8,12},{12,16},{16,20},{20,24},{24,28},{1,5},{5,9},{9,... | collective-permute-start | bytes 393224 | tf_op jit(solution)/shard_map/ppermute | solution.py:507
  51.2 1.7 dispatch.6
  52.9 1.6 collective-permute-start.9
  54.5 1.7 collective-permute-start.10
  56.5 3.5 %experts.4 = (bf16[64,2048]{1,0:T(8,128)(2,1)S(1)}, bf16[64,2048]{1,0:T(8,128)(2,1)S(1)}, bf16[64,2048]{1,0:T(8,128)(2,1)S(1)}, bf16[64,2048]{1,0:T(8,128)(2,1)S(1)}) custom-call(bf16[1,2048,1024]{2,1,0:T(8,128)(2,1)S(1)} %copy-done, bf16[1,2048,1024]{2,1,0:T(8,128)(2,1)S(1)} %copy-done.1, bf16[1,1024,2048]{2,1,0:T(8,128)(2,1)S(1)} %copy-done.2, ...), custom_call_target="tpu_custom_call" | custom-call | flops 3221225472 | bytes 2097152 | tf_op jit(solution)/shard_map/experts/pallas_call | solution.py:219
  60.0 1.6 collective-permute-start.6
  61.6 1.7 dispatch.7
  63.3 1.8 collective-permute-start.7
  65.4 3.9 %collective-permute-done.11.refs_3_ = bf16[64,2048]{1,0:T(8,128)(2,1)S(1)} collective-permute-done((bf16[64,2048]{1,0:T(8,128)(2,1)S(1)}, bf16[64,2048]{1,0:T(8,128)(2,1)S(1)}, u32[]{:S(2)}, u32[]{:S(2)}) %collective-permute-start.11) | collective-permute-done | bytes 262176 | tf_op jit(solution)/shard_map/ppermute | solution.py:485
  69.3 1.5 collective-permute-start.18
  70.8 3.5 %experts.5 = (bf16[64,2048]{1,0:T(8,128)(2,1)S(1)}, bf16[64,2048]{1,0:T(8,128)(2,1)S(1)}, bf16[64,2048]{1,0:T(8,128)(2,1)S(1)}, bf16[64,2048]{1,0:T(8,128)(2,1)S(1)}) custom-call(bf16[1,2048,1024]{2,1,0:T(8,128)(2,1)S(1)} %copy-done, bf16[1,2048,1024]{2,1,0:T(8,128)(2,1)S(1)} %copy-done.1, bf16[1,1024,2048]{2,1,0:T(8,128)(2,1)S(1)} %copy-done.2, ...), custom_call_target="tpu_custom_call" | custom-call | flops 3221225472 | bytes 2097152 | tf_op jit(solution)/shard_map/experts/pallas_call | solution.py:219
  74.9 1.7 collective-permute-start.19
  76.6 1.2 collective-permute-start.20
  77.8 2.7 %collective-permute-done.8.refs_3_ = bf16[64,2048]{1,0:T(8,128)(2,1)S(1)} collective-permute-done((bf16[64,2048]{1,0:T(8,128)(2,1)S(1)}, bf16[64,2048]{1,0:T(8,128)(2,1)S(1)}, u32[]{:S(2)}, u32[]{:S(2)}) %collective-permute-start.8) | collective-permute-done | bytes 262176 | tf_op jit(solution)/shard_map/ppermute | solution.py:485
  80.6 3.5 %experts.6 = (bf16[64,2048]{1,0:T(8,128)(2,1)S(1)}, bf16[64,2048]{1,0:T(8,128)(2,1)S(1)}, bf16[64,2048]{1,0:T(8,128)(2,1)S(1)}, bf16[64,2048]{1,0:T(8,128)(2,1)S(1)}) custom-call(bf16[1,2048,1024]{2,1,0:T(8,128)(2,1)S(1)} %copy-done, bf16[1,2048,1024]{2,1,0:T(8,128)(2,1)S(1)} %copy-done.1, bf16[1,1024,2048]{2,1,0:T(8,128)(2,1)S(1)} %copy-done.2, ...), custom_call_target="tpu_custom_call" | custom-call | flops 3221225472 | bytes 2097152 | tf_op jit(solution)/shard_map/experts/pallas_call | solution.py:219
  84.2 7.5 %attention.2.refs_4_ = bf16[512,512]{1,0:T(8,128)(2,1)S(1)} custom-call(s32[2]{0:T(128)S(1)} %pad_add_fusion.info_ref, f32[8]{0:T(128)S(1)} %copy-done.12, f32[168,128]{1,0:T(8,128)S(1)} %pad_maximum_fusion.3.table_ref, bf16[1024,512]{1,0:T(8,128)(2,1)S(1)} %copy-done.7, bf16[1024,256]{1,0:T(8,128)(2,1)S(1)} %copy-done.5, bf16[1024,256]{1,0:T(8,128)(2,1)S(1)} %copy-done.6, ...), custom_call_target="tpu_custom_call" | custom-call | flops 2415919104 | bytes 4194304 | tf_op jit(solution)/shard_map/attention/pallas_call | solution.py:383
  91.7 3.5 %experts.7 = (bf16[64,2048]{1,0:T(8,128)(2,1)S(1)}, bf16[64,2048]{1,0:T(8,128)(2,1)S(1)}, bf16[64,2048]{1,0:T(8,128)(2,1)S(1)}, bf16[64,2048]{1,0:T(8,128)(2,1)S(1)}) custom-call(bf16[1,2048,1024]{2,1,0:T(8,128)(2,1)S(1)} %copy-done, bf16[1,2048,1024]{2,1,0:T(8,128)(2,1)S(1)} %copy-done.1, bf16[1,1024,2048]{2,1,0:T(8,128)(2,1)S(1)} %copy-done.2, ...), custom_call_target="tpu_custom_call" | custom-call | flops 3221225472 | bytes 2097152 | tf_op jit(solution)/shard_map/experts/pallas_call | solution.py:219
  95.2 1.6 collective-permute-start.30
  96.8 1.7 collective-permute-start.31
  98.8 4.8 %collective-permute-done.30.refs_3_ = bf16[64,2048]{1,0:T(8,128)(2,1)S(1)} collective-permute-done((bf16[64,2048]{1,0:T(8,128)(2,1)S(1)}, bf16[64,2048]{1,0:T(8,128)(2,1)S(1)}, u32[]{:S(2)}, u32[]{:S(2)}) %collective-permute-start.30) | collective-permute-done | bytes 262176 | tf_op jit(solution)/shard_map/ppermute | solution.py:485
  103.6 2.1 %collective-permute-done.31.refs_4_ = bf16[64,2048]{1,0:T(8,128)(2,1)S(1)} collective-permute-done((bf16[64,2048]{1,0:T(8,128)(2,1)S(1)}, bf16[64,2048]{1,0:T(8,128)(2,1)S(1)}, u32[]{:S(2)}, u32[]{:S(2)}) %collective-permute-start.31) | collective-permute-done | bytes 262176 | tf_op jit(solution)/shard_map/ppermute | solution.py:485
  105.7 2.8 %collective-permute-done.32.refs_5_ = bf16[64,2048]{1,0:T(8,128)(2,1)S(1)} collective-permute-done((bf16[64,2048]{1,0:T(8,128)(2,1)S(1)}, bf16[64,2048]{1,0:T(8,128)(2,1)S(1)}, u32[]{:S(2)}, u32[]{:S(2)}) %collective-permute-start.32) | collective-permute-done | bytes 262176 | tf_op jit(solution)/shard_map/ppermute | solution.py:485
  108.5 1.9 combine.4
  110.4 1.6 collective-permute-start.27
  112.0 1.8 collective-permute-start.28
  114.1 1.5 collective-permute-start.24
  115.6 4.2 %collective-permute-done.27.refs_3_ = bf16[64,2048]{1,0:T(8,128)(2,1)S(1)} collective-permute-done((bf16[64,2048]{1,0:T(8,128)(2,1)S(1)}, bf16[64,2048]{1,0:T(8,128)(2,1)S(1)}, u32[]{:S(2)}, u32[]{:S(2)}) %collective-permute-start.27) | collective-permute-done | bytes 262176 | tf_op jit(solution)/shard_map/ppermute | solution.py:485
  119.8 1.7 collective-permute-start.25
  121.5 1.2 collective-permute-start.26
  123.6 1.3 collective-permute-start.17
  124.9 2.0 collective-permute-done.29.refs_5_
  126.9 1.5 collective-permute-start.21
  128.4 2.7 %combine.5 = (f32[128,2048]{1,0:T(8,128)S(1)}, bf16[128,2048]{1,0:T(8,128)(2,1)}) custom-call(s32[2]{0:T(128)S(1)} %pad_add_fusion.1.where_ref, bf16[128,2176]{1,0:T(8,128)(2,1)S(1)} %collective-permute-done.1.refs_0_, bf16[128,2176]{1,0:T(8,128)(2,1)S(1)} %collective-permute-done.2.refs_1_, bf16[64,2048]{1,0:T(8,128)(2,1)S(1)} %get-tuple-element.57.after_ref.refs_2_, ...), custom_call_target="tpu_custom_call" | custom-call | flops 2000000000 | bytes 1048576 | tf_op jit(solution)/shard_map/combine/pallas_call | solution.py:179
  131.1 1.8 collective-permute-start.22
  132.8 1.8 collective-permute-done.25.refs_4_
  134.6 2.4 %collective-permute-start.23 = (bf16[64,2048]{1,0:T(8,128)(2,1)S(1)}, bf16[64,2048]{1,0:T(8,128)(2,1)}, u32[]{:S(2)}, u32[]{:S(2)}) collective-permute-start(bf16[64,2048]{1,0:T(8,128)(2,1)S(1)} %get-tuple-element.64), channel_id=1, source_target_pairs={{0,6},{1,7},{2,4},{3,5},{4,2},{5,3},{6,0},{7,1},{8,14},{9,15},{10,... | collective-permute-start | bytes 786440 | tf_op jit(solution)/shard_map/ppermute | solution.py:485
  137.0 3.3 %collective-permute-done.26.refs_5_ = bf16[64,2048]{1,0:T(8,128)(2,1)S(1)} collective-permute-done((bf16[64,2048]{1,0:T(8,128)(2,1)S(1)}, bf16[64,2048]{1,0:T(8,128)(2,1)S(1)}, u32[]{:S(2)}, u32[]{:S(2)}) %collective-permute-start.26) | collective-permute-done | bytes 262176 | tf_op jit(solution)/shard_map/ppermute | solution.py:485
  140.3 2.7 %combine.6 = (f32[128,2048]{1,0:T(8,128)S(1)}, bf16[128,2048]{1,0:T(8,128)(2,1)}) custom-call(s32[2]{0:T(128)S(1)} %pad_add_fusion.1.where_ref, bf16[128,2176]{1,0:T(8,128)(2,1)S(1)} %collective-permute-done.3.refs_0_, bf16[128,2176]{1,0:T(8,128)(2,1)S(1)} %collective-permute-done.4.refs_1_, bf16[64,2048]{1,0:T(8,128)(2,1)S(1)} %get-tuple-element.56.refs_4_.refs_2_, ...), custom_call_target="tpu_custom_call" | custom-call | flops 2000000000 | bytes 1048576 | tf_op jit(solution)/shard_map/combine/pallas_call | solution.py:179
  143.0 1.0 copy-done.3
  144.0 7.3 %attention.3 = bf16[512,512]{1,0:T(8,128)(2,1)S(1)} custom-call(s32[2]{0:T(128)S(1)} %pad_add_fusion.info_ref, f32[8]{0:T(128)S(1)} %copy-done.12, f32[168,128]{1,0:T(8,128)S(1)} %pad_maximum_fusion.3.table_ref, bf16[1024,512]{1,0:T(8,128)(2,1)S(1)} %copy-done.7, bf16[1024,256]{1,0:T(8,128)(2,1)S(1)} %copy-done.5, bf16[1024,256]{1,0:T(8,128)(2,1)S(1)} %copy-done.6, ...), custom_call_target="tpu_custom_call" | custom-call | flops 2415919104 | bytes 4194304 | tf_op jit(solution)/shard_map/attention/pallas_call | solution.py:383
  151.3 1.0 pad_maximum_fusion
  152.3 3.8 %all-to-all-start = ((bf16[4,256,512]{2,1,0:T(8,128)(2,1)}), bf16[4,256,512]{2,1,0:T(8,128)(2,1)S(1)}, u32[]{:S(2)}, u32[]{:S(2)}) async-start(bf16[4,256,512]{2,1,0:T(8,128)(2,1)} %bitcast.7), calls=%async_computation | async-start | bytes 2097152 | tf_op jit(solution)/shard_map/all_to_all | solution.py:549
  156.1 1.2 collective-permute-start.38
  157.6 1.2 copy-done.4
  158.8 1.1 copy-done.9
  159.8 1.1 copy-done.11
  160.9 3.2 %combine.7 = (f32[128,2048]{1,0:T(8,128)S(1)}, bf16[128,2048]{1,0:T(8,128)(2,1)}) custom-call(s32[2]{0:T(128)S(1)} %pad_add_fusion.1.where_ref, bf16[128,2176]{1,0:T(8,128)(2,1)S(1)} %copy-done.9, bf16[128,2176]{1,0:T(8,128)(2,1)S(1)} %copy-done.11, bf16[64,2048]{1,0:T(8,128)(2,1)S(1)} %get-tuple-element.54.refs_2_, ...), custom_call_target="tpu_custom_call" | custom-call | flops 2000000000 | bytes 1048576 | tf_op jit(solution)/shard_map/combine/pallas_call | solution.py:179
  164.4 2.3 %add_convert_fusion.2 = bf16[128,2048]{1,0:T(8,128)(2,1)} fusion(f32[128,2048]{1,0:T(8,128)} %copy-done.3, bf16[128,2048]{1,0:T(8,128)(2,1)} %collective-permute-done.35), kind=kLoop, calls=%fused_computation.3 | loop fusion | flops 786432 | bytes 2097152 | tf_op jit(solution)/shard_map/convert_element_type | solution.py:557
  167.6 3.6 %collective-permute-done.38 = bf16[128,2048]{1,0:T(8,128)(2,1)S(1)} collective-permute-done((bf16[128,2048]{1,0:T(8,128)(2,1)}, bf16[128,2048]{1,0:T(8,128)(2,1)S(1)}, u32[]{:S(2)}, u32[]{:S(2)}) %collective-permute-start.38) | collective-permute-done | bytes 524320 | tf_op jit(solution)/shard_map/ppermute | solution.py:452
  172.2 2.4 %collective-permute-start.39 = (bf16[128,2048]{1,0:T(8,128)(2,1)}, bf16[128,2048]{1,0:T(8,128)(2,1)S(1)}, u32[]{:S(2)}, u32[]{:S(2)}) collective-permute-start(bf16[128,2048]{1,0:T(8,128)(2,1)} %add_convert_fusion.1), channel_id=1, source_target_pairs={{0,16},{16,0},{1,17},{17,1},{2,18},{18,2},{3,19},{19,3},{4,20},{20... | collective-permute-start | bytes 1572872 | tf_op jit(solution)/shard_map/ppermute | solution.py:452
  174.5 5.2 %mixer.1 = bf16[256,2048]{1,0:T(8,128)(2,1)} custom-call(bf16[4,256,512]{2,1,0:T(8,128)(2,1)S(1)} %all-to-all-done.rows_ref, bf16[2048,2048]{1,0:T(8,128)(2,1)} %weight_hbm.1), custom_call_target="tpu_custom_call" | custom-call | flops 3000000000 | bytes 1048576 | tf_op jit(solution)/shard_map/mixer/pallas_call | solution.py:435
  179.7 11.1 %collective-permute-done.36 = bf16[128,2048]{1,0:T(8,128)(2,1)} collective-permute-done((bf16[128,2048]{1,0:T(8,128)(2,1)}, bf16[128,2048]{1,0:T(8,128)(2,1)}, u32[]{:S(2)}, u32[]{:S(2)}) %collective-permute-start.36) | collective-permute-done | bytes 524320 | tf_op jit(solution)/shard_map/ppermute | solution.py:452
  190.8 6.8 %collective-permute-done.39 = bf16[128,2048]{1,0:T(8,128)(2,1)S(1)} collective-permute-done((bf16[128,2048]{1,0:T(8,128)(2,1)}, bf16[128,2048]{1,0:T(8,128)(2,1)S(1)}, u32[]{:S(2)}, u32[]{:S(2)}) %collective-permute-start.39) | collective-permute-done | bytes 524320 | tf_op jit(solution)/shard_map/ppermute | solution.py:452
  197.6 2.3 %add_convert_fusion = bf16[128,2048]{1,0:T(8,128)(2,1)} fusion(bf16[128,2048]{1,0:T(8,128)(2,1)S(1)} %collective-permute-done.39, bf16[128,2048]{1,0:T(8,128)(2,1)} %collective-permute-done.36, f32[128,2048]{1,0:T(8,128)S(1)} %get-tuple-element.78, bf16[128,2048]{1,0:T(8,128)(2,1)} %collective-permute-done.34), kind=kLoop, calls=%fused_computation.1 | loop fusion | flops 1835008 | bytes 3145728 | tf_op jit(solution)/shard_map/convert_element_type | solution.py:557
  (79 shorter events, 8.1 us)
Async XLA Ops:
  2.1 33.2 %copy-start.8 = (bf16[128,2176]{1,0:T(8,128)(2,1)}, bf16[128,2176]{1,0:T(8,128)(2,1)S(1)}, u32[]{:S(2)}) copy-start(bf16[128,2176]{1,0:T(8,128)(2,1)S(1)} %norm.1.refs_0_) | copy-start | bytes 1671172
  2.1 31.5 %collective-permute-start.5 = (bf16[128,2176]{1,0:T(8,128)(2,1)S(1)}, bf16[128,2176]{1,0:T(8,128)(2,1)S(1)}, u32[]{:S(2)}, u32[]{:S(2)}) collective-permute-start(bf16[128,2176]{1,0:T(8,128)(2,1)S(1)} %norm.1.refs_0_), channel_id=1, source_target_pairs={{0,1},{1,0},{2,3},{3,2},{4,5},{5,4},{6,7},{7,6},{8,9},{9,8},{10,11... | collective-permute-start | bytes 1671176 | tf_op jit(solution)/shard_map/ppermute | solution.py:485
  2.6 27.7 %collective-permute-start.3 = (bf16[128,2176]{1,0:T(8,128)(2,1)S(1)}, bf16[128,2176]{1,0:T(8,128)(2,1)S(1)}, u32[]{:S(2)}, u32[]{:S(2)}) collective-permute-start(bf16[128,2176]{1,0:T(8,128)(2,1)S(1)} %norm.1.refs_0_), channel_id=1, source_target_pairs={{0,8},{8,0},{1,9},{9,1},{2,10},{10,2},{3,11},{11,3},{4,12},{12,4},... | collective-permute-start | bytes 1671176 | tf_op jit(solution)/shard_map/ppermute | solution.py:452
  5.3 27.6 %collective-permute-start.1 = (bf16[128,2176]{1,0:T(8,128)(2,1)S(1)}, bf16[128,2176]{1,0:T(8,128)(2,1)S(1)}, u32[]{:S(2)}, u32[]{:S(2)}) collective-permute-start(bf16[128,2176]{1,0:T(8,128)(2,1)S(1)} %norm.1.refs_0_), channel_id=1, source_target_pairs={{0,16},{16,0},{1,17},{17,1},{2,18},{18,2},{3,19},{19,3},{4,20},{20... | collective-permute-start | bytes 1671176 | tf_op jit(solution)/shard_map/ppermute | solution.py:452
  30.3 8.0 %collective-permute-start.4 = (bf16[128,2176]{1,0:T(8,128)(2,1)S(1)}, bf16[128,2176]{1,0:T(8,128)(2,1)S(1)}, u32[]{:S(2)}, u32[]{:S(2)}) collective-permute-start(bf16[128,2176]{1,0:T(8,128)(2,1)S(1)} %collective-permute-done.3.refs_0_), channel_id=1, source_target_pairs={{0,1},{1,0},{2,3},{3,2},{4,5},{5,4},{6,7},{7,6},{8,9},{9,8},{10,11... | collective-permute-start | bytes 1671176 | tf_op jit(solution)/shard_map/ppermute | solution.py:485
  32.8 12.8 %collective-permute-start.12 = (bf16[128,2176]{1,0:T(8,128)(2,1)S(1)}, bf16[128,2176]{1,0:T(8,128)(2,1)S(1)}, u32[]{:S(2)}, u32[]{:S(2)}) collective-permute-start(bf16[128,2176]{1,0:T(8,128)(2,1)S(1)} %collective-permute-done.1.refs_0_), channel_id=1, source_target_pairs={{0,8},{8,0},{1,9},{9,1},{2,10},{10,2},{3,11},{11,3},{4,12},{12,4},... | collective-permute-start | bytes 1671176 | tf_op jit(solution)/shard_map/ppermute | solution.py:452
  33.4 14.0 %collective-permute-start.2 = (bf16[128,2176]{1,0:T(8,128)(2,1)S(1)}, bf16[128,2176]{1,0:T(8,128)(2,1)S(1)}, u32[]{:S(2)}, u32[]{:S(2)}) collective-permute-start(bf16[128,2176]{1,0:T(8,128)(2,1)S(1)} %collective-permute-done.1.refs_0_), channel_id=1, source_target_pairs={{0,1},{1,0},{2,3},{3,2},{4,5},{5,4},{6,7},{7,6},{8,9},{9,8},{10,11... | collective-permute-start | bytes 1671176 | tf_op jit(solution)/shard_map/ppermute | solution.py:485
  33.6 13.7 %copy-start.10 = (bf16[128,2176]{1,0:T(8,128)(2,1)}, bf16[128,2176]{1,0:T(8,128)(2,1)S(1)}, u32[]{:S(2)}) copy-start(bf16[128,2176]{1,0:T(8,128)(2,1)S(1)} %collective-permute-done.5.refs_1_) | copy-start | bytes 1671172
  35.3 17.6 %collective-permute-start.14 = (bf16[64,2048]{1,0:T(8,128)(2,1)S(1)}, bf16[64,2048]{1,0:T(8,128)(2,1)S(1)}, u32[]{:S(2)}, u32[]{:S(2)}) collective-permute-start(bf16[64,2048]{1,0:T(8,128)(2,1)S(1)} %get-tuple-element.51), channel_id=1, source_target_pairs={{0,2},{1,3},{2,0},{3,1},{4,6},{5,7},{6,4},{7,5},{8,10},{9,11},{10,... | collective-permute-start | bytes 786440 | tf_op jit(solution)/shard_map/ppermute | solution.py:485
  36.9 17.6 %collective-permute-start.15 = (bf16[64,2048]{1,0:T(8,128)(2,1)S(1)}, bf16[64,2048]{1,0:T(8,128)(2,1)S(1)}, u32[]{:S(2)}, u32[]{:S(2)}) collective-permute-start(bf16[64,2048]{1,0:T(8,128)(2,1)S(1)} %get-tuple-element.52), channel_id=1, source_target_pairs={{0,4},{1,5},{2,6},{3,7},{4,0},{5,1},{6,2},{7,3},{8,12},{9,13},{10,... | collective-permute-start | bytes 786440 | tf_op jit(solution)/shard_map/ppermute | solution.py:485
  38.4 17.8 %collective-permute-start.16 = (bf16[64,2048]{1,0:T(8,128)(2,1)S(1)}, bf16[64,2048]{1,0:T(8,128)(2,1)S(1)}, u32[]{:S(2)}, u32[]{:S(2)}) collective-permute-start(bf16[64,2048]{1,0:T(8,128)(2,1)S(1)} %get-tuple-element.53), channel_id=1, source_target_pairs={{0,6},{1,7},{2,4},{3,5},{4,2},{5,3},{6,0},{7,1},{8,14},{9,15},{10,... | collective-permute-start | bytes 786440 | tf_op jit(solution)/shard_map/ppermute | solution.py:485
  45.6 14.4 %collective-permute-start.13 = (bf16[128,2176]{1,0:T(8,128)(2,1)S(1)}, bf16[128,2176]{1,0:T(8,128)(2,1)S(1)}, u32[]{:S(2)}, u32[]{:S(2)}) collective-permute-start(bf16[128,2176]{1,0:T(8,128)(2,1)S(1)} %collective-permute-done.12.refs_0_), channel_id=1, source_target_pairs={{0,1},{1,0},{2,3},{3,2},{4,5},{5,4},{6,7},{7,6},{8,9},{9,8},{10,11... | collective-permute-start | bytes 1671176 | tf_op jit(solution)/shard_map/ppermute | solution.py:485
  45.6 10.9 %copy-start.1 = (bf16[1,2048,1024]{2,1,0:T(8,128)(2,1)S(1)}, bf16[1,2048,1024]{2,1,0:T(8,128)(2,1)}, u32[]{:S(2)}) copy-start(bf16[1,2048,1024]{2,1,0:T(8,128)(2,1)} %up_ref.7) | copy-start | bytes 12582916
  45.6 10.9 %copy-start.2 = (bf16[1,1024,2048]{2,1,0:T(8,128)(2,1)S(1)}, bf16[1,1024,2048]{2,1,0:T(8,128)(2,1)}, u32[]{:S(2)}) copy-start(bf16[1,1024,2048]{2,1,0:T(8,128)(2,1)} %down_ref.7) | copy-start | bytes 12582916
  47.3 9.1 %copy-start = (bf16[1,2048,1024]{2,1,0:T(8,128)(2,1)S(1)}, bf16[1,2048,1024]{2,1,0:T(8,128)(2,1)}, u32[]{:S(2)}) copy-start(bf16[1,2048,1024]{2,1,0:T(8,128)(2,1)} %gate_ref.7) | copy-start | bytes 12582916
  47.3 36.8 %collective-permute-start = (bf16[128,512]{1,0:T(8,128)(2,1)S(1)}, bf16[128,512]{1,0:T(8,128)(2,1)S(1)}, u32[]{:S(2)}, u32[]{:S(2)}) collective-permute-start(bf16[128,512]{1,0:T(8,128)(2,1)S(1)} %pad_maximum_fusion.1), channel_id=1, source_target_pairs={{0,4},{4,8},{8,12},{12,16},{16,20},{20,24},{24,28},{1,5},{5,9},{9,... | collective-permute-start | bytes 393224 | tf_op jit(solution)/shard_map/ppermute | solution.py:507
  52.9 10.4 %collective-permute-start.9 = (bf16[64,2048]{1,0:T(8,128)(2,1)S(1)}, bf16[64,2048]{1,0:T(8,128)(2,1)S(1)}, u32[]{:S(2)}, u32[]{:S(2)}) collective-permute-start(bf16[64,2048]{1,0:T(8,128)(2,1)S(1)} %get-tuple-element.48), channel_id=1, source_target_pairs={{0,2},{1,3},{2,0},{3,1},{4,6},{5,7},{6,4},{7,5},{8,10},{9,11},{10,... | collective-permute-start | bytes 786440 | tf_op jit(solution)/shard_map/ppermute | solution.py:485
  54.5 10.6 %collective-permute-start.10 = (bf16[64,2048]{1,0:T(8,128)(2,1)S(1)}, bf16[64,2048]{1,0:T(8,128)(2,1)S(1)}, u32[]{:S(2)}, u32[]{:S(2)}) collective-permute-start(bf16[64,2048]{1,0:T(8,128)(2,1)S(1)} %get-tuple-element.49), channel_id=1, source_target_pairs={{0,4},{1,5},{2,6},{3,7},{4,0},{5,1},{6,2},{7,3},{8,12},{9,13},{10,... | collective-permute-start | bytes 786440 | tf_op jit(solution)/shard_map/ppermute | solution.py:485
  56.2 13.1 %collective-permute-start.11 = (bf16[64,2048]{1,0:T(8,128)(2,1)S(1)}, bf16[64,2048]{1,0:T(8,128)(2,1)S(1)}, u32[]{:S(2)}, u32[]{:S(2)}) collective-permute-start(bf16[64,2048]{1,0:T(8,128)(2,1)S(1)} %get-tuple-element.50), channel_id=1, source_target_pairs={{0,6},{1,7},{2,4},{3,5},{4,2},{5,3},{6,0},{7,1},{8,14},{9,15},{10,... | collective-permute-start | bytes 786440 | tf_op jit(solution)/shard_map/ppermute | solution.py:485
  60.0 14.8 %collective-permute-start.6 = (bf16[64,2048]{1,0:T(8,128)(2,1)S(1)}, bf16[64,2048]{1,0:T(8,128)(2,1)S(1)}, u32[]{:S(2)}, u32[]{:S(2)}) collective-permute-start(bf16[64,2048]{1,0:T(8,128)(2,1)S(1)} %get-tuple-element.45), channel_id=1, source_target_pairs={{0,2},{1,3},{2,0},{3,1},{4,6},{5,7},{6,4},{7,5},{8,10},{9,11},{10,... | collective-permute-start | bytes 786440 | tf_op jit(solution)/shard_map/ppermute | solution.py:485
  63.3 13.3 %collective-permute-start.7 = (bf16[64,2048]{1,0:T(8,128)(2,1)S(1)}, bf16[64,2048]{1,0:T(8,128)(2,1)S(1)}, u32[]{:S(2)}, u32[]{:S(2)}) collective-permute-start(bf16[64,2048]{1,0:T(8,128)(2,1)S(1)} %get-tuple-element.46), channel_id=1, source_target_pairs={{0,4},{1,5},{2,6},{3,7},{4,0},{5,1},{6,2},{7,3},{8,12},{9,13},{10,... | collective-permute-start | bytes 786440 | tf_op jit(solution)/shard_map/ppermute | solution.py:485
  65.1 15.5 %collective-permute-start.8 = (bf16[64,2048]{1,0:T(8,128)(2,1)S(1)}, bf16[64,2048]{1,0:T(8,128)(2,1)S(1)}, u32[]{:S(2)}, u32[]{:S(2)}) collective-permute-start(bf16[64,2048]{1,0:T(8,128)(2,1)S(1)} %get-tuple-element.47), channel_id=1, source_target_pairs={{0,6},{1,7},{2,4},{3,5},{4,2},{5,3},{6,0},{7,1},{8,14},{9,15},{10,... | collective-permute-start | bytes 786440 | tf_op jit(solution)/shard_map/ppermute | solution.py:485
  69.3 22.4 %collective-permute-start.18 = (bf16[64,2048]{1,0:T(8,128)(2,1)S(1)}, bf16[64,2048]{1,0:T(8,128)(2,1)S(1)}, u32[]{:S(2)}, u32[]{:S(2)}) collective-permute-start(bf16[64,2048]{1,0:T(8,128)(2,1)S(1)} %get-tuple-element.58), channel_id=1, source_target_pairs={{0,2},{1,3},{2,0},{3,1},{4,6},{5,7},{6,4},{7,5},{8,10},{9,11},{10,... | collective-permute-start | bytes 786440 | tf_op jit(solution)/shard_map/ppermute | solution.py:485
  74.9 16.8 %collective-permute-start.19 = (bf16[64,2048]{1,0:T(8,128)(2,1)S(1)}, bf16[64,2048]{1,0:T(8,128)(2,1)S(1)}, u32[]{:S(2)}, u32[]{:S(2)}) collective-permute-start(bf16[64,2048]{1,0:T(8,128)(2,1)S(1)} %get-tuple-element.59), channel_id=1, source_target_pairs={{0,4},{1,5},{2,6},{3,7},{4,0},{5,1},{6,2},{7,3},{8,12},{9,13},{10,... | collective-permute-start | bytes 786440 | tf_op jit(solution)/shard_map/ppermute | solution.py:485
  76.6 15.1 %collective-permute-start.20 = (bf16[64,2048]{1,0:T(8,128)(2,1)S(1)}, bf16[64,2048]{1,0:T(8,128)(2,1)S(1)}, u32[]{:S(2)}, u32[]{:S(2)}) collective-permute-start(bf16[64,2048]{1,0:T(8,128)(2,1)S(1)} %get-tuple-element.60), channel_id=1, source_target_pairs={{0,6},{1,7},{2,4},{3,5},{4,2},{5,3},{6,0},{7,1},{8,14},{9,15},{10,... | collective-permute-start | bytes 786440 | tf_op jit(solution)/shard_map/ppermute | solution.py:485
  80.6 3.6 %copy-start.5 = (bf16[1024,256]{1,0:T(8,128)(2,1)S(1)}, bf16[1024,256]{1,0:T(8,128)(2,1)}, u32[]{:S(2)}) copy-start(bf16[1024,256]{1,0:T(8,128)(2,1)} %k_hbm.3) | copy-start | bytes 1572868
  80.6 3.6 %copy-start.6 = (bf16[1024,256]{1,0:T(8,128)(2,1)S(1)}, bf16[1024,256]{1,0:T(8,128)(2,1)}, u32[]{:S(2)}) copy-start(bf16[1024,256]{1,0:T(8,128)(2,1)} %v_hbm.3) | copy-start | bytes 1572868
  80.6 3.6 %copy-start.7 = (bf16[1024,512]{1,0:T(8,128)(2,1)S(1)}, bf16[1024,512]{1,0:T(8,128)(2,1)}, u32[]{:S(2)}) copy-start(bf16[1024,512]{1,0:T(8,128)(2,1)} %q_hbm.3) | copy-start | bytes 3145732
  80.6 3.6 %copy-start.12 = (f32[8]{0:T(128)S(1)}, f32[8]{0:T(128)}, u32[]{:S(2)}) copy-start(f32[8]{0:T(128)} %sink_ref.3) | copy-start | bytes 100
  95.2 8.4 %collective-permute-start.30 = (bf16[64,2048]{1,0:T(8,128)(2,1)S(1)}, bf16[64,2048]{1,0:T(8,128)(2,1)S(1)}, u32[]{:S(2)}, u32[]{:S(2)}) collective-permute-start(bf16[64,2048]{1,0:T(8,128)(2,1)S(1)} %get-tuple-element.71), channel_id=1, source_target_pairs={{0,2},{1,3},{2,0},{3,1},{4,6},{5,7},{6,4},{7,5},{8,10},{9,11},{10,... | collective-permute-start | bytes 786440 | tf_op jit(solution)/shard_map/ppermute | solution.py:485
  96.8 8.9 %collective-permute-start.31 = (bf16[64,2048]{1,0:T(8,128)(2,1)S(1)}, bf16[64,2048]{1,0:T(8,128)(2,1)S(1)}, u32[]{:S(2)}, u32[]{:S(2)}) collective-permute-start(bf16[64,2048]{1,0:T(8,128)(2,1)S(1)} %get-tuple-element.72), channel_id=1, source_target_pairs={{0,4},{1,5},{2,6},{3,7},{4,0},{5,1},{6,2},{7,3},{8,12},{9,13},{10,... | collective-permute-start | bytes 786440 | tf_op jit(solution)/shard_map/ppermute | solution.py:485
  98.6 9.9 %collective-permute-start.32 = (bf16[64,2048]{1,0:T(8,128)(2,1)S(1)}, bf16[64,2048]{1,0:T(8,128)(2,1)S(1)}, u32[]{:S(2)}, u32[]{:S(2)}) collective-permute-start(bf16[64,2048]{1,0:T(8,128)(2,1)S(1)} %get-tuple-element.73), channel_id=1, source_target_pairs={{0,6},{1,7},{2,4},{3,5},{4,2},{5,3},{6,0},{7,1},{8,14},{9,15},{10,... | collective-permute-start | bytes 786440 | tf_op jit(solution)/shard_map/ppermute | solution.py:485
  110.3 11.1 %collective-permute-start.33 = (bf16[128,2048]{1,0:T(8,128)(2,1)S(1)}, bf16[128,2048]{1,0:T(8,128)(2,1)S(1)}, u32[]{:S(2)}, u32[]{:S(2)}) collective-permute-start(bf16[128,2048]{1,0:T(8,128)(2,1)S(1)} %get-tuple-element.75), channel_id=1, source_target_pairs={{0,1},{1,0},{2,3},{3,2},{4,5},{5,4},{6,7},{7,6},{8,9},{9,8},{10,11... | collective-permute-start | bytes 1572872 | tf_op jit(solution)/shard_map/ppermute | solution.py:485
  110.4 9.3 %collective-permute-start.27 = (bf16[64,2048]{1,0:T(8,128)(2,1)S(1)}, bf16[64,2048]{1,0:T(8,128)(2,1)S(1)}, u32[]{:S(2)}, u32[]{:S(2)}) collective-permute-start(bf16[64,2048]{1,0:T(8,128)(2,1)S(1)} %get-tuple-element.68), channel_id=1, source_target_pairs={{0,2},{1,3},{2,0},{3,1},{4,6},{5,7},{6,4},{7,5},{8,10},{9,11},{10,... | collective-permute-start | bytes 786440 | tf_op jit(solution)/shard_map/ppermute | solution.py:485
  112.0 11.6 %collective-permute-start.28 = (bf16[64,2048]{1,0:T(8,128)(2,1)S(1)}, bf16[64,2048]{1,0:T(8,128)(2,1)S(1)}, u32[]{:S(2)}, u32[]{:S(2)}) collective-permute-start(bf16[64,2048]{1,0:T(8,128)(2,1)S(1)} %get-tuple-element.69), channel_id=1, source_target_pairs={{0,4},{1,5},{2,6},{3,7},{4,0},{5,1},{6,2},{7,3},{8,12},{9,13},{10,... | collective-permute-start | bytes 786440 | tf_op jit(solution)/shard_map/ppermute | solution.py:485
  113.8 13.0 %collective-permute-start.29 = (bf16[64,2048]{1,0:T(8,128)(2,1)S(1)}, bf16[64,2048]{1,0:T(8,128)(2,1)S(1)}, u32[]{:S(2)}, u32[]{:S(2)}) collective-permute-start(bf16[64,2048]{1,0:T(8,128)(2,1)S(1)} %get-tuple-element.70), channel_id=1, source_target_pairs={{0,6},{1,7},{2,4},{3,5},{4,2},{5,3},{6,0},{7,1},{8,14},{9,15},{10,... | collective-permute-start | bytes 786440 | tf_op jit(solution)/shard_map/ppermute | solution.py:485
  114.1 17.0 %collective-permute-start.24 = (bf16[64,2048]{1,0:T(8,128)(2,1)S(1)}, bf16[64,2048]{1,0:T(8,128)(2,1)S(1)}, u32[]{:S(2)}, u32[]{:S(2)}) collective-permute-start(bf16[64,2048]{1,0:T(8,128)(2,1)S(1)} %get-tuple-element.65), channel_id=1, source_target_pairs={{0,2},{1,3},{2,0},{3,1},{4,6},{5,7},{6,4},{7,5},{8,10},{9,11},{10,... | collective-permute-start | bytes 786440 | tf_op jit(solution)/shard_map/ppermute | solution.py:485
  119.8 14.9 %collective-permute-start.25 = (bf16[64,2048]{1,0:T(8,128)(2,1)S(1)}, bf16[64,2048]{1,0:T(8,128)(2,1)S(1)}, u32[]{:S(2)}, u32[]{:S(2)}) collective-permute-start(bf16[64,2048]{1,0:T(8,128)(2,1)S(1)} %get-tuple-element.66), channel_id=1, source_target_pairs={{0,4},{1,5},{2,6},{3,7},{4,0},{5,1},{6,2},{7,3},{8,12},{9,13},{10,... | collective-permute-start | bytes 786440 | tf_op jit(solution)/shard_map/ppermute | solution.py:485
  121.5 18.8 %collective-permute-start.26 = (bf16[64,2048]{1,0:T(8,128)(2,1)S(1)}, bf16[64,2048]{1,0:T(8,128)(2,1)S(1)}, u32[]{:S(2)}, u32[]{:S(2)}) collective-permute-start(bf16[64,2048]{1,0:T(8,128)(2,1)S(1)} %get-tuple-element.67), channel_id=1, source_target_pairs={{0,6},{1,7},{2,4},{3,5},{4,2},{5,3},{6,0},{7,1},{8,14},{9,15},{10,... | collective-permute-start | bytes 786440 | tf_op jit(solution)/shard_map/ppermute | solution.py:485
  123.6 20.4 %collective-permute-start.17 = (bf16[128,512]{1,0:T(8,128)(2,1)S(1)}, bf16[128,512]{1,0:T(8,128)(2,1)S(1)}, u32[]{:S(2)}, u32[]{:S(2)}) collective-permute-start(bf16[128,512]{1,0:T(8,128)(2,1)S(1)} %pad_maximum_fusion.2), channel_id=1, source_target_pairs={{4,0},{8,4},{12,8},{16,12},{20,16},{24,20},{28,24},{5,1},{9,5},{13... | collective-permute-start | bytes 393224 | tf_op jit(solution)/shard_map/ppermute | solution.py:508
  126.9 30.5 %collective-permute-start.21 = (bf16[64,2048]{1,0:T(8,128)(2,1)S(1)}, bf16[64,2048]{1,0:T(8,128)(2,1)}, u32[]{:S(2)}, u32[]{:S(2)}) collective-permute-start(bf16[64,2048]{1,0:T(8,128)(2,1)S(1)} %get-tuple-element.62), channel_id=1, source_target_pairs={{0,2},{1,3},{2,0},{3,1},{4,6},{5,7},{6,4},{7,5},{8,10},{9,11},{10,... | collective-permute-start | bytes 786440 | tf_op jit(solution)/shard_map/ppermute | solution.py:485
  131.1 26.5 %collective-permute-start.22 = (bf16[64,2048]{1,0:T(8,128)(2,1)S(1)}, bf16[64,2048]{1,0:T(8,128)(2,1)}, u32[]{:S(2)}, u32[]{:S(2)}) collective-permute-start(bf16[64,2048]{1,0:T(8,128)(2,1)S(1)} %get-tuple-element.63), channel_id=1, source_target_pairs={{0,4},{1,5},{2,6},{3,7},{4,0},{5,1},{6,2},{7,3},{8,12},{9,13},{10,... | collective-permute-start | bytes 786440 | tf_op jit(solution)/shard_map/ppermute | solution.py:485
  134.6 22.9 %collective-permute-start.23 = (bf16[64,2048]{1,0:T(8,128)(2,1)S(1)}, bf16[64,2048]{1,0:T(8,128)(2,1)}, u32[]{:S(2)}, u32[]{:S(2)}) collective-permute-start(bf16[64,2048]{1,0:T(8,128)(2,1)S(1)} %get-tuple-element.64), channel_id=1, source_target_pairs={{0,6},{1,7},{2,4},{3,5},{4,2},{5,3},{6,0},{7,1},{8,14},{9,15},{10,... | collective-permute-start | bytes 786440 | tf_op jit(solution)/shard_map/ppermute | solution.py:485
  143.0 1.0 copy-start.3
  144.0 20.4 %collective-permute-start.35 = (bf16[128,2048]{1,0:T(8,128)(2,1)}, bf16[128,2048]{1,0:T(8,128)(2,1)}, u32[]{:S(2)}, u32[]{:S(2)}) collective-permute-start(bf16[128,2048]{1,0:T(8,128)(2,1)} %get-tuple-element.80), channel_id=1, source_target_pairs={{0,1},{1,0},{2,3},{3,2},{4,5},{5,4},{6,7},{7,6},{8,9},{9,8},{10,11... | collective-permute-start | bytes 1572872 | tf_op jit(solution)/shard_map/ppermute | solution.py:485
  152.3 22.2 %all-to-all-start = ((bf16[4,256,512]{2,1,0:T(8,128)(2,1)}), bf16[4,256,512]{2,1,0:T(8,128)(2,1)S(1)}, u32[]{:S(2)}, u32[]{:S(2)}) async-start(bf16[4,256,512]{2,1,0:T(8,128)(2,1)} %bitcast.7), calls=%async_computation | async-start | bytes 2097152 | tf_op jit(solution)/shard_map/all_to_all | solution.py:549
  156.1 15.1 %collective-permute-start.38 = (bf16[128,2048]{1,0:T(8,128)(2,1)}, bf16[128,2048]{1,0:T(8,128)(2,1)S(1)}, u32[]{:S(2)}, u32[]{:S(2)}) collective-permute-start(bf16[128,2048]{1,0:T(8,128)(2,1)} %add_convert_fusion.3.refs_6_), channel_id=1, source_target_pairs={{0,8},{8,0},{1,9},{9,1},{2,10},{10,2},{3,11},{11,3},{4,12},{12,4},... | collective-permute-start | bytes 1572872 | tf_op jit(solution)/shard_map/ppermute | solution.py:452
  157.3 10.3 %collective-permute-start.37 = (bf16[128,2048]{1,0:T(8,128)(2,1)}, bf16[128,2048]{1,0:T(8,128)(2,1)S(1)}, u32[]{:S(2)}, u32[]{:S(2)}) collective-permute-start(bf16[128,2048]{1,0:T(8,128)(2,1)} %get-tuple-element.81), channel_id=1, source_target_pairs={{0,1},{1,0},{2,3},{3,2},{4,5},{5,4},{6,7},{7,6},{8,9},{9,8},{10,11... | collective-permute-start | bytes 1572872 | tf_op jit(solution)/shard_map/ppermute | solution.py:485
  157.6 1.2 copy-start.4
  158.8 1.1 copy-start.9
  159.8 1.1 copy-start.11
  164.1 15.6 %collective-permute-start.34 = (bf16[128,2048]{1,0:T(8,128)(2,1)}, bf16[128,2048]{1,0:T(8,128)(2,1)}, u32[]{:S(2)}, u32[]{:S(2)}) collective-permute-start(bf16[128,2048]{1,0:T(8,128)(2,1)} %get-tuple-element.79), channel_id=1, source_target_pairs={{0,1},{1,0},{2,3},{3,2},{4,5},{5,4},{6,7},{7,6},{8,9},{9,8},{10,11... | collective-permute-start | bytes 1572872 | tf_op jit(solution)/shard_map/ppermute | solution.py:485
  166.7 24.1 %collective-permute-start.36 = (bf16[128,2048]{1,0:T(8,128)(2,1)}, bf16[128,2048]{1,0:T(8,128)(2,1)}, u32[]{:S(2)}, u32[]{:S(2)}) collective-permute-start(bf16[128,2048]{1,0:T(8,128)(2,1)} %add_convert_fusion.2), channel_id=1, source_target_pairs={{0,8},{8,0},{1,9},{9,1},{2,10},{10,2},{3,11},{11,3},{4,12},{12,4},... | collective-permute-start | bytes 1572872 | tf_op jit(solution)/shard_map/ppermute | solution.py:452
  172.2 25.4 %collective-permute-start.39 = (bf16[128,2048]{1,0:T(8,128)(2,1)}, bf16[128,2048]{1,0:T(8,128)(2,1)S(1)}, u32[]{:S(2)}, u32[]{:S(2)}) collective-permute-start(bf16[128,2048]{1,0:T(8,128)(2,1)} %add_convert_fusion.1), channel_id=1, source_target_pairs={{0,16},{16,0},{1,17},{17,1},{2,18},{18,2},{3,19},{19,3},{4,20},{20... | collective-permute-start | bytes 1572872 | tf_op jit(solution)/shard_map/ppermute | solution.py:452
where the time goes:
time: 200 us
  waiting for transfers between devices  79.8 us (40%)
  Pallas kernels  52.8 us (26%)
  starting transfers between devices  52.8 us (26%)
  other arithmetic  8 us (4%)
  local copies, waits for them, and re-layouts  5.41 us (3%)
    ppermute x6, waiting for transfers between devices, relay(): return lax.ppermute(x, axis, [(0, 1), (1, 0)])  51.7 us
    ppermute x32, starting transfers between devices, mate(): return lax.ppermute(x, inner, [(i, i ^ step) for i in range(plane)])  33.7 us
    ppermute x32, waiting for transfers between devices, mate(): return lax.ppermute(x, inner, [(i, i ^ step) for i in range(plane)])  28.1 us
    pallas_call x2, Pallas kernels, attention(): pl.pallas_call(functools.partial(attention_kernel, first, count), out_sha...  14.8 us
    pallas_call x4, Pallas kernels, experts(): pl.pallas_call(functools.partial(expert_kernel, pieces), in_specs=[VMEM]...  14.1 us
    pallas_call x4, Pallas kernels, combine(): pl.pallas_call(functools.partial(combine_kernel, plan, len(back), count),...  10.5 us
    ppermute x6, starting transfers between devices, relay(): return lax.ppermute(x, axis, [(0, 1), (1, 0)])  10.1 us
    pallas_call x4, Pallas kernels, dispatch(): pl.pallas_call(functools.partial(dispatch_kernel, plan, pieces, len(paylo...  6.78 us
  transfers between devices with their start and end apart: 41, of which 16 were waited for; matrix products, arithmetic and copies ran while one was open for 3% of the time, Pallas kernels for 23%

commit v1 on v0

--- a/solution.py
+++ b/solution.py
@@ -19,6 +19,7 @@
 NORM_EPS = 1e-05
 LANES = 128
 MASKED = -1e30
+STRIDE = (2, 1, 2, 1)
 
 VMEM = pl.BlockSpec(memory_space=pltpu.VMEM)
 SMEM = pl.BlockSpec(memory_space=pltpu.SMEM)
@@ -87,16 +88,16 @@
         scratch_shapes=[pltpu.VMEM(o.shape, o.dtype) for o in operands]
         + [pltpu.SemaphoreType.DMA((4,))],
         compiler_params=params(6),
-        cost_estimate=cost(1e9),
+        cost_estimate=cost(2e10),
         name="norm",
     )(*operands)
 
 
 def slot_match(extra, where_ref, plan, weighted):
     tokens = extra.shape[0]
-    top, cap, plane, xor = plan
+    top, cap, plane, stride = plan
     lane = iota((1, LANES), 1)
-    piece = (2 * lane) ^ where_ref[1] if xor else lane
+    piece = (stride * lane) ^ where_ref[1] if stride else lane
     target = jnp.where(lane < plane, where_ref[0] + piece, -1).astype(F32)
     named = jnp.zeros((tokens, LANES), F32)
     high = jnp.zeros((tokens, LANES), F32)
@@ -150,7 +151,7 @@
         in_specs=[SMEM] + [VMEM] * len(payloads) + [ANY] * len(after),
         out_specs=[VMEM] * pieces,
         compiler_params=params(8),
-        cost_estimate=cost(2e9),
+        cost_estimate=cost(2e10),
         name="dispatch",
     )(where, *payloads, *after)
 
@@ -178,13 +179,35 @@
     count = len(payloads)
     return pl.pallas_call(
         functools.partial(combine_kernel, plan, len(back), count),
-        out_shape=[jax.ShapeDtypeStruct((tokens, width), d) for d in (F32, BF16)[:count]],
+        out_shape=[
+            jax.ShapeDtypeStruct((tokens, width), d)
+            for d in ((F32, BF16) if count > 1 else (BF16,))
+        ],
         in_specs=[SMEM] + [VMEM] * (count + len(back)) + [ANY] * len(after),
         out_specs=[VMEM] * count,
         compiler_params=params(10),
-        cost_estimate=cost(2e9),
+        cost_estimate=cost(2e10),
         name="combine",
     )(where, *payloads, *back, *after)
+
+
+def add_kernel(*refs):
+    total = refs[0][...].astype(F32)
+    for r in refs[1:-1]:
+        total = total + r[...].astype(F32)
+    refs[-1][...] = total.astype(BF16)
+
+
+def add(parts):
+    return pl.pallas_call(
+        add_kernel,
+        out_shape=jax.ShapeDtypeStruct(parts[0].shape, BF16),
+        in_specs=[VMEM] * len(parts),
+        out_specs=VMEM,
+        compiler_params=params(6),
+        cost_estimate=cost(2e10),
+        name="add",
+    )(*parts)
 
 
 def expert_kernel(pieces, gate_ref, up_ref, down_ref, *refs):
@@ -443,7 +466,7 @@
             pltpu.SemaphoreType.DMA((parts,)),
         ],
         compiler_params=params(18),
-        cost_estimate=cost(3e9),
+        cost_estimate=cost(2e10),
         name="mixer",
     )(rows, pltpu.with_memory_space_constraint(weight, pltpu.HBM))
 
@@ -475,8 +498,13 @@
     tok_local, top = routes.shape
     cap = 2 * tok_local * top // experts_all
     xor = plane <= 8 and plane & (plane - 1) == 0 and plane > 1
-    pieces = plane // 2 if xor else 1
-    plan = (top, cap, pieces if xor else plane, xor)
+
+    def layout(i):
+        if not xor:
+            return 1, (top, cap, plane, 0)
+        stride = STRIDE[i]
+        return plane // stride, (top, cap, plane // stride, stride)
+
     position = lax.axis_index(inner)
     base = lax.axis_index(("zh", "zl")) * plane
     where = jnp.stack([base, position]).astype(jnp.int32)
@@ -484,15 +512,16 @@
     def mate(x, step):
         return lax.ppermute(x, inner, [(i, i ^ step) for i in range(plane)])
 
-    def both(x):
-        return [x, mate(x, 1)] if xor else [x]
-
-    def exchange(parts):
+    def both(x, i):
+        return [x, mate(x, 1)] if layout(i)[1][3] == 2 else [x]
+
+    def exchange(parts, i):
         if not xor:
             block = parts[0].reshape(-1, plane, cap, parts[0].shape[1]).swapaxes(0, 1)
             turned = lax.all_to_all(block, inner, 0, 0, tiled=True)
             return [turned.swapaxes(0, 1).reshape(parts[0].shape)]
-        return [parts[0]] + [mate(parts[p], 2 * p) for p in range(1, pieces)]
+        stride = layout(i)[1][3]
+        return [parts[0]] + [mate(parts[p], stride * p) for p in range(1, len(parts))]
 
     own = make_payload(expert_input, norm_gain, routes, route_weights)
     near = relay(own, "zl")
@@ -510,18 +539,22 @@
     info = jnp.stack([first_global, jnp.int32(rows_here * ring_size)]).astype(jnp.int32)
     blocks = rows_here // WINDOW
 
+    half = (blocks - 2) // 2
+    ranges = ((1, half), (1 + half, blocks - 2 - half), (0, 1), (blocks - 1, 1))
+
     def attend(i, after):
+        first, count = ranges[i]
         return attention(
-            queries, key_heads, value_heads, right if i else left, left if not i else right,
-            sink_logits, table, info,
-            i * (blocks // 2), blocks // 2, after,
+            queries, key_heads, value_heads, left if i == 2 else table,
+            right if i == 3 else table, sink_logits, table, info, first, count, after,
         )
 
-    chunks = [both(x) for x in (own, near, far, far_near)]
+    chunks = [both(x, i) for i, x in enumerate((own, near, far, far_near))]
 
     def send(i, after):
+        pieces, plan = layout(i)
         parts = dispatch(plan, pieces, where, chunks[i], after)
-        return exchange(parts), parts[0]
+        return exchange(parts, i), parts[0]
 
     held = [
         pltpu.with_memory_space_constraint(w, pltpu.VMEM)
@@ -531,39 +564,38 @@
     def work(i, after):
         return experts(arrived[i], held, after)
 
-    arrived, made = {}, {}
-    arrived[0], sent = send(0, [])
-    arrived[1], sent = send(1, [sent])
-    arrived[2], sent = send(2, [sent])
+    arrived, made, rows = {}, {}, {}
+    arrived[0], sent = send(0, [table, info])
+    rows[0] = attend(0, sent)
+    arrived[1], sent = send(1, [rows[0]])
     made[0] = work(0, [sent])
-    arrived[3], sent = send(3, [made[0][0]])
+    arrived[2], sent = send(2, [made[0][0]])
     made[1] = work(1, [sent])
-    made[2] = work(2, [made[1][0]])
-    upper = attend(0, made[2][0])
-    made[3] = work(3, [upper])
-    lower = attend(1, made[3][0])
-    attended = jnp.concatenate([upper, lower], axis=0)
-
-    back = {i: exchange(made[i]) for i in (3, 2, 1, 0)}
+    arrived[3], sent = send(3, [made[1][0]])
+    made[2] = work(2, [sent])
+    rows[1] = attend(1, made[2][0])
+    made[3] = work(3, [rows[1]])
+    rows[3] = attend(3, made[3][0])
+    rows[2] = attend(2, rows[3])
+    attended = jnp.concatenate([rows[i] for i in (2, 0, 1, 3)], axis=0)
+
+    back = {i: exchange(made[i], i) for i in (3, 2, 1, 0)}
     tp_blocks = attended.reshape(tp_size, rows_here // tp_size, attended.shape[1])
     token_rows = lax.all_to_all(tp_blocks, "tp", split_axis=0, concat_axis=0, tiled=True)
+
+    def gather(i, after):
+        own_part, *other = combine(layout(i)[1], where, chunks[i], back[i], after)
+        return [own_part] + [mate(x, 1) for x in other], own_part
+
+    parts, done = gather(3, [])
+    last = add(parts) if len(parts) > 1 else parts[0].astype(BF16)
+    parts, done = gather(2, [last])
+    mid = add(parts + [relay(last, "zl")])
+    parts, done = gather(1, [done])
+    side = add(parts) if len(parts) > 1 else parts[0].astype(BF16)
+    parts, _ = gather(0, [done])
     mixer_out = mix(token_rows, mix_weight)
-
-    def gather(i, after):
-        own_part, *other = combine(plan, where, chunks[i], back[i], after)
-        return [own_part] + [mate(x, 1) for x in other], own_part
-
-    def total(parts):
-        return sum(x.astype(F32) for x in parts).astype(BF16)
-
-    parts, done = gather(3, [])
-    last = total(parts)
-    parts, done = gather(2, [last])
-    mid = total(parts + [relay(last, "zl")])
-    parts, done = gather(1, [done])
-    side = total(parts)
-    parts, _ = gather(0, [done])
-    summed = total(parts + [relay(side, "zl"), relay(mid, "zh")])
+    summed = add(parts + [relay(side, "zl"), relay(mid, "zh")])
     return (mixer_out, summed)
 
 

time: 200 us -> 198 us (0.990)
  other arithmetic: 8 us -> 1.56 us
  starting transfers between devices: 52.8 us -> 59.2 us
  waiting for transfers between devices: 79.8 us -> 74.1 us
  Pallas kernels: 52.8 us -> 55.8 us
    ppermute x32 -> x44, starting transfers between devices: 33.7 us -> 41.7 us  [mate(): return lax.ppermute(x, inner, [(i, i ^ step) for i in range(plane)])]
    ppermute x6, waiting for transfers between devices: 51.7 us -> 44.2 us  [relay(): return lax.ppermute(x, axis, [(0, 1), (1, 0)])]
    convert_element_type x4 -> x0, other arithmetic: 6.44 us -> none  [total(): return sum((x.astype(F32) for x in parts)).astype(BF16)]
    pallas_call x2 -> x4, Pallas kernels: 14.8 us -> 17.9 us  [attention(): pl.pallas_call(functools.partial(attention_kernel, first, count), out_sha...]
    pallas_call x4, Pallas kernels: 10.5 us -> 7.95 us  [combine(): pl.pallas_call(functools.partial(combine_kernel, plan, len(back), count),...]
    ppermute x6, starting transfers between devices: 10.1 us -> 7.89 us  [relay(): return lax.ppermute(x, axis, [(0, 1), (1, 0)])]
    pallas_call x0 -> x2, Pallas kernels: none -> 2.04 us  [add(): pl.pallas_call(add_kernel, out_shape=jax.ShapeDtypeStruct(parts[0].shape,...]
    ppermute x32 -> x44, waiting for transfers between devices: 28.1 us -> 29.8 us  [mate(): return lax.ppermute(x, inner, [(i, i ^ step) for i in range(plane)])]
  transfers between devices with their start and end apart: 41 -> 53, of which waited for: 16 -> 11; matrix products, arithmetic and copies ran while one was open for 3% -> 1% of each run, Pallas kernels for 23% -> 27%
where the time goes in v1:
time: 198 us
  waiting for transfers between devices  74.1 us (37%)
  starting transfers between devices  59.2 us (30%)
  Pallas kernels  55.8 us (28%)
  local copies, waits for them, and re-layouts  5.82 us (3%)
    ppermute x6, waiting for transfers between devices, relay(): return lax.ppermute(x, axis, [(0, 1), (1, 0)])  44.2 us
    ppermute x44, starting transfers between devices, mate(): return lax.ppermute(x, inner, [(i, i ^ step) for i in range(plane)])  41.7 us
    ppermute x44, waiting for transfers between devices, mate(): return lax.ppermute(x, inner, [(i, i ^ step) for i in range(plane)])  29.8 us
    pallas_call x4, Pallas kernels, attention(): pl.pallas_call(functools.partial(attention_kernel, first, count), out_sha...  17.9 us
    pallas_call x4, Pallas kernels, experts(): pl.pallas_call(functools.partial(expert_kernel, pieces), in_specs=[VMEM]...  15 us
    pallas_call x4, Pallas kernels, combine(): pl.pallas_call(functools.partial(combine_kernel, plan, len(back), count),...  7.95 us
    ppermute x6, starting transfers between devices, relay(): return lax.ppermute(x, axis, [(0, 1), (1, 0)])  7.89 us
    pallas_call x4, Pallas kernels, dispatch(): pl.pallas_call(functools.partial(dispatch_kernel, plan, pieces, len(paylo...  6.12 us
  transfers between devices with their start and end apart: 53, of which 11 were waited for; matrix products, arithmetic and copies ran while one was open for 1% of the time, Pallas kernels for 27%

profile of v1, /device:TPU:0, one launch (start us, length us, event | category | flops | bytes accessed | tf_op | source)
XLA Modules:
  0.0 197.8 jit_solution(3170531217011302247)
XLA Ops:
  0.7 1.5 norm.1.refs_0_
  2.7 2.6 %collective-permute-start.4 = (bf16[128,2176]{1,0:T(8,128)(2,1)S(1)}, bf16[128,2176]{1,0:T(8,128)(2,1)S(1)}, u32[]{:S(2)}, u32[]{:S(2)}) collective-permute-start(bf16[128,2176]{1,0:T(8,128)(2,1)S(1)} %norm.1.refs_0_), channel_id=1, source_target_pairs={{0,8},{8,0},{1,9},{9,1},{2,10},{10,2},{3,11},{11,3},{4,12},{12,4},... | collective-permute-start | bytes 1671176 | tf_op jit(solution)/shard_map/ppermute | solution.py:475
  5.4 2.6 %collective-permute-start.2 = (bf16[128,2176]{1,0:T(8,128)(2,1)S(1)}, bf16[128,2176]{1,0:T(8,128)(2,1)S(1)}, u32[]{:S(2)}, u32[]{:S(2)}) collective-permute-start(bf16[128,2176]{1,0:T(8,128)(2,1)S(1)} %norm.1.refs_0_), channel_id=1, source_target_pairs={{0,16},{16,0},{1,17},{17,1},{2,18},{18,2},{3,19},{19,3},{4,20},{20... | collective-permute-start | bytes 1671176 | tf_op jit(solution)/shard_map/ppermute | solution.py:475
  8.7 1.7 dispatch.4
  10.4 1.6 collective-permute-start.14
  12.0 1.5 collective-permute-start.15
  14.0 19.0 %collective-permute-done.2.refs_0_ = bf16[128,2176]{1,0:T(8,128)(2,1)S(1)} collective-permute-done((bf16[128,2176]{1,0:T(8,128)(2,1)S(1)}, bf16[128,2176]{1,0:T(8,128)(2,1)S(1)}, u32[]{:S(2)}, u32[]{:S(2)}) %collective-permute-start.2) | collective-permute-done | bytes 557088 | tf_op jit(solution)/shard_map/ppermute | solution.py:475
  33.0 6.1 %attention.4.refs_1_ = bf16[384,512]{1,0:T(8,128)(2,1)S(1)} custom-call(s32[2]{0:T(128)S(1)} %pad_add_fusion.refs_3_.info_ref, f32[8]{0:T(128)S(1)} %copy-done.6, f32[168,128]{1,0:T(8,128)S(1)} %pad_maximum_fusion.3.refs_2_.table_ref.left_ref.right_ref, bf16[1024,512]{1,0:T(8,128)(2,1)S(1)} %copy-done.3, bf16[1024,256]{1,0:T(8,128)(2,1)S(1)} %copy-done.4, ...), custom_call_target="tpu_custom_call" | custom-call | flops 1811939328 | bytes 4194304 | tf_op jit(solution)/shard_map/attention/pallas_call | solution.py:406
  39.1 1.4 dispatch.5
  40.5 1.7 collective-permute-start.10
  42.1 1.5 collective-permute-start.11
  44.4 0.8 collective-permute-start.6
  45.2 3.6 %experts.4 = (bf16[64,2048]{1,0:T(8,128)(2,1)S(1)}, bf16[64,2048]{1,0:T(8,128)(2,1)S(1)}, bf16[64,2048]{1,0:T(8,128)(2,1)S(1)}, bf16[64,2048]{1,0:T(8,128)(2,1)S(1)}) custom-call(bf16[1,2048,1024]{2,1,0:T(8,128)(2,1)S(1)} %copy-done, bf16[1,2048,1024]{2,1,0:T(8,128)(2,1)S(1)} %copy-done.1, bf16[1,1024,2048]{2,1,0:T(8,128)(2,1)S(1)} %copy-done.2, ...), custom_call_target="tpu_custom_call" | custom-call | flops 3221225472 | bytes 2097152 | tf_op jit(solution)/shard_map/experts/pallas_call | solution.py:242
  49.5 1.6 collective-permute-start.7
  51.1 1.1 collective-permute-done.12.refs_7_
  52.2 1.6 collective-permute-start.9
  54.3 1.7 dispatch.6
  56.5 0.8 collective-permute-start.25
  57.3 1.0 collective-permute-done.8.refs_3_
  58.3 1.4 collective-permute-start.26
  59.7 3.5 %experts.5 = (bf16[32,2048]{1,0:T(8,128)(2,1)S(1)}, bf16[32,2048]{1,0:T(8,128)(2,1)S(1)}, bf16[32,2048]{1,0:T(8,128)(2,1)S(1)}, bf16[32,2048]{1,0:T(8,128)(2,1)S...) custom-call(bf16[1,2048,1024]{2,1,0:T(8,128)(2,1)S(1)} %copy-done, ...), custom_call_target="tpu_custom_call" | custom-call | flops 3221225472 | bytes 2097152 | tf_op jit(solution)/shard_map/experts/pallas_call | solution.py:242
  63.3 5.3 %collective-permute-done.3.refs_0_ = bf16[128,2176]{1,0:T(8,128)(2,1)S(1)} collective-permute-done((bf16[128,2176]{1,0:T(8,128)(2,1)S(1)}, bf16[128,2176]{1,0:T(8,128)(2,1)S(1)}, u32[]{:S(2)}, u32[]{:S(2)}) %collective-permute-start.3) | collective-permute-done | bytes 557088 | tf_op jit(solution)/shard_map/ppermute | solution.py:475
  68.6 1.4 dispatch.7
  70.7 1.3 collective-permute-start.19
  72.5 1.2 collective-permute-start.21
  73.7 3.6 %experts.6 = (bf16[64,2048]{1,0:T(8,128)(2,1)S(1)}, bf16[64,2048]{1,0:T(8,128)(2,1)S(1)}, bf16[64,2048]{1,0:T(8,128)(2,1)S(1)}, bf16[64,2048]{1,0:T(8,128)(2,1)S(1)}) custom-call(bf16[1,2048,1024]{2,1,0:T(8,128)(2,1)S(1)} %copy-done, bf16[1,2048,1024]{2,1,0:T(8,128)(2,1)S(1)} %copy-done.1, bf16[1,1024,2048]{2,1,0:T(8,128)(2,1)S(1)} %copy-done.2, ...), custom_call_target="tpu_custom_call" | custom-call | flops 3221225472 | bytes 2097152 | tf_op jit(solution)/shard_map/experts/pallas_call | solution.py:242
  78.4 2.3 %collective-permute-start.23 = (bf16[32,2048]{1,0:T(8,128)(2,1)S(1)}, bf16[32,2048]{1,0:T(8,128)(2,1)S(1)}, u32[]{:S(2)}, u32[]{:S(2)}) collective-permute-start(bf16[32,2048]{1,0:T(8,128)(2,1)S(1)} %get-tuple-element.76), channel_id=1, source_target_pairs={{0,7},{1,6},{2,5},{3,4},{4,3},{5,2},{6,1},{7,0},{8,15},{9,14},{10,... | collective-permute-start | bytes 393224 | tf_op jit(solution)/shard_map/ppermute | solution.py:513
  80.7 6.1 %attention.5.refs_8_ = bf16[384,512]{1,0:T(8,128)(2,1)S(1)} custom-call(s32[2]{0:T(128)S(1)} %pad_add_fusion.refs_3_.info_ref, f32[8]{0:T(128)S(1)} %copy-done.6, f32[168,128]{1,0:T(8,128)S(1)} %pad_maximum_fusion.3.refs_2_.table_ref.left_ref.right_ref, bf16[1024,512]{1,0:T(8,128)(2,1)S(1)} %copy-done.3, bf16[1024,256]{1,0:T(8,128)(2,1)S(1)} %copy-done.4, ...), custom_call_target="tpu_custom_call" | custom-call | flops 1811939328 | bytes 4194304 | tf_op jit(solution)/shard_map/attention/pallas_call | solution.py:406
  86.9 1.3 collective-permute-start.1
  88.2 4.6 %collective-permute-start = (bf16[128,512]{1,0:T(8,128)(2,1)S(1)}, bf16[128,512]{1,0:T(8,128)(2,1)S(1)}, u32[]{:S(2)}, u32[]{:S(2)}) collective-permute-start(bf16[128,512]{1,0:T(8,128)(2,1)S(1)} %pad_maximum_fusion.1), channel_id=1, source_target_pairs={{0,4},{4,8},{8,12},{12,16},{16,20},{20,24},{24,28},{1,5},{5,9},{9,... | collective-permute-start | bytes 393224 | tf_op jit(solution)/shard_map/ppermute | solution.py:536
  92.8 4.3 %experts.7 = (bf16[32,2048]{1,0:T(8,128)(2,1)S(1)}, bf16[32,2048]{1,0:T(8,128)(2,1)S(1)}, bf16[32,2048]{1,0:T(8,128)(2,1)S(1)}, bf16[32,2048]{1,0:T(8,128)(2,1)}...) custom-call(bf16[1,2048,1024]{2,1,0:T(8,128)(2,1)S(1)} %copy-done, ...), custom_call_target="tpu_custom_call" | custom-call | flops 3221225472 | bytes 2097152 | tf_op jit(solution)/shard_map/experts/pallas_call | solution.py:242
  97.6 1.4 collective-permute-start.42
  99.0 1.4 collective-permute-start.43
  100.4 2.9 %attention.6.after_ref = bf16[128,512]{1,0:T(8,128)(2,1)S(1)} custom-call(s32[2]{0:T(128)S(1)} %pad_add_fusion.refs_3_.info_ref, f32[8]{0:T(128)S(1)} %copy-done.6, f32[168,128]{1,0:T(8,128)S(1)} %pad_maximum_fusion.3.refs_2_.table_ref.left_ref.right_ref, bf16[1024,512]{1,0:T(8,128)(2,1)S(1)} %copy-done.3, bf16[1024,256]{1,0:T(8,128)(2,1)S(1)} %copy-done.4, ...), custom_call_target="tpu_custom_call" | custom-call | flops 603979776 | bytes 4194304 | tf_op jit(solution)/shard_map/attention/pallas_call | solution.py:406
  103.6 2.9 %attention.7 = bf16[128,512]{1,0:T(8,128)(2,1)S(1)} custom-call(s32[2]{0:T(128)S(1)} %pad_add_fusion.refs_3_.info_ref, f32[8]{0:T(128)S(1)} %copy-done.6, f32[168,128]{1,0:T(8,128)S(1)} %pad_maximum_fusion.3.refs_2_.table_ref.left_ref.right_ref, bf16[1024,512]{1,0:T(8,128)(2,1)S(1)} %copy-done.3, bf16[1024,256]{1,0:T(8,128)(2,1)S(1)} %copy-done.4, ...), custom_call_target="tpu_custom_call" | custom-call | flops 603979776 | bytes 4194304 | tf_op jit(solution)/shard_map/attention/pallas_call | solution.py:406
  107.1 1.3 collective-permute-start.45
  109.0 1.5 collective-permute-start.46
  110.5 1.0 pad_maximum_fusion
  111.5 3.8 %all-to-all-start = ((bf16[4,256,512]{2,1,0:T(8,128)(2,1)}), bf16[4,256,512]{2,1,0:T(8,128)(2,1)S(1)}, u32[]{:S(2)}, u32[]{:S(2)}) async-start(bf16[4,256,512]{2,1,0:T(8,128)(2,1)} %bitcast.7), calls=%async_computation | async-start | bytes 2097152 | tf_op jit(solution)/shard_map/all_to_all | solution.py:584
  115.7 1.5 collective-permute-start.31
  117.7 1.4 collective-permute-start.38
  119.1 1.6 collective-permute-start.39
  120.7 1.1 copy-done.10
  121.7 0.9 copy-done.39
  122.6 0.9 copy-done.41
  123.6 2.1 %combine.4.refs_6_ = bf16[128,2048]{1,0:T(8,128)(2,1)S(1)} custom-call(s32[2]{0:T(128)S(1)} %pad_add_fusion.1.where_ref, bf16[128,2176]{1,0:T(8,128)(2,1)S(1)} %copy-done.10, bf16[32,2048]{1,0:T(8,128)(2,1)S(1)} %get-tuple-element.81.after_ref.refs_1_, bf16[32,2048]{1,0:T(8,128)(2,1)S(1)} %copy-done.39, bf16[32,2048]{1,0:T(8,128)(2,1)S(1)} %copy-done.41, ...), custom_call_target="tpu_custom_call" | custom-call | flops 20000000000 | bytes 1048576 | tf_op jit(solution)/shard_map/combine/pallas_call | solution.py:180
  125.7 12.7 %collective-permute-done.31.refs_3_ = bf16[32,2048]{1,0:T(8,128)(2,1)S(1)} collective-permute-done((bf16[32,2048]{1,0:T(8,128)(2,1)}, bf16[32,2048]{1,0:T(8,128)(2,1)S(1)}, u32[]{:S(2)}, u32[]{:S(2)}) %collective-permute-start.31) | collective-permute-done | bytes 131104 | tf_op jit(solution)/shard_map/ppermute | solution.py:513
  138.5 1.4 collective-permute-start.33
  139.9 4.2 %collective-permute-done.37.refs_3_ = bf16[64,2048]{1,0:T(8,128)(2,1)S(1)} collective-permute-done((bf16[64,2048]{1,0:T(8,128)(2,1)}, bf16[64,2048]{1,0:T(8,128)(2,1)S(1)}, u32[]{:S(2)}, u32[]{:S(2)}) %collective-permute-start.37) | collective-permute-done | bytes 262176 | tf_op jit(solution)/shard_map/ppermute | solution.py:513
  144.1 1.2 collective-permute-start.35
  145.3 2.6 %collective-permute-start.36 = (bf16[32,2048]{1,0:T(8,128)(2,1)S(1)}, bf16[32,2048]{1,0:T(8,128)(2,1)S(1)}, u32[]{:S(2)}, u32[]{:S(2)}) collective-permute-start(bf16[32,2048]{1,0:T(8,128)(2,1)S(1)} %copy-done.27), channel_id=1, source_target_pairs={{0,7},{1,6},{2,5},{3,4},{4,3},{5,2},{6,1},{7,0},{8,15},{9,14},{10,... | collective-permute-start | bytes 393224 | tf_op jit(solution)/shard_map/ppermute | solution.py:513
  148.0 1.9 combine.5
  150.8 2.6 %collective-permute-start.29 = (bf16[64,2048]{1,0:T(8,128)(2,1)S(1)}, bf16[64,2048]{1,0:T(8,128)(2,1)S(1)}, u32[]{:S(2)}, u32[]{:S(2)}) collective-permute-start(bf16[64,2048]{1,0:T(8,128)(2,1)S(1)} %copy-done.14), channel_id=1, source_target_pairs={{0,6},{1,7},{2,4},{3,5},{4,2},{5,3},{6,0},{7,1},{8,14},{9,15},{10,... | collective-permute-start | bytes 786440 | tf_op jit(solution)/shard_map/ppermute | solution.py:513
  153.9 1.4 collective-permute-done.36.refs_8_
  155.3 1.4 combine.6.refs_6_
  156.6 4.1 %collective-permute-done.27.refs_3_ = bf16[64,2048]{1,0:T(8,128)(2,1)S(1)} collective-permute-done((bf16[64,2048]{1,0:T(8,128)(2,1)S(1)}, bf16[64,2048]{1,0:T(8,128)(2,1)S(1)}, u32[]{:S(2)}, u32[]{:S(2)}) %collective-permute-start.27) | collective-permute-done | bytes 262176 | tf_op jit(solution)/shard_map/ppermute | solution.py:513
  161.2 5.2 %collective-permute-done.29.refs_5_ = bf16[64,2048]{1,0:T(8,128)(2,1)S(1)} collective-permute-done((bf16[64,2048]{1,0:T(8,128)(2,1)S(1)}, bf16[64,2048]{1,0:T(8,128)(2,1)S(1)}, u32[]{:S(2)}, u32[]{:S(2)}) %collective-permute-start.29) | collective-permute-done | bytes 262176 | tf_op jit(solution)/shard_map/ppermute | solution.py:513
  166.4 2.7 %combine.7 = (f32[128,2048]{1,0:T(8,128)S(1)}, bf16[128,2048]{1,0:T(8,128)(2,1)}) custom-call(s32[2]{0:T(128)S(1)} %pad_add_fusion.1.where_ref, bf16[128,2176]{1,0:T(8,128)(2,1)S(1)} %norm.1.refs_0_, bf16[128,2176]{1,0:T(8,128)(2,1)S(1)} %collective-permute-done.5.refs_1_, bf16[64,2048]{1,0:T(8,128)(2,1)S(1)} %copy-done.12, ...), custom_call_target="tpu_custom_call" | custom-call | flops 20000000000 | bytes 1048576 | tf_op jit(solution)/shard_map/combine/pallas_call | solution.py:180
  169.2 1.0 add.52
  170.2 1.3 collective-permute-start.51
  171.5 5.3 %mixer.1 = bf16[256,2048]{1,0:T(8,128)(2,1)} custom-call(bf16[4,256,512]{2,1,0:T(8,128)(2,1)S(1)} %all-to-all-done.rows_ref, bf16[2048,2048]{1,0:T(8,128)(2,1)} %weight_hbm.1), custom_call_target="tpu_custom_call" | custom-call | flops 20000000000 | bytes 1048576 | tf_op jit(solution)/shard_map/mixer/pallas_call | solution.py:458
  176.8 4.7 %collective-permute-done.48.refs_2_ = bf16[128,2048]{1,0:T(8,128)(2,1)S(1)} collective-permute-done((bf16[128,2048]{1,0:T(8,128)(2,1)S(1)}, bf16[128,2048]{1,0:T(8,128)(2,1)S(1)}, u32[]{:S(2)}, u32[]{:S(2)}) %collective-permute-start.48) | collective-permute-done | bytes 524320 | tf_op jit(solution)/shard_map/ppermute | solution.py:475
  181.5 15.2 %collective-permute-done.51.refs_3_ = bf16[128,2048]{1,0:T(8,128)(2,1)S(1)} collective-permute-done((bf16[128,2048]{1,0:T(8,128)(2,1)}, bf16[128,2048]{1,0:T(8,128)(2,1)S(1)}, u32[]{:S(2)}, u32[]{:S(2)}) %collective-permute-start.51) | collective-permute-done | bytes 524320 | tf_op jit(solution)/shard_map/ppermute | solution.py:475
  196.8 1.0 add.53
  (165 shorter events, 11.6 us)
Async XLA Ops:
  2.2 6.5 %collective-permute-start.5 = (bf16[128,2176]{1,0:T(8,128)(2,1)S(1)}, bf16[128,2176]{1,0:T(8,128)(2,1)S(1)}, u32[]{:S(2)}, u32[]{:S(2)}) collective-permute-start(bf16[128,2176]{1,0:T(8,128)(2,1)S(1)} %norm.1.refs_0_), channel_id=1, source_target_pairs={{0,1},{1,0},{2,3},{3,2},{4,5},{5,4},{6,7},{7,6},{8,9},{9,8},{10,11... | collective-permute-start | bytes 1671176 | tf_op jit(solution)/shard_map/ppermute | solution.py:513
  2.7 36.3 %collective-permute-start.4 = (bf16[128,2176]{1,0:T(8,128)(2,1)S(1)}, bf16[128,2176]{1,0:T(8,128)(2,1)S(1)}, u32[]{:S(2)}, u32[]{:S(2)}) collective-permute-start(bf16[128,2176]{1,0:T(8,128)(2,1)S(1)} %norm.1.refs_0_), channel_id=1, source_target_pairs={{0,8},{8,0},{1,9},{9,1},{2,10},{10,2},{3,11},{11,3},{4,12},{12,4},... | collective-permute-start | bytes 1671176 | tf_op jit(solution)/shard_map/ppermute | solution.py:475
  5.4 27.6 %collective-permute-start.2 = (bf16[128,2176]{1,0:T(8,128)(2,1)S(1)}, bf16[128,2176]{1,0:T(8,128)(2,1)S(1)}, u32[]{:S(2)}, u32[]{:S(2)}) collective-permute-start(bf16[128,2176]{1,0:T(8,128)(2,1)S(1)} %norm.1.refs_0_), channel_id=1, source_target_pairs={{0,16},{16,0},{1,17},{17,1},{2,18},{18,2},{3,19},{19,3},{4,20},{20... | collective-permute-start | bytes 1671176 | tf_op jit(solution)/shard_map/ppermute | solution.py:475
  8.7 24.3 %copy-start.3 = (bf16[1024,512]{1,0:T(8,128)(2,1)S(1)}, bf16[1024,512]{1,0:T(8,128)(2,1)}, u32[]{:S(2)}) copy-start(bf16[1024,512]{1,0:T(8,128)(2,1)} %q_hbm.7) | copy-start | bytes 3145732
  8.7 24.3 %copy-start.6 = (f32[8]{0:T(128)S(1)}, f32[8]{0:T(128)}, u32[]{:S(2)}) copy-start(f32[8]{0:T(128)} %sink_ref.7) | copy-start | bytes 100
  10.4 31.7 %collective-permute-start.14 = (bf16[64,2048]{1,0:T(8,128)(2,1)S(1)}, bf16[64,2048]{1,0:T(8,128)(2,1)S(1)}, u32[]{:S(2)}, u32[]{:S(2)}) collective-permute-start(bf16[64,2048]{1,0:T(8,128)(2,1)S(1)} %get-tuple-element.63), channel_id=1, source_target_pairs={{0,2},{1,3},{2,0},{3,1},{4,6},{5,7},{6,4},{7,5},{8,10},{9,11},{10,... | collective-permute-start | bytes 786440 | tf_op jit(solution)/shard_map/ppermute | solution.py:513
  12.0 31.6 %collective-permute-start.15 = (bf16[64,2048]{1,0:T(8,128)(2,1)S(1)}, bf16[64,2048]{1,0:T(8,128)(2,1)S(1)}, u32[]{:S(2)}, u32[]{:S(2)}) collective-permute-start(bf16[64,2048]{1,0:T(8,128)(2,1)S(1)} %get-tuple-element.64), channel_id=1, source_target_pairs={{0,4},{1,5},{2,6},{3,7},{4,0},{5,1},{6,2},{7,3},{8,12},{9,13},{10,... | collective-permute-start | bytes 786440 | tf_op jit(solution)/shard_map/ppermute | solution.py:513
  13.5 30.9 %collective-permute-start.16 = (bf16[64,2048]{1,0:T(8,128)(2,1)S(1)}, bf16[64,2048]{1,0:T(8,128)(2,1)S(1)}, u32[]{:S(2)}, u32[]{:S(2)}) collective-permute-start(bf16[64,2048]{1,0:T(8,128)(2,1)S(1)} %get-tuple-element.65), channel_id=1, source_target_pairs={{0,6},{1,7},{2,4},{3,5},{4,2},{5,3},{6,0},{7,1},{8,14},{9,15},{10,... | collective-permute-start | bytes 786440 | tf_op jit(solution)/shard_map/ppermute | solution.py:513
  32.9 20.9 %collective-permute-start.13 = (bf16[128,2176]{1,0:T(8,128)(2,1)S(1)}, bf16[128,2176]{1,0:T(8,128)(2,1)S(1)}, u32[]{:S(2)}, u32[]{:S(2)}) collective-permute-start(bf16[128,2176]{1,0:T(8,128)(2,1)S(1)} %collective-permute-done.2.refs_0_), channel_id=1, source_target_pairs={{0,1},{1,0},{2,3},{3,2},{4,5},{5,4},{6,7},{7,6},{8,9},{9,8},{10,11... | collective-permute-start | bytes 1671176 | tf_op jit(solution)/shard_map/ppermute | solution.py:513
  40.5 9.0 %collective-permute-start.10 = (bf16[32,2048]{1,0:T(8,128)(2,1)S(1)}, bf16[32,2048]{1,0:T(8,128)(2,1)S(1)}, u32[]{:S(2)}, u32[]{:S(2)}) collective-permute-start(bf16[32,2048]{1,0:T(8,128)(2,1)S(1)} %get-tuple-element.60), channel_id=1, source_target_pairs={{0,5},{1,4},{2,7},{3,6},{4,1},{5,0},{6,3},{7,2},{8,13},{9,12},{10,... | collective-permute-start | bytes 393224 | tf_op jit(solution)/shard_map/ppermute | solution.py:513
  42.1 8.9 %collective-permute-start.11 = (bf16[32,2048]{1,0:T(8,128)(2,1)S(1)}, bf16[32,2048]{1,0:T(8,128)(2,1)S(1)}, u32[]{:S(2)}, u32[]{:S(2)}) collective-permute-start(bf16[32,2048]{1,0:T(8,128)(2,1)S(1)} %get-tuple-element.61), channel_id=1, source_target_pairs={{0,6},{1,7},{2,4},{3,5},{4,2},{5,3},{6,0},{7,1},{8,14},{9,15},{10,... | collective-permute-start | bytes 393224 | tf_op jit(solution)/shard_map/ppermute | solution.py:513
  43.6 8.6 %collective-permute-start.12 = (bf16[32,2048]{1,0:T(8,128)(2,1)S(1)}, bf16[32,2048]{1,0:T(8,128)(2,1)S(1)}, u32[]{:S(2)}, u32[]{:S(2)}) collective-permute-start(bf16[32,2048]{1,0:T(8,128)(2,1)S(1)} %get-tuple-element.62), channel_id=1, source_target_pairs={{0,7},{1,6},{2,5},{3,4},{4,3},{5,2},{6,1},{7,0},{8,15},{9,14},{10,... | collective-permute-start | bytes 393224 | tf_op jit(solution)/shard_map/ppermute | solution.py:513
  44.4 11.6 %collective-permute-start.6 = (bf16[32,2048]{1,0:T(8,128)(2,1)S(1)}, bf16[32,2048]{1,0:T(8,128)(2,1)S(1)}, u32[]{:S(2)}, u32[]{:S(2)}) collective-permute-start(bf16[32,2048]{1,0:T(8,128)(2,1)S(1)} %get-tuple-element.56), channel_id=1, source_target_pairs={{0,1},{1,0},{2,3},{3,2},{4,5},{5,4},{6,7},{7,6},{8,9},{9,8},{10,11... | collective-permute-start | bytes 393224 | tf_op jit(solution)/shard_map/ppermute | solution.py:513
  49.5 7.0 %collective-permute-start.7 = (bf16[32,2048]{1,0:T(8,128)(2,1)S(1)}, bf16[32,2048]{1,0:T(8,128)(2,1)S(1)}, u32[]{:S(2)}, u32[]{:S(2)}) collective-permute-start(bf16[32,2048]{1,0:T(8,128)(2,1)S(1)} %get-tuple-element.57), channel_id=1, source_target_pairs={{0,2},{1,3},{2,0},{3,1},{4,6},{5,7},{6,4},{7,5},{8,10},{9,11},{10,... | collective-permute-start | bytes 393224 | tf_op jit(solution)/shard_map/ppermute | solution.py:513
  51.1 7.2 %collective-permute-start.8 = (bf16[32,2048]{1,0:T(8,128)(2,1)S(1)}, bf16[32,2048]{1,0:T(8,128)(2,1)S(1)}, u32[]{:S(2)}, u32[]{:S(2)}) collective-permute-start(bf16[32,2048]{1,0:T(8,128)(2,1)S(1)} %get-tuple-element.58), channel_id=1, source_target_pairs={{0,3},{1,2},{2,1},{3,0},{4,7},{5,6},{6,5},{7,4},{8,11},{9,10},{10,... | collective-permute-start | bytes 393224 | tf_op jit(solution)/shard_map/ppermute | solution.py:513
  52.2 7.5 %collective-permute-start.9 = (bf16[32,2048]{1,0:T(8,128)(2,1)S(1)}, bf16[32,2048]{1,0:T(8,128)(2,1)S(1)}, u32[]{:S(2)}, u32[]{:S(2)}) collective-permute-start(bf16[32,2048]{1,0:T(8,128)(2,1)S(1)} %get-tuple-element.59), channel_id=1, source_target_pairs={{0,4},{1,5},{2,6},{3,7},{4,0},{5,1},{6,2},{7,3},{8,12},{9,13},{10,... | collective-permute-start | bytes 393224 | tf_op jit(solution)/shard_map/ppermute | solution.py:513
  53.8 14.8 %collective-permute-start.3 = (bf16[128,2176]{1,0:T(8,128)(2,1)S(1)}, bf16[128,2176]{1,0:T(8,128)(2,1)S(1)}, u32[]{:S(2)}, u32[]{:S(2)}) collective-permute-start(bf16[128,2176]{1,0:T(8,128)(2,1)S(1)} %collective-permute-done.2.refs_0_), channel_id=1, source_target_pairs={{0,8},{8,0},{1,9},{9,1},{2,10},{10,2},{3,11},{11,3},{4,12},{12,4},... | collective-permute-start | bytes 1671176 | tf_op jit(solution)/shard_map/ppermute | solution.py:475
  56.0 14.7 %collective-permute-start.24 = (bf16[64,2048]{1,0:T(8,128)(2,1)S(1)}, bf16[64,2048]{1,0:T(8,128)(2,1)S(1)}, u32[]{:S(2)}, u32[]{:S(2)}) collective-permute-start(bf16[64,2048]{1,0:T(8,128)(2,1)S(1)} %get-tuple-element.77), channel_id=1, source_target_pairs={{0,2},{1,3},{2,0},{3,1},{4,6},{5,7},{6,4},{7,5},{8,10},{9,11},{10,... | collective-permute-start | bytes 786440 | tf_op jit(solution)/shard_map/ppermute | solution.py:513
  56.5 15.5 %collective-permute-start.25 = (bf16[64,2048]{1,0:T(8,128)(2,1)S(1)}, bf16[64,2048]{1,0:T(8,128)(2,1)S(1)}, u32[]{:S(2)}, u32[]{:S(2)}) collective-permute-start(bf16[64,2048]{1,0:T(8,128)(2,1)S(1)} %get-tuple-element.78), channel_id=1, source_target_pairs={{0,4},{1,5},{2,6},{3,7},{4,0},{5,1},{6,2},{7,3},{8,12},{9,13},{10,... | collective-permute-start | bytes 786440 | tf_op jit(solution)/shard_map/ppermute | solution.py:513
  58.3 14.2 %collective-permute-start.26 = (bf16[64,2048]{1,0:T(8,128)(2,1)S(1)}, bf16[64,2048]{1,0:T(8,128)(2,1)S(1)}, u32[]{:S(2)}, u32[]{:S(2)}) collective-permute-start(bf16[64,2048]{1,0:T(8,128)(2,1)S(1)} %get-tuple-element.79), channel_id=1, source_target_pairs={{0,6},{1,7},{2,4},{3,5},{4,2},{5,3},{6,0},{7,1},{8,14},{9,15},{10,... | collective-permute-start | bytes 786440 | tf_op jit(solution)/shard_map/ppermute | solution.py:513
  70.0 7.9 %collective-permute-start.17 = (bf16[32,2048]{1,0:T(8,128)(2,1)S(1)}, bf16[32,2048]{1,0:T(8,128)(2,1)S(1)}, u32[]{:S(2)}, u32[]{:S(2)}) collective-permute-start(bf16[32,2048]{1,0:T(8,128)(2,1)S(1)} %get-tuple-element.70), channel_id=1, source_target_pairs={{0,1},{1,0},{2,3},{3,2},{4,5},{5,4},{6,7},{7,6},{8,9},{9,8},{10,11... | collective-permute-start | bytes 393224 | tf_op jit(solution)/shard_map/ppermute | solution.py:513
  70.1 8.3 %collective-permute-start.18 = (bf16[32,2048]{1,0:T(8,128)(2,1)S(1)}, bf16[32,2048]{1,0:T(8,128)(2,1)S(1)}, u32[]{:S(2)}, u32[]{:S(2)}) collective-permute-start(bf16[32,2048]{1,0:T(8,128)(2,1)S(1)} %get-tuple-element.71), channel_id=1, source_target_pairs={{0,2},{1,3},{2,0},{3,1},{4,6},{5,7},{6,4},{7,5},{8,10},{9,11},{10,... | collective-permute-start | bytes 393224 | tf_op jit(solution)/shard_map/ppermute | solution.py:513
  70.7 16.2 %collective-permute-start.19 = (bf16[32,2048]{1,0:T(8,128)(2,1)S(1)}, bf16[32,2048]{1,0:T(8,128)(2,1)S(1)}, u32[]{:S(2)}, u32[]{:S(2)}) collective-permute-start(bf16[32,2048]{1,0:T(8,128)(2,1)S(1)} %get-tuple-element.72), channel_id=1, source_target_pairs={{0,3},{1,2},{2,1},{3,0},{4,7},{5,6},{6,5},{7,4},{8,11},{9,10},{10,... | collective-permute-start | bytes 393224 | tf_op jit(solution)/shard_map/ppermute | solution.py:513
  72.0 16.2 %collective-permute-start.20 = (bf16[32,2048]{1,0:T(8,128)(2,1)S(1)}, bf16[32,2048]{1,0:T(8,128)(2,1)S(1)}, u32[]{:S(2)}, u32[]{:S(2)}) collective-permute-start(bf16[32,2048]{1,0:T(8,128)(2,1)S(1)} %get-tuple-element.73), channel_id=1, source_target_pairs={{0,4},{1,5},{2,6},{3,7},{4,0},{5,1},{6,2},{7,3},{8,12},{9,13},{10,... | collective-permute-start | bytes 393224 | tf_op jit(solution)/shard_map/ppermute | solution.py:513
  72.5 20.3 %collective-permute-start.21 = (bf16[32,2048]{1,0:T(8,128)(2,1)S(1)}, bf16[32,2048]{1,0:T(8,128)(2,1)S(1)}, u32[]{:S(2)}, u32[]{:S(2)}) collective-permute-start(bf16[32,2048]{1,0:T(8,128)(2,1)S(1)} %get-tuple-element.74), channel_id=1, source_target_pairs={{0,5},{1,4},{2,7},{3,6},{4,1},{5,0},{6,3},{7,2},{8,13},{9,12},{10,... | collective-permute-start | bytes 393224 | tf_op jit(solution)/shard_map/ppermute | solution.py:513
  78.0 14.8 %collective-permute-start.22 = (bf16[32,2048]{1,0:T(8,128)(2,1)S(1)}, bf16[32,2048]{1,0:T(8,128)(2,1)S(1)}, u32[]{:S(2)}, u32[]{:S(2)}) collective-permute-start(bf16[32,2048]{1,0:T(8,128)(2,1)S(1)} %get-tuple-element.75), channel_id=1, source_target_pairs={{0,6},{1,7},{2,4},{3,5},{4,2},{5,3},{6,0},{7,1},{8,14},{9,15},{10,... | collective-permute-start | bytes 393224 | tf_op jit(solution)/shard_map/ppermute | solution.py:513
  78.4 14.4 %collective-permute-start.23 = (bf16[32,2048]{1,0:T(8,128)(2,1)S(1)}, bf16[32,2048]{1,0:T(8,128)(2,1)S(1)}, u32[]{:S(2)}, u32[]{:S(2)}) collective-permute-start(bf16[32,2048]{1,0:T(8,128)(2,1)S(1)} %get-tuple-element.76), channel_id=1, source_target_pairs={{0,7},{1,6},{2,5},{3,4},{4,3},{5,2},{6,1},{7,0},{8,15},{9,14},{10,... | collective-permute-start | bytes 393224 | tf_op jit(solution)/shard_map/ppermute | solution.py:513
  86.9 12.1 %collective-permute-start.1 = (bf16[128,512]{1,0:T(8,128)(2,1)S(1)}, bf16[128,512]{1,0:T(8,128)(2,1)S(1)}, u32[]{:S(2)}, u32[]{:S(2)}) collective-permute-start(bf16[128,512]{1,0:T(8,128)(2,1)S(1)} %pad_maximum_fusion.2), channel_id=1, source_target_pairs={{4,0},{8,4},{12,8},{16,12},{20,16},{24,20},{28,24},{5,1},{9,5},{13... | collective-permute-start | bytes 393224 | tf_op jit(solution)/shard_map/ppermute | solution.py:537
  88.2 15.1 %collective-permute-start = (bf16[128,512]{1,0:T(8,128)(2,1)S(1)}, bf16[128,512]{1,0:T(8,128)(2,1)S(1)}, u32[]{:S(2)}, u32[]{:S(2)}) collective-permute-start(bf16[128,512]{1,0:T(8,128)(2,1)S(1)} %pad_maximum_fusion.1), channel_id=1, source_target_pairs={{0,4},{4,8},{8,12},{12,16},{16,20},{20,24},{24,28},{1,5},{5,9},{9,... | collective-permute-start | bytes 393224 | tf_op jit(solution)/shard_map/ppermute | solution.py:536
  97.1 9.3 %collective-permute-start.40 = (bf16[32,2048]{1,0:T(8,128)(2,1)S(1)}, bf16[32,2048]{1,0:T(8,128)(2,1)S(1)}, u32[]{:S(2)}, u32[]{:S(2)}) collective-permute-start(bf16[32,2048]{1,0:T(8,128)(2,1)S(1)} %get-tuple-element.95), channel_id=1, source_target_pairs={{0,1},{1,0},{2,3},{3,2},{4,5},{5,4},{6,7},{7,6},{8,9},{9,8},{10,11... | collective-permute-start | bytes 393224 | tf_op jit(solution)/shard_map/ppermute | solution.py:513
  97.1 11.2 %collective-permute-start.41 = (bf16[32,2048]{1,0:T(8,128)(2,1)S(1)}, bf16[32,2048]{1,0:T(8,128)(2,1)S(1)}, u32[]{:S(2)}, u32[]{:S(2)}) collective-permute-start(bf16[32,2048]{1,0:T(8,128)(2,1)S(1)} %get-tuple-element.96), channel_id=1, source_target_pairs={{0,2},{1,3},{2,0},{3,1},{4,6},{5,7},{6,4},{7,5},{8,10},{9,11},{10,... | collective-permute-start | bytes 393224 | tf_op jit(solution)/shard_map/ppermute | solution.py:513
  97.6 17.7 %collective-permute-start.42 = (bf16[32,2048]{1,0:T(8,128)(2,1)}, bf16[32,2048]{1,0:T(8,128)(2,1)}, u32[]{:S(2)}, u32[]{:S(2)}) collective-permute-start(bf16[32,2048]{1,0:T(8,128)(2,1)} %get-tuple-element.97), channel_id=1, source_target_pairs={{0,3},{1,2},{2,1},{3,0},{4,7},{5,6},{6,5},{7,4},{8,11},{9,10},{10,... | collective-permute-start | bytes 393224 | tf_op jit(solution)/shard_map/ppermute | solution.py:513
  99.0 16.7 %collective-permute-start.43 = (bf16[32,2048]{1,0:T(8,128)(2,1)}, bf16[32,2048]{1,0:T(8,128)(2,1)}, u32[]{:S(2)}, u32[]{:S(2)}) collective-permute-start(bf16[32,2048]{1,0:T(8,128)(2,1)} %get-tuple-element.98), channel_id=1, source_target_pairs={{0,4},{1,5},{2,6},{3,7},{4,0},{5,1},{6,2},{7,3},{8,12},{9,13},{10,... | collective-permute-start | bytes 393224 | tf_op jit(solution)/shard_map/ppermute | solution.py:513
  103.3 13.9 %collective-permute-start.44 = (bf16[32,2048]{1,0:T(8,128)(2,1)}, bf16[32,2048]{1,0:T(8,128)(2,1)}, u32[]{:S(2)}, u32[]{:S(2)}) collective-permute-start(bf16[32,2048]{1,0:T(8,128)(2,1)} %get-tuple-element.99), channel_id=1, source_target_pairs={{0,5},{1,4},{2,7},{3,6},{4,1},{5,0},{6,3},{7,2},{8,13},{9,12},{10,... | collective-permute-start | bytes 393224 | tf_op jit(solution)/shard_map/ppermute | solution.py:513
  107.1 10.6 %collective-permute-start.45 = (bf16[32,2048]{1,0:T(8,128)(2,1)}, bf16[32,2048]{1,0:T(8,128)(2,1)}, u32[]{:S(2)}, u32[]{:S(2)}) collective-permute-start(bf16[32,2048]{1,0:T(8,128)(2,1)} %get-tuple-element.100), channel_id=1, source_target_pairs={{0,6},{1,7},{2,4},{3,5},{4,2},{5,3},{6,0},{7,1},{8,14},{9,15},{10,... | collective-permute-start | bytes 393224 | tf_op jit(solution)/shard_map/ppermute | solution.py:513
  109.0 10.1 %collective-permute-start.46 = (bf16[32,2048]{1,0:T(8,128)(2,1)}, bf16[32,2048]{1,0:T(8,128)(2,1)}, u32[]{:S(2)}, u32[]{:S(2)}) collective-permute-start(bf16[32,2048]{1,0:T(8,128)(2,1)} %get-tuple-element.101), channel_id=1, source_target_pairs={{0,7},{1,6},{2,5},{3,4},{4,3},{5,2},{6,1},{7,0},{8,15},{9,14},{10,... | collective-permute-start | bytes 393224 | tf_op jit(solution)/shard_map/ppermute | solution.py:513
  111.5 60.0 %all-to-all-start = ((bf16[4,256,512]{2,1,0:T(8,128)(2,1)}), bf16[4,256,512]{2,1,0:T(8,128)(2,1)S(1)}, u32[]{:S(2)}, u32[]{:S(2)}) async-start(bf16[4,256,512]{2,1,0:T(8,128)(2,1)} %bitcast.7), calls=%async_computation | async-start | bytes 2097152 | tf_op jit(solution)/shard_map/all_to_all | solution.py:584
  115.3 10.3 %collective-permute-start.30 = (bf16[32,2048]{1,0:T(8,128)(2,1)}, bf16[32,2048]{1,0:T(8,128)(2,1)S(1)}, u32[]{:S(2)}, u32[]{:S(2)}) collective-permute-start(bf16[32,2048]{1,0:T(8,128)(2,1)} %copy-done.37), channel_id=1, source_target_pairs={{0,1},{1,0},{2,3},{3,2},{4,5},{5,4},{6,7},{7,6},{8,9},{9,8},{10,11... | collective-permute-start | bytes 393224 | tf_op jit(solution)/shard_map/ppermute | solution.py:513
  115.7 22.8 %collective-permute-start.31 = (bf16[32,2048]{1,0:T(8,128)(2,1)}, bf16[32,2048]{1,0:T(8,128)(2,1)S(1)}, u32[]{:S(2)}, u32[]{:S(2)}) collective-permute-start(bf16[32,2048]{1,0:T(8,128)(2,1)} %copy-done.36), channel_id=1, source_target_pairs={{0,2},{1,3},{2,0},{3,1},{4,6},{5,7},{6,4},{7,5},{8,10},{9,11},{10,... | collective-permute-start | bytes 393224 | tf_op jit(solution)/shard_map/ppermute | solution.py:513
  117.2 26.9 %collective-permute-start.37 = (bf16[64,2048]{1,0:T(8,128)(2,1)}, bf16[64,2048]{1,0:T(8,128)(2,1)S(1)}, u32[]{:S(2)}, u32[]{:S(2)}) collective-permute-start(bf16[64,2048]{1,0:T(8,128)(2,1)} %copy-done.23), channel_id=1, source_target_pairs={{0,2},{1,3},{2,0},{3,1},{4,6},{5,7},{6,4},{7,5},{8,10},{9,11},{10,... | collective-permute-start | bytes 786440 | tf_op jit(solution)/shard_map/ppermute | solution.py:513
  117.7 26.4 %collective-permute-start.38 = (bf16[64,2048]{1,0:T(8,128)(2,1)}, bf16[64,2048]{1,0:T(8,128)(2,1)S(1)}, u32[]{:S(2)}, u32[]{:S(2)}) collective-permute-start(bf16[64,2048]{1,0:T(8,128)(2,1)} %copy-done.22), channel_id=1, source_target_pairs={{0,4},{1,5},{2,6},{3,7},{4,0},{5,1},{6,2},{7,3},{8,12},{9,13},{10,... | collective-permute-start | bytes 786440 | tf_op jit(solution)/shard_map/ppermute | solution.py:513
  119.1 28.8 %copy-start.8 = (bf16[128,2176]{1,0:T(8,128)(2,1)S(1)}, bf16[128,2176]{1,0:T(8,128)(2,1)}, u32[]{:S(2)}) copy-start(bf16[128,2176]{1,0:T(8,128)(2,1)} %copy-done.7) | copy-start | bytes 1671172
  119.1 26.2 %collective-permute-start.39 = (bf16[64,2048]{1,0:T(8,128)(2,1)}, bf16[64,2048]{1,0:T(8,128)(2,1)S(1)}, u32[]{:S(2)}, u32[]{:S(2)}) collective-permute-start(bf16[64,2048]{1,0:T(8,128)(2,1)} %copy-done.21), channel_id=1, source_target_pairs={{0,6},{1,7},{2,4},{3,5},{4,2},{5,3},{6,0},{7,1},{8,14},{9,15},{10,... | collective-permute-start | bytes 786440 | tf_op jit(solution)/shard_map/ppermute | solution.py:513
  123.5 14.9 %copy-start.33 = (bf16[32,2048]{1,0:T(8,128)(2,1)S(1)}, bf16[32,2048]{1,0:T(8,128)(2,1)}, u32[]{:S(2)}) copy-start(bf16[32,2048]{1,0:T(8,128)(2,1)} %copy-done.32) | copy-start | bytes 393220
  123.5 20.5 %copy-start.31 = (bf16[32,2048]{1,0:T(8,128)(2,1)S(1)}, bf16[32,2048]{1,0:T(8,128)(2,1)}, u32[]{:S(2)}) copy-start(bf16[32,2048]{1,0:T(8,128)(2,1)} %copy-done.30) | copy-start | bytes 393220
  123.6 20.5 %copy-start.29 = (bf16[32,2048]{1,0:T(8,128)(2,1)S(1)}, bf16[32,2048]{1,0:T(8,128)(2,1)}, u32[]{:S(2)}) copy-start(bf16[32,2048]{1,0:T(8,128)(2,1)} %copy-done.28) | copy-start | bytes 393220
  123.6 21.7 %copy-start.27 = (bf16[32,2048]{1,0:T(8,128)(2,1)S(1)}, bf16[32,2048]{1,0:T(8,128)(2,1)}, u32[]{:S(2)}) copy-start(bf16[32,2048]{1,0:T(8,128)(2,1)} %copy-done.26) | copy-start | bytes 393220
  123.6 24.4 %copy-start.20 = (bf16[64,2048]{1,0:T(8,128)(2,1)S(1)}, bf16[64,2048]{1,0:T(8,128)(2,1)}, u32[]{:S(2)}) copy-start(bf16[64,2048]{1,0:T(8,128)(2,1)} %copy-done.19) | copy-start | bytes 786436
  125.7 24.2 %collective-permute-start.32 = (bf16[32,2048]{1,0:T(8,128)(2,1)S(1)}, bf16[32,2048]{1,0:T(8,128)(2,1)S(1)}, u32[]{:S(2)}, u32[]{:S(2)}) collective-permute-start(bf16[32,2048]{1,0:T(8,128)(2,1)S(1)} %copy-done.35), channel_id=1, source_target_pairs={{0,3},{1,2},{2,1},{3,0},{4,7},{5,6},{6,5},{7,4},{8,11},{9,10},{10,... | collective-permute-start | bytes 393224 | tf_op jit(solution)/shard_map/ppermute | solution.py:513
  138.5 11.7 %collective-permute-start.33 = (bf16[32,2048]{1,0:T(8,128)(2,1)S(1)}, bf16[32,2048]{1,0:T(8,128)(2,1)S(1)}, u32[]{:S(2)}, u32[]{:S(2)}) collective-permute-start(bf16[32,2048]{1,0:T(8,128)(2,1)S(1)} %copy-done.33), channel_id=1, source_target_pairs={{0,4},{1,5},{2,6},{3,7},{4,0},{5,1},{6,2},{7,3},{8,12},{9,13},{10,... | collective-permute-start | bytes 393224 | tf_op jit(solution)/shard_map/ppermute | solution.py:513
  144.1 6.8 %collective-permute-start.34 = (bf16[32,2048]{1,0:T(8,128)(2,1)S(1)}, bf16[32,2048]{1,0:T(8,128)(2,1)S(1)}, u32[]{:S(2)}, u32[]{:S(2)}) collective-permute-start(bf16[32,2048]{1,0:T(8,128)(2,1)S(1)} %copy-done.31), channel_id=1, source_target_pairs={{0,5},{1,4},{2,7},{3,6},{4,1},{5,0},{6,3},{7,2},{8,13},{9,12},{10,... | collective-permute-start | bytes 393224 | tf_op jit(solution)/shard_map/ppermute | solution.py:513
  144.1 9.3 %collective-permute-start.35 = (bf16[32,2048]{1,0:T(8,128)(2,1)S(1)}, bf16[32,2048]{1,0:T(8,128)(2,1)S(1)}, u32[]{:S(2)}, u32[]{:S(2)}) collective-permute-start(bf16[32,2048]{1,0:T(8,128)(2,1)S(1)} %copy-done.29), channel_id=1, source_target_pairs={{0,6},{1,7},{2,4},{3,5},{4,2},{5,3},{6,0},{7,1},{8,14},{9,15},{10,... | collective-permute-start | bytes 393224 | tf_op jit(solution)/shard_map/ppermute | solution.py:513
  145.3 10.0 %copy-start.25 = (bf16[32,2048]{1,0:T(8,128)(2,1)S(1)}, bf16[32,2048]{1,0:T(8,128)(2,1)}, u32[]{:S(2)}) copy-start(bf16[32,2048]{1,0:T(8,128)(2,1)} %copy-done.24) | copy-start | bytes 393220
  145.3 9.9 %collective-permute-start.36 = (bf16[32,2048]{1,0:T(8,128)(2,1)S(1)}, bf16[32,2048]{1,0:T(8,128)(2,1)S(1)}, u32[]{:S(2)}, u32[]{:S(2)}) collective-permute-start(bf16[32,2048]{1,0:T(8,128)(2,1)S(1)} %copy-done.27), channel_id=1, source_target_pairs={{0,7},{1,6},{2,5},{3,4},{4,3},{5,2},{6,1},{7,0},{8,15},{9,14},{10,... | collective-permute-start | bytes 393224 | tf_op jit(solution)/shard_map/ppermute | solution.py:513
  149.9 10.9 %collective-permute-start.27 = (bf16[64,2048]{1,0:T(8,128)(2,1)S(1)}, bf16[64,2048]{1,0:T(8,128)(2,1)S(1)}, u32[]{:S(2)}, u32[]{:S(2)}) collective-permute-start(bf16[64,2048]{1,0:T(8,128)(2,1)S(1)} %copy-done.18), channel_id=1, source_target_pairs={{0,2},{1,3},{2,0},{3,1},{4,6},{5,7},{6,4},{7,5},{8,10},{9,11},{10,... | collective-permute-start | bytes 786440 | tf_op jit(solution)/shard_map/ppermute | solution.py:513
  150.2 11.0 %collective-permute-start.28 = (bf16[64,2048]{1,0:T(8,128)(2,1)S(1)}, bf16[64,2048]{1,0:T(8,128)(2,1)S(1)}, u32[]{:S(2)}, u32[]{:S(2)}) collective-permute-start(bf16[64,2048]{1,0:T(8,128)(2,1)S(1)} %copy-done.16), channel_id=1, source_target_pairs={{0,4},{1,5},{2,6},{3,7},{4,0},{5,1},{6,2},{7,3},{8,12},{9,13},{10,... | collective-permute-start | bytes 786440 | tf_op jit(solution)/shard_map/ppermute | solution.py:513
  150.8 15.6 %collective-permute-start.29 = (bf16[64,2048]{1,0:T(8,128)(2,1)S(1)}, bf16[64,2048]{1,0:T(8,128)(2,1)S(1)}, u32[]{:S(2)}, u32[]{:S(2)}) collective-permute-start(bf16[64,2048]{1,0:T(8,128)(2,1)S(1)} %copy-done.14), channel_id=1, source_target_pairs={{0,6},{1,7},{2,4},{3,5},{4,2},{5,3},{6,0},{7,1},{8,14},{9,15},{10,... | collective-permute-start | bytes 786440 | tf_op jit(solution)/shard_map/ppermute | solution.py:513
  153.4 15.8 %collective-permute-start.50 = (bf16[128,2048]{1,0:T(8,128)(2,1)S(1)}, bf16[128,2048]{1,0:T(8,128)(2,1)S(1)}, u32[]{:S(2)}, u32[]{:S(2)}) collective-permute-start(bf16[128,2048]{1,0:T(8,128)(2,1)S(1)} %combine.4.refs_6_), channel_id=1, source_target_pairs={{0,8},{8,0},{1,9},{9,1},{2,10},{10,2},{3,11},{11,3},{4,12},{12,4},... | collective-permute-start | bytes 1572872 | tf_op jit(solution)/shard_map/ppermute | solution.py:475
  155.3 13.9 %collective-permute-start.49 = (bf16[128,2048]{1,0:T(8,128)(2,1)S(1)}, bf16[128,2048]{1,0:T(8,128)(2,1)S(1)}, u32[]{:S(2)}, u32[]{:S(2)}) collective-permute-start(bf16[128,2048]{1,0:T(8,128)(2,1)S(1)} %get-tuple-element.105), channel_id=1, source_target_pairs={{0,1},{1,0},{2,3},{3,2},{4,5},{5,4},{6,7},{7,6},{8,9},{9,8},{10,11... | collective-permute-start | bytes 1572872 | tf_op jit(solution)/shard_map/ppermute | solution.py:513
  155.3 11.1 %copy-start.12 = (bf16[64,2048]{1,0:T(8,128)(2,1)S(1)}, bf16[64,2048]{1,0:T(8,128)(2,1)}, u32[]{:S(2)}) copy-start(bf16[64,2048]{1,0:T(8,128)(2,1)} %copy-done.11) | copy-start | bytes 786436
  160.8 20.7 %collective-permute-start.48 = (bf16[128,2048]{1,0:T(8,128)(2,1)S(1)}, bf16[128,2048]{1,0:T(8,128)(2,1)S(1)}, u32[]{:S(2)}, u32[]{:S(2)}) collective-permute-start(bf16[128,2048]{1,0:T(8,128)(2,1)S(1)} %combine.6.refs_6_), channel_id=1, source_target_pairs={{0,8},{8,0},{1,9},{9,1},{2,10},{10,2},{3,11},{11,3},{4,12},{12,4},... | collective-permute-start | bytes 1572872 | tf_op jit(solution)/shard_map/ppermute | solution.py:475
  169.1 7.7 %collective-permute-start.47 = (bf16[128,2048]{1,0:T(8,128)(2,1)}, bf16[128,2048]{1,0:T(8,128)(2,1)S(1)}, u32[]{:S(2)}, u32[]{:S(2)}) collective-permute-start(bf16[128,2048]{1,0:T(8,128)(2,1)} %get-tuple-element.104), channel_id=1, source_target_pairs={{0,1},{1,0},{2,3},{3,2},{4,5},{5,4},{6,7},{7,6},{8,9},{9,8},{10,11... | collective-permute-start | bytes 1572872 | tf_op jit(solution)/shard_map/ppermute | solution.py:513
  170.2 26.6 %collective-permute-start.51 = (bf16[128,2048]{1,0:T(8,128)(2,1)}, bf16[128,2048]{1,0:T(8,128)(2,1)S(1)}, u32[]{:S(2)}, u32[]{:S(2)}) collective-permute-start(bf16[128,2048]{1,0:T(8,128)(2,1)} %add.52), channel_id=1, source_target_pairs={{0,16},{16,0},{1,17},{17,1},{2,18},{18,2},{3,19},{19,3},{4,20},{20... | collective-permute-start | bytes 1572872 | tf_op jit(solution)/shard_map/ppermute | solution.py:475
  171.5 25.2 %copy-start.43 = (f32[128,2048]{1,0:T(8,128)S(1)}, f32[128,2048]{1,0:T(8,128)}, u32[]{:S(2)}) copy-start(f32[128,2048]{1,0:T(8,128)} %copy-done.42) | copy-start | bytes 3145732
  (33 other events, 161.8 us)

commit v2 on v1

--- a/solution.py
+++ b/solution.py
@@ -573,10 +573,10 @@
     made[1] = work(1, [sent])
     arrived[3], sent = send(3, [made[1][0]])
     made[2] = work(2, [sent])
-    rows[1] = attend(1, made[2][0])
-    made[3] = work(3, [rows[1]])
+    made[3] = work(3, [made[2][0]])
     rows[3] = attend(3, made[3][0])
     rows[2] = attend(2, rows[3])
+    rows[1] = attend(1, rows[2])
     attended = jnp.concatenate([rows[i] for i in (2, 0, 1, 3)], axis=0)
 
     back = {i: exchange(made[i], i) for i in (3, 2, 1, 0)}
@@ -587,12 +587,12 @@
         own_part, *other = combine(layout(i)[1], where, chunks[i], back[i], after)
         return [own_part] + [mate(x, 1) for x in other], own_part
 
-    parts, done = gather(3, [])
+    parts, done = gather(1, [])
+    side = add(parts) if len(parts) > 1 else parts[0].astype(BF16)
+    parts, done = gather(3, [done])
     last = add(parts) if len(parts) > 1 else parts[0].astype(BF16)
     parts, done = gather(2, [last])
     mid = add(parts + [relay(last, "zl")])
-    parts, done = gather(1, [done])
-    side = add(parts) if len(parts) > 1 else parts[0].astype(BF16)
     parts, _ = gather(0, [done])
     mixer_out = mix(token_rows, mix_weight)
     summed = add(parts + [relay(side, "zl"), relay(mid, "zh")])

time: 198 us -> 226 us (1.14)
  waiting for transfers between devices: 74.1 us -> 95.1 us
  starting transfers between devices: 59.2 us -> 64.5 us
    ppermute x6, waiting for transfers between devices: 44.2 us -> 57.1 us  [relay(): return lax.ppermute(x, axis, [(0, 1), (1, 0)])]
    ppermute x44, waiting for transfers between devices: 29.8 us -> 38 us  [mate(): return lax.ppermute(x, inner, [(i, i ^ step) for i in range(plane)])]
    ppermute x44, starting transfers between devices: 41.7 us -> 46 us  [mate(): return lax.ppermute(x, inner, [(i, i ^ step) for i in range(plane)])]
    unnamed x88 -> x48, local copies, waits for them, and re-layouts: 5.72 us -> 4.92 us
  transfers between devices with their start and end apart: 53 -> 53, of which waited for: 11 -> 10; matrix products, arithmetic and copies ran while one was open for 1% -> 1% of each run, Pallas kernels for 27% -> 24%
where the time goes in v2:
time: 226 us; the launch traced here: 225 us
  waiting for transfers between devices  95.1 us (42%)
  starting transfers between devices  64.5 us (29%)
  Pallas kernels  57.8 us (26%)
  local copies, waits for them, and re-layouts  5.03 us (2%)
    ppermute x6, waiting for transfers between devices, relay(): return lax.ppermute(x, axis, [(0, 1), (1, 0)])  57.1 us
    ppermute x44, starting transfers between devices, mate(): return lax.ppermute(x, inner, [(i, i ^ step) for i in range(plane)])  46 us
    ppermute x44, waiting for transfers between devices, mate(): return lax.ppermute(x, inner, [(i, i ^ step) for i in range(plane)])  38 us
    pallas_call x4, Pallas kernels, attention(): pl.pallas_call(functools.partial(attention_kernel, first, count), out_sha...  17.7 us
    pallas_call x4, Pallas kernels, experts(): pl.pallas_call(functools.partial(expert_kernel, pieces), in_specs=[VMEM]...  15.1 us
    ppermute x6, starting transfers between devices, relay(): return lax.ppermute(x, axis, [(0, 1), (1, 0)])  8.9 us
    pallas_call x4, Pallas kernels, combine(): pl.pallas_call(functools.partial(combine_kernel, plan, len(back), count),...  8.43 us
    pallas_call x4, Pallas kernels, dispatch(): pl.pallas_call(functools.partial(dispatch_kernel, plan, pieces, len(paylo...  6.79 us
  transfers between devices with their start and end apart: 53, of which 10 were waited for; matrix products, arithmetic and copies ran while one was open for 1% of the time, Pallas kernels for 24%

profile of v2, /device:TPU:0, one launch (start us, length us, event | category | flops | bytes accessed | tf_op | source)
XLA Modules:
  0.0 225.2 jit_solution(14642969517165952829)
XLA Ops:
  0.7 1.5 norm.1.refs_0_
  2.7 2.6 %collective-permute-start.4 = (bf16[128,2176]{1,0:T(8,128)(2,1)S(1)}, bf16[128,2176]{1,0:T(8,128)(2,1)}, u32[]{:S(2)}, u32[]{:S(2)}) collective-permute-start(bf16[128,2176]{1,0:T(8,128)(2,1)S(1)} %norm.1.refs_0_), channel_id=1, source_target_pairs={{0,8},{8,0},{1,9},{9,1},{2,10},{10,2},{3,11},{11,3},{4,12},{12,4},... | collective-permute-start | bytes 1671176 | tf_op jit(solution)/shard_map/ppermute | solution.py:475
  5.4 2.6 %collective-permute-start.2 = (bf16[128,2176]{1,0:T(8,128)(2,1)S(1)}, bf16[128,2176]{1,0:T(8,128)(2,1)S(1)}, u32[]{:S(2)}, u32[]{:S(2)}) collective-permute-start(bf16[128,2176]{1,0:T(8,128)(2,1)S(1)} %norm.1.refs_0_), channel_id=1, source_target_pairs={{0,16},{16,0},{1,17},{17,1},{2,18},{18,2},{3,19},{19,3},{4,20},{20... | collective-permute-start | bytes 1671176 | tf_op jit(solution)/shard_map/ppermute | solution.py:475
  8.7 1.7 dispatch.4
  10.4 1.6 collective-permute-start.14
  12.0 1.5 collective-permute-start.15
  13.9 19.0 %collective-permute-done.2.refs_0_ = bf16[128,2176]{1,0:T(8,128)(2,1)S(1)} collective-permute-done((bf16[128,2176]{1,0:T(8,128)(2,1)S(1)}, bf16[128,2176]{1,0:T(8,128)(2,1)S(1)}, u32[]{:S(2)}, u32[]{:S(2)}) %collective-permute-start.2) | collective-permute-done | bytes 557088 | tf_op jit(solution)/shard_map/ppermute | solution.py:475
  33.0 6.1 %attention.4.refs_1_ = bf16[384,512]{1,0:T(8,128)(2,1)S(1)} custom-call(s32[2]{0:T(128)S(1)} %pad_add_fusion.refs_3_.info_ref, f32[8]{0:T(128)S(1)} %copy-done.6, f32[168,128]{1,0:T(8,128)S(1)} %pad_maximum_fusion.3.refs_2_.table_ref.left_ref.right_ref, bf16[1024,512]{1,0:T(8,128)(2,1)S(1)} %copy-done.3, bf16[1024,256]{1,0:T(8,128)(2,1)S(1)} %copy-done.4, ...), custom_call_target="tpu_custom_call" | custom-call | flops 1811939328 | bytes 4194304 | tf_op jit(solution)/shard_map/attention/pallas_call | solution.py:406
  39.1 2.0 dispatch.5
  41.1 1.7 collective-permute-start.10
  42.8 1.5 collective-permute-start.11
  45.9 3.5 %experts.4 = (bf16[64,2048]{1,0:T(8,128)(2,1)S(1)}, bf16[64,2048]{1,0:T(8,128)(2,1)S(1)}, bf16[64,2048]{1,0:T(8,128)(2,1)S(1)}, bf16[64,2048]{1,0:T(8,128)(2,1)S(1)}) custom-call(bf16[1,2048,1024]{2,1,0:T(8,128)(2,1)S(1)} %copy-done, bf16[1,2048,1024]{2,1,0:T(8,128)(2,1)S(1)} %copy-done.1, bf16[1,1024,2048]{2,1,0:T(8,128)(2,1)S(1)} %copy-done.2, ...), custom_call_target="tpu_custom_call" | custom-call | flops 3221225472 | bytes 2097152 | tf_op jit(solution)/shard_map/experts/pallas_call | solution.py:242
  50.1 1.5 collective-permute-start.7
  51.6 1.3 collective-permute-done.12.refs_7_
  52.9 1.6 collective-permute-start.9
  54.9 1.7 dispatch.6
  56.7 2.4 %collective-permute-done.8.refs_3_ = bf16[32,2048]{1,0:T(8,128)(2,1)S(1)} collective-permute-done((bf16[32,2048]{1,0:T(8,128)(2,1)S(1)}, bf16[32,2048]{1,0:T(8,128)(2,1)S(1)}, u32[]{:S(2)}, u32[]{:S(2)}) %collective-permute-start.8) | collective-permute-done | bytes 131104 | tf_op jit(solution)/shard_map/ppermute | solution.py:513
  59.1 3.5 %experts.5 = (bf16[32,2048]{1,0:T(8,128)(2,1)S(1)}, bf16[32,2048]{1,0:T(8,128)(2,1)S(1)}, bf16[32,2048]{1,0:T(8,128)(2,1)S(1)}, bf16[32,2048]{1,0:T(8,128)(2,1)S...) custom-call(bf16[1,2048,1024]{2,1,0:T(8,128)(2,1)S(1)} %copy-done, ...), custom_call_target="tpu_custom_call" | custom-call | flops 3221225472 | bytes 2097152 | tf_op jit(solution)/shard_map/experts/pallas_call | solution.py:242
  63.6 1.0 collective-permute-start.42
  64.7 1.5 collective-permute-start.43
  66.2 3.1 %collective-permute-done.3.refs_0_ = bf16[128,2176]{1,0:T(8,128)(2,1)S(1)} collective-permute-done((bf16[128,2176]{1,0:T(8,128)(2,1)S(1)}, bf16[128,2176]{1,0:T(8,128)(2,1)S(1)}, u32[]{:S(2)}, u32[]{:S(2)}) %collective-permute-start.3) | collective-permute-done | bytes 557088 | tf_op jit(solution)/shard_map/ppermute | solution.py:475
  69.3 1.0 collective-permute-start.45
  70.2 1.9 collective-permute-start.46
  72.1 1.4 dispatch.7
  74.0 1.6 collective-permute-start.25
  75.6 1.5 collective-permute-start.26
  77.7 2.9 %collective-permute-done.46.refs_8_ = bf16[32,2048]{1,0:T(8,128)(2,1)S(1)} collective-permute-done((bf16[32,2048]{1,0:T(8,128)(2,1)S(1)}, bf16[32,2048]{1,0:T(8,128)(2,1)S(1)}, u32[]{:S(2)}, u32[]{:S(2)}) %collective-permute-start.46) | collective-permute-done | bytes 131104 | tf_op jit(solution)/shard_map/ppermute | solution.py:513
  80.6 1.5 collective-permute-start.18
  82.2 2.7 %combine.4.refs_9_ = bf16[128,2048]{1,0:T(8,128)(2,1)} custom-call(s32[2]{0:T(128)S(1)} %pad_add_fusion.1.where_ref, bf16[128,2176]{1,0:T(8,128)(2,1)} %collective-permute-done.4.refs_0_, bf16[32,2048]{1,0:T(8,128)(2,1)S(1)} %get-tuple-element.68.refs_1_, bf16[32,2048]{1,0:T(8,128)(2,1)S(1)} %collective-permute-done.40.refs_2_, ...), custom_call_target="tpu_custom_call" | custom-call | flops 20000000000 | bytes 1048576 | tf_op jit(solution)/shard_map/combine/pallas_call | solution.py:180
  84.8 9.5 %collective-permute-done.18.refs_2_ = bf16[32,2048]{1,0:T(8,128)(2,1)S(1)} collective-permute-done((bf16[32,2048]{1,0:T(8,128)(2,1)S(1)}, bf16[32,2048]{1,0:T(8,128)(2,1)S(1)}, u32[]{:S(2)}, u32[]{:S(2)}) %collective-permute-start.18) | collective-permute-done | bytes 131104 | tf_op jit(solution)/shard_map/ppermute | solution.py:513
  95.6 1.9 collective-permute-start.22
  97.5 1.2 collective-permute-start.23
  98.7 3.8 %experts.6 = (bf16[64,2048]{1,0:T(8,128)(2,1)S(1)}, bf16[64,2048]{1,0:T(8,128)(2,1)S(1)}, bf16[64,2048]{1,0:T(8,128)(2,1)S(1)}, bf16[64,2048]{1,0:T(8,128)(2,1)S(1)}) custom-call(bf16[1,2048,1024]{2,1,0:T(8,128)(2,1)S(1)} %copy-done, bf16[1,2048,1024]{2,1,0:T(8,128)(2,1)S(1)} %copy-done.1, bf16[1,1024,2048]{2,1,0:T(8,128)(2,1)S(1)} %copy-done.2, ...), custom_call_target="tpu_custom_call" | custom-call | flops 3221225472 | bytes 2097152 | tf_op jit(solution)/shard_map/experts/pallas_call | solution.py:242
  102.5 1.3 collective-permute-start.1
  103.8 4.6 %collective-permute-start = (bf16[128,512]{1,0:T(8,128)(2,1)S(1)}, bf16[128,512]{1,0:T(8,128)(2,1)S(1)}, u32[]{:S(2)}, u32[]{:S(2)}) collective-permute-start(bf16[128,512]{1,0:T(8,128)(2,1)S(1)} %pad_maximum_fusion.1), channel_id=1, source_target_pairs={{0,4},{4,8},{8,12},{12,16},{16,20},{20,24},{24,28},{1,5},{5,9},{9,... | collective-permute-start | bytes 393224 | tf_op jit(solution)/shard_map/ppermute | solution.py:536
  108.4 4.3 %experts.7 = (bf16[32,2048]{1,0:T(8,128)(2,1)S(1)}, bf16[32,2048]{1,0:T(8,128)(2,1)S(1)}, bf16[32,2048]{1,0:T(8,128)(2,1)S(1)}, bf16[32,2048]{1,0:T(8,128)(2,1)}...) custom-call(bf16[1,2048,1024]{2,1,0:T(8,128)(2,1)S(1)} %copy-done, ...), custom_call_target="tpu_custom_call" | custom-call | flops 3221225472 | bytes 2097152 | tf_op jit(solution)/shard_map/experts/pallas_call | solution.py:242
  112.7 1.5 collective-permute-start.33
  114.8 0.9 collective-permute-start.35
  115.6 2.9 %collective-permute-start.36 = (bf16[32,2048]{1,0:T(8,128)(2,1)}, bf16[32,2048]{1,0:T(8,128)(2,1)}, u32[]{:S(2)}, u32[]{:S(2)}) collective-permute-start(bf16[32,2048]{1,0:T(8,128)(2,1)} %get-tuple-element.91), channel_id=1, source_target_pairs={{0,4},{1,5},{2,6},{3,7},{4,0},{5,1},{6,2},{7,3},{8,12},{9,13},{10,... | collective-permute-start | bytes 393224 | tf_op jit(solution)/shard_map/ppermute | solution.py:513
  118.5 2.9 %attention.5.after_ref = bf16[128,512]{1,0:T(8,128)(2,1)S(1)} custom-call(s32[2]{0:T(128)S(1)} %pad_add_fusion.refs_3_.info_ref, f32[8]{0:T(128)S(1)} %copy-done.6, f32[168,128]{1,0:T(8,128)S(1)} %pad_maximum_fusion.3.refs_2_.table_ref.left_ref.right_ref, bf16[1024,512]{1,0:T(8,128)(2,1)S(1)} %copy-done.3, bf16[1024,256]{1,0:T(8,128)(2,1)S(1)} %copy-done.4, ...), custom_call_target="tpu_custom_call" | custom-call | flops 603979776 | bytes 4194304 | tf_op jit(solution)/shard_map/attention/pallas_call | solution.py:406
  121.8 2.9 %attention.6.after_ref = bf16[128,512]{1,0:T(8,128)(2,1)S(1)} custom-call(s32[2]{0:T(128)S(1)} %pad_add_fusion.refs_3_.info_ref, f32[8]{0:T(128)S(1)} %copy-done.6, f32[168,128]{1,0:T(8,128)S(1)} %pad_maximum_fusion.3.refs_2_.table_ref.left_ref.right_ref, bf16[1024,512]{1,0:T(8,128)(2,1)S(1)} %copy-done.3, bf16[1024,256]{1,0:T(8,128)(2,1)S(1)} %copy-done.4, ...), custom_call_target="tpu_custom_call" | custom-call | flops 603979776 | bytes 4194304 | tf_op jit(solution)/shard_map/attention/pallas_call | solution.py:406
  124.7 5.9 %attention.7 = bf16[384,512]{1,0:T(8,128)(2,1)S(1)} custom-call(s32[2]{0:T(128)S(1)} %pad_add_fusion.refs_3_.info_ref, f32[8]{0:T(128)S(1)} %copy-done.6, f32[168,128]{1,0:T(8,128)S(1)} %pad_maximum_fusion.3.refs_2_.table_ref.left_ref.right_ref, bf16[1024,512]{1,0:T(8,128)(2,1)S(1)} %copy-done.3, bf16[1024,256]{1,0:T(8,128)(2,1)S(1)} %copy-done.4, ...), custom_call_target="tpu_custom_call" | custom-call | flops 1811939328 | bytes 4194304 | tf_op jit(solution)/shard_map/attention/pallas_call | solution.py:406
  131.2 1.7 collective-permute-start.38
  134.3 1.0 pad_maximum_fusion
  135.3 3.8 %all-to-all-start = ((bf16[4,256,512]{2,1,0:T(8,128)(2,1)}), bf16[4,256,512]{2,1,0:T(8,128)(2,1)S(1)}, u32[]{:S(2)}, u32[]{:S(2)}) async-start(bf16[4,256,512]{2,1,0:T(8,128)(2,1)} %bitcast.7), calls=%async_computation | async-start | bytes 2097152 | tf_op jit(solution)/shard_map/all_to_all | solution.py:584
  139.1 1.7 collective-permute-start.27
  140.8 1.7 collective-permute-start.28
  143.2 2.8 %collective-permute-start.32 = (bf16[64,2048]{1,0:T(8,128)(2,1)}, bf16[64,2048]{1,0:T(8,128)(2,1)S(1)}, u32[]{:S(2)}, u32[]{:S(2)}) collective-permute-start(bf16[64,2048]{1,0:T(8,128)(2,1)} %copy-done.15), channel_id=1, source_target_pairs={{0,6},{1,7},{2,4},{3,5},{4,2},{5,3},{6,0},{7,1},{8,14},{9,15},{10,... | collective-permute-start | bytes 786440 | tf_op jit(solution)/shard_map/ppermute | solution.py:513
  146.0 1.1 copy-done.10
  147.1 0.9 copy-done.19
  148.0 0.9 copy-done.21
  148.9 2.0 combine.5.refs_6_
  150.9 19.2 %collective-permute-done.30.refs_3_ = bf16[64,2048]{1,0:T(8,128)(2,1)S(1)} collective-permute-done((bf16[64,2048]{1,0:T(8,128)(2,1)}, bf16[64,2048]{1,0:T(8,128)(2,1)S(1)}, u32[]{:S(2)}, u32[]{:S(2)}) %collective-permute-start.30) | collective-permute-done | bytes 262176 | tf_op jit(solution)/shard_map/ppermute | solution.py:513
  170.1 2.0 collective-permute-start.29
  172.5 1.6 collective-permute-start.50
  174.1 1.9 combine.6
  176.1 2.6 %collective-permute-done.29.refs_5_ = bf16[64,2048]{1,0:T(8,128)(2,1)S(1)} collective-permute-done((bf16[64,2048]{1,0:T(8,128)(2,1)S(1)}, bf16[64,2048]{1,0:T(8,128)(2,1)S(1)}, u32[]{:S(2)}, u32[]{:S(2)}) %collective-permute-start.29) | collective-permute-done | bytes 262176 | tf_op jit(solution)/shard_map/ppermute | solution.py:513
  178.7 1.9 combine.7
  180.7 16.5 %collective-permute-done.50.refs_2_ = bf16[128,2048]{1,0:T(8,128)(2,1)S(1)} collective-permute-done((bf16[128,2048]{1,0:T(8,128)(2,1)S(1)}, bf16[128,2048]{1,0:T(8,128)(2,1)S(1)}, u32[]{:S(2)}, u32[]{:S(2)}) %collective-permute-start.50) | collective-permute-done | bytes 524320 | tf_op jit(solution)/shard_map/ppermute | solution.py:475
  197.2 0.9 add.52
  198.1 1.2 collective-permute-start.51
  199.4 5.3 %mixer.1 = bf16[256,2048]{1,0:T(8,128)(2,1)} custom-call(bf16[4,256,512]{2,1,0:T(8,128)(2,1)S(1)} %all-to-all-done.rows_ref, bf16[2048,2048]{1,0:T(8,128)(2,1)} %weight_hbm.1), custom_call_target="tpu_custom_call" | custom-call | flops 20000000000 | bytes 1048576 | tf_op jit(solution)/shard_map/mixer/pallas_call | solution.py:458
  204.6 18.5 %collective-permute-done.51.refs_3_ = bf16[128,2048]{1,0:T(8,128)(2,1)S(1)} collective-permute-done((bf16[128,2048]{1,0:T(8,128)(2,1)}, bf16[128,2048]{1,0:T(8,128)(2,1)S(1)}, u32[]{:S(2)}, u32[]{:S(2)}) %collective-permute-start.51) | collective-permute-done | bytes 524320 | tf_op jit(solution)/shard_map/ppermute | solution.py:475
  223.2 2.1 add.53
  (125 shorter events, 12.0 us)
Async XLA Ops:
  0.6 8.0 %copy-start.4 = (bf16[1024,256]{1,0:T(8,128)(2,1)S(1)}, bf16[1024,256]{1,0:T(8,128)(2,1)}, u32[]{:S(2)}) copy-start(bf16[1024,256]{1,0:T(8,128)(2,1)} %k_hbm.7) | copy-start | bytes 1572868
  0.6 8.0 %copy-start.5 = (bf16[1024,256]{1,0:T(8,128)(2,1)S(1)}, bf16[1024,256]{1,0:T(8,128)(2,1)}, u32[]{:S(2)}) copy-start(bf16[1024,256]{1,0:T(8,128)(2,1)} %v_hbm.7) | copy-start | bytes 1572868
  2.2 6.5 %collective-permute-start.5 = (bf16[128,2176]{1,0:T(8,128)(2,1)S(1)}, bf16[128,2176]{1,0:T(8,128)(2,1)S(1)}, u32[]{:S(2)}, u32[]{:S(2)}) collective-permute-start(bf16[128,2176]{1,0:T(8,128)(2,1)S(1)} %norm.1.refs_0_), channel_id=1, source_target_pairs={{0,1},{1,0},{2,3},{3,2},{4,5},{5,4},{6,7},{7,6},{8,9},{9,8},{10,11... | collective-permute-start | bytes 1671176 | tf_op jit(solution)/shard_map/ppermute | solution.py:513
  2.7 36.3 %collective-permute-start.4 = (bf16[128,2176]{1,0:T(8,128)(2,1)S(1)}, bf16[128,2176]{1,0:T(8,128)(2,1)}, u32[]{:S(2)}, u32[]{:S(2)}) collective-permute-start(bf16[128,2176]{1,0:T(8,128)(2,1)S(1)} %norm.1.refs_0_), channel_id=1, source_target_pairs={{0,8},{8,0},{1,9},{9,1},{2,10},{10,2},{3,11},{11,3},{4,12},{12,4},... | collective-permute-start | bytes 1671176 | tf_op jit(solution)/shard_map/ppermute | solution.py:475
  5.4 27.6 %collective-permute-start.2 = (bf16[128,2176]{1,0:T(8,128)(2,1)S(1)}, bf16[128,2176]{1,0:T(8,128)(2,1)S(1)}, u32[]{:S(2)}, u32[]{:S(2)}) collective-permute-start(bf16[128,2176]{1,0:T(8,128)(2,1)S(1)} %norm.1.refs_0_), channel_id=1, source_target_pairs={{0,16},{16,0},{1,17},{17,1},{2,18},{18,2},{3,19},{19,3},{4,20},{20... | collective-permute-start | bytes 1671176 | tf_op jit(solution)/shard_map/ppermute | solution.py:475
  8.6 24.3 %copy-start.3 = (bf16[1024,512]{1,0:T(8,128)(2,1)S(1)}, bf16[1024,512]{1,0:T(8,128)(2,1)}, u32[]{:S(2)}) copy-start(bf16[1024,512]{1,0:T(8,128)(2,1)} %q_hbm.7) | copy-start | bytes 3145732
  8.7 24.3 %copy-start.6 = (f32[8]{0:T(128)S(1)}, f32[8]{0:T(128)}, u32[]{:S(2)}) copy-start(f32[8]{0:T(128)} %sink_ref.7) | copy-start | bytes 100
  10.4 32.4 %collective-permute-start.14 = (bf16[64,2048]{1,0:T(8,128)(2,1)S(1)}, bf16[64,2048]{1,0:T(8,128)(2,1)S(1)}, u32[]{:S(2)}, u32[]{:S(2)}) collective-permute-start(bf16[64,2048]{1,0:T(8,128)(2,1)S(1)} %get-tuple-element.63), channel_id=1, source_target_pairs={{0,2},{1,3},{2,0},{3,1},{4,6},{5,7},{6,4},{7,5},{8,10},{9,11},{10,... | collective-permute-start | bytes 786440 | tf_op jit(solution)/shard_map/ppermute | solution.py:513
  12.0 32.3 %collective-permute-start.15 = (bf16[64,2048]{1,0:T(8,128)(2,1)S(1)}, bf16[64,2048]{1,0:T(8,128)(2,1)S(1)}, u32[]{:S(2)}, u32[]{:S(2)}) collective-permute-start(bf16[64,2048]{1,0:T(8,128)(2,1)S(1)} %get-tuple-element.64), channel_id=1, source_target_pairs={{0,4},{1,5},{2,6},{3,7},{4,0},{5,1},{6,2},{7,3},{8,12},{9,13},{10,... | collective-permute-start | bytes 786440 | tf_op jit(solution)/shard_map/ppermute | solution.py:513
  13.5 31.6 %collective-permute-start.16 = (bf16[64,2048]{1,0:T(8,128)(2,1)S(1)}, bf16[64,2048]{1,0:T(8,128)(2,1)S(1)}, u32[]{:S(2)}, u32[]{:S(2)}) collective-permute-start(bf16[64,2048]{1,0:T(8,128)(2,1)S(1)} %get-tuple-element.65), channel_id=1, source_target_pairs={{0,6},{1,7},{2,4},{3,5},{4,2},{5,3},{6,0},{7,1},{8,14},{9,15},{10,... | collective-permute-start | bytes 786440 | tf_op jit(solution)/shard_map/ppermute | solution.py:513
  32.9 21.5 %collective-permute-start.13 = (bf16[128,2176]{1,0:T(8,128)(2,1)S(1)}, bf16[128,2176]{1,0:T(8,128)(2,1)S(1)}, u32[]{:S(2)}, u32[]{:S(2)}) collective-permute-start(bf16[128,2176]{1,0:T(8,128)(2,1)S(1)} %collective-permute-done.2.refs_0_), channel_id=1, source_target_pairs={{0,1},{1,0},{2,3},{3,2},{4,5},{5,4},{6,7},{7,6},{8,9},{9,8},{10,11... | collective-permute-start | bytes 1671176 | tf_op jit(solution)/shard_map/ppermute | solution.py:513
  41.1 9.0 %collective-permute-start.10 = (bf16[32,2048]{1,0:T(8,128)(2,1)S(1)}, bf16[32,2048]{1,0:T(8,128)(2,1)S(1)}, u32[]{:S(2)}, u32[]{:S(2)}) collective-permute-start(bf16[32,2048]{1,0:T(8,128)(2,1)S(1)} %get-tuple-element.60), channel_id=1, source_target_pairs={{0,5},{1,4},{2,7},{3,6},{4,1},{5,0},{6,3},{7,2},{8,13},{9,12},{10,... | collective-permute-start | bytes 393224 | tf_op jit(solution)/shard_map/ppermute | solution.py:513
  42.8 8.8 %collective-permute-start.11 = (bf16[32,2048]{1,0:T(8,128)(2,1)S(1)}, bf16[32,2048]{1,0:T(8,128)(2,1)S(1)}, u32[]{:S(2)}, u32[]{:S(2)}) collective-permute-start(bf16[32,2048]{1,0:T(8,128)(2,1)S(1)} %get-tuple-element.61), channel_id=1, source_target_pairs={{0,6},{1,7},{2,4},{3,5},{4,2},{5,3},{6,0},{7,1},{8,14},{9,15},{10,... | collective-permute-start | bytes 393224 | tf_op jit(solution)/shard_map/ppermute | solution.py:513
  44.3 8.6 %collective-permute-start.12 = (bf16[32,2048]{1,0:T(8,128)(2,1)S(1)}, bf16[32,2048]{1,0:T(8,128)(2,1)S(1)}, u32[]{:S(2)}, u32[]{:S(2)}) collective-permute-start(bf16[32,2048]{1,0:T(8,128)(2,1)S(1)} %get-tuple-element.62), channel_id=1, source_target_pairs={{0,7},{1,6},{2,5},{3,4},{4,3},{5,2},{6,1},{7,0},{8,15},{9,14},{10,... | collective-permute-start | bytes 393224 | tf_op jit(solution)/shard_map/ppermute | solution.py:513
  45.1 11.6 %collective-permute-start.6 = (bf16[32,2048]{1,0:T(8,128)(2,1)S(1)}, bf16[32,2048]{1,0:T(8,128)(2,1)S(1)}, u32[]{:S(2)}, u32[]{:S(2)}) collective-permute-start(bf16[32,2048]{1,0:T(8,128)(2,1)S(1)} %get-tuple-element.56), channel_id=1, source_target_pairs={{0,1},{1,0},{2,3},{3,2},{4,5},{5,4},{6,7},{7,6},{8,9},{9,8},{10,11... | collective-permute-start | bytes 393224 | tf_op jit(solution)/shard_map/ppermute | solution.py:513
  50.1 6.6 %collective-permute-start.7 = (bf16[32,2048]{1,0:T(8,128)(2,1)S(1)}, bf16[32,2048]{1,0:T(8,128)(2,1)S(1)}, u32[]{:S(2)}, u32[]{:S(2)}) collective-permute-start(bf16[32,2048]{1,0:T(8,128)(2,1)S(1)} %get-tuple-element.57), channel_id=1, source_target_pairs={{0,2},{1,3},{2,0},{3,1},{4,6},{5,7},{6,4},{7,5},{8,10},{9,11},{10,... | collective-permute-start | bytes 393224 | tf_op jit(solution)/shard_map/ppermute | solution.py:513
  51.6 7.5 %collective-permute-start.8 = (bf16[32,2048]{1,0:T(8,128)(2,1)S(1)}, bf16[32,2048]{1,0:T(8,128)(2,1)S(1)}, u32[]{:S(2)}, u32[]{:S(2)}) collective-permute-start(bf16[32,2048]{1,0:T(8,128)(2,1)S(1)} %get-tuple-element.58), channel_id=1, source_target_pairs={{0,3},{1,2},{2,1},{3,0},{4,7},{5,6},{6,5},{7,4},{8,11},{9,10},{10,... | collective-permute-start | bytes 393224 | tf_op jit(solution)/shard_map/ppermute | solution.py:513
  52.9 6.2 %collective-permute-start.9 = (bf16[32,2048]{1,0:T(8,128)(2,1)S(1)}, bf16[32,2048]{1,0:T(8,128)(2,1)S(1)}, u32[]{:S(2)}, u32[]{:S(2)}) collective-permute-start(bf16[32,2048]{1,0:T(8,128)(2,1)S(1)} %get-tuple-element.59), channel_id=1, source_target_pairs={{0,4},{1,5},{2,6},{3,7},{4,0},{5,1},{6,2},{7,3},{8,12},{9,13},{10,... | collective-permute-start | bytes 393224 | tf_op jit(solution)/shard_map/ppermute | solution.py:513
  54.5 14.8 %collective-permute-start.3 = (bf16[128,2176]{1,0:T(8,128)(2,1)S(1)}, bf16[128,2176]{1,0:T(8,128)(2,1)S(1)}, u32[]{:S(2)}, u32[]{:S(2)}) collective-permute-start(bf16[128,2176]{1,0:T(8,128)(2,1)S(1)} %collective-permute-done.2.refs_0_), channel_id=1, source_target_pairs={{0,8},{8,0},{1,9},{9,1},{2,10},{10,2},{3,11},{11,3},{4,12},{12,4},... | collective-permute-start | bytes 1671176 | tf_op jit(solution)/shard_map/ppermute | solution.py:475
  62.6 6.6 %collective-permute-start.40 = (bf16[32,2048]{1,0:T(8,128)(2,1)S(1)}, bf16[32,2048]{1,0:T(8,128)(2,1)S(1)}, u32[]{:S(2)}, u32[]{:S(2)}) collective-permute-start(bf16[32,2048]{1,0:T(8,128)(2,1)S(1)} %get-tuple-element.95), channel_id=1, source_target_pairs={{0,1},{1,0},{2,3},{3,2},{4,5},{5,4},{6,7},{7,6},{8,9},{9,8},{10,11... | collective-permute-start | bytes 393224 | tf_op jit(solution)/shard_map/ppermute | solution.py:513
  62.9 7.3 %collective-permute-start.41 = (bf16[32,2048]{1,0:T(8,128)(2,1)S(1)}, bf16[32,2048]{1,0:T(8,128)(2,1)S(1)}, u32[]{:S(2)}, u32[]{:S(2)}) collective-permute-start(bf16[32,2048]{1,0:T(8,128)(2,1)S(1)} %get-tuple-element.96), channel_id=1, source_target_pairs={{0,2},{1,3},{2,0},{3,1},{4,6},{5,7},{6,4},{7,5},{8,10},{9,11},{10,... | collective-permute-start | bytes 393224 | tf_op jit(solution)/shard_map/ppermute | solution.py:513
  63.6 9.9 %collective-permute-start.42 = (bf16[32,2048]{1,0:T(8,128)(2,1)S(1)}, bf16[32,2048]{1,0:T(8,128)(2,1)S(1)}, u32[]{:S(2)}, u32[]{:S(2)}) collective-permute-start(bf16[32,2048]{1,0:T(8,128)(2,1)S(1)} %get-tuple-element.97), channel_id=1, source_target_pairs={{0,3},{1,2},{2,1},{3,0},{4,7},{5,6},{6,5},{7,4},{8,11},{9,10},{10,... | collective-permute-start | bytes 393224 | tf_op jit(solution)/shard_map/ppermute | solution.py:513
  64.7 9.4 %collective-permute-start.43 = (bf16[32,2048]{1,0:T(8,128)(2,1)S(1)}, bf16[32,2048]{1,0:T(8,128)(2,1)S(1)}, u32[]{:S(2)}, u32[]{:S(2)}) collective-permute-start(bf16[32,2048]{1,0:T(8,128)(2,1)S(1)} %get-tuple-element.98), channel_id=1, source_target_pairs={{0,4},{1,5},{2,6},{3,7},{4,0},{5,1},{6,2},{7,3},{8,12},{9,13},{10,... | collective-permute-start | bytes 393224 | tf_op jit(solution)/shard_map/ppermute | solution.py:513
  69.2 6.4 %collective-permute-start.44 = (bf16[32,2048]{1,0:T(8,128)(2,1)S(1)}, bf16[32,2048]{1,0:T(8,128)(2,1)S(1)}, u32[]{:S(2)}, u32[]{:S(2)}) collective-permute-start(bf16[32,2048]{1,0:T(8,128)(2,1)S(1)} %get-tuple-element.99), channel_id=1, source_target_pairs={{0,5},{1,4},{2,7},{3,6},{4,1},{5,0},{6,3},{7,2},{8,13},{9,12},{10,... | collective-permute-start | bytes 393224 | tf_op jit(solution)/shard_map/ppermute | solution.py:513
  69.3 7.8 %collective-permute-start.45 = (bf16[32,2048]{1,0:T(8,128)(2,1)S(1)}, bf16[32,2048]{1,0:T(8,128)(2,1)S(1)}, u32[]{:S(2)}, u32[]{:S(2)}) collective-permute-start(bf16[32,2048]{1,0:T(8,128)(2,1)S(1)} %get-tuple-element.100), channel_id=1, source_target_pairs={{0,6},{1,7},{2,4},{3,5},{4,2},{5,3},{6,0},{7,1},{8,14},{9,15},{10,... | collective-permute-start | bytes 393224 | tf_op jit(solution)/shard_map/ppermute | solution.py:513
  70.2 10.4 %collective-permute-start.46 = (bf16[32,2048]{1,0:T(8,128)(2,1)S(1)}, bf16[32,2048]{1,0:T(8,128)(2,1)S(1)}, u32[]{:S(2)}, u32[]{:S(2)}) collective-permute-start(bf16[32,2048]{1,0:T(8,128)(2,1)S(1)} %get-tuple-element.101), channel_id=1, source_target_pairs={{0,7},{1,6},{2,5},{3,4},{4,3},{5,2},{6,1},{7,0},{8,15},{9,14},{10,... | collective-permute-start | bytes 393224 | tf_op jit(solution)/shard_map/ppermute | solution.py:513
  73.5 21.6 %collective-permute-start.24 = (bf16[64,2048]{1,0:T(8,128)(2,1)S(1)}, bf16[64,2048]{1,0:T(8,128)(2,1)S(1)}, u32[]{:S(2)}, u32[]{:S(2)}) collective-permute-start(bf16[64,2048]{1,0:T(8,128)(2,1)S(1)} %get-tuple-element.77), channel_id=1, source_target_pairs={{0,2},{1,3},{2,0},{3,1},{4,6},{5,7},{6,4},{7,5},{8,10},{9,11},{10,... | collective-permute-start | bytes 786440 | tf_op jit(solution)/shard_map/ppermute | solution.py:513
  74.0 21.6 %collective-permute-start.25 = (bf16[64,2048]{1,0:T(8,128)(2,1)S(1)}, bf16[64,2048]{1,0:T(8,128)(2,1)S(1)}, u32[]{:S(2)}, u32[]{:S(2)}) collective-permute-start(bf16[64,2048]{1,0:T(8,128)(2,1)S(1)} %get-tuple-element.78), channel_id=1, source_target_pairs={{0,4},{1,5},{2,6},{3,7},{4,0},{5,1},{6,2},{7,3},{8,12},{9,13},{10,... | collective-permute-start | bytes 786440 | tf_op jit(solution)/shard_map/ppermute | solution.py:513
  75.6 21.9 %collective-permute-start.26 = (bf16[64,2048]{1,0:T(8,128)(2,1)S(1)}, bf16[64,2048]{1,0:T(8,128)(2,1)S(1)}, u32[]{:S(2)}, u32[]{:S(2)}) collective-permute-start(bf16[64,2048]{1,0:T(8,128)(2,1)S(1)} %get-tuple-element.79), channel_id=1, source_target_pairs={{0,6},{1,7},{2,4},{3,5},{4,2},{5,3},{6,0},{7,1},{8,14},{9,15},{10,... | collective-permute-start | bytes 786440 | tf_op jit(solution)/shard_map/ppermute | solution.py:513
  77.1 7.7 %collective-permute-start.17 = (bf16[32,2048]{1,0:T(8,128)(2,1)S(1)}, bf16[32,2048]{1,0:T(8,128)(2,1)S(1)}, u32[]{:S(2)}, u32[]{:S(2)}) collective-permute-start(bf16[32,2048]{1,0:T(8,128)(2,1)S(1)} %get-tuple-element.70), channel_id=1, source_target_pairs={{0,1},{1,0},{2,3},{3,2},{4,5},{5,4},{6,7},{7,6},{8,9},{9,8},{10,11... | collective-permute-start | bytes 393224 | tf_op jit(solution)/shard_map/ppermute | solution.py:513
  80.6 13.7 %collective-permute-start.18 = (bf16[32,2048]{1,0:T(8,128)(2,1)S(1)}, bf16[32,2048]{1,0:T(8,128)(2,1)S(1)}, u32[]{:S(2)}, u32[]{:S(2)}) collective-permute-start(bf16[32,2048]{1,0:T(8,128)(2,1)S(1)} %get-tuple-element.71), channel_id=1, source_target_pairs={{0,2},{1,3},{2,0},{3,1},{4,6},{5,7},{6,4},{7,5},{8,10},{9,11},{10,... | collective-permute-start | bytes 393224 | tf_op jit(solution)/shard_map/ppermute | solution.py:513
  84.8 17.7 %collective-permute-start.19 = (bf16[32,2048]{1,0:T(8,128)(2,1)S(1)}, bf16[32,2048]{1,0:T(8,128)(2,1)S(1)}, u32[]{:S(2)}, u32[]{:S(2)}) collective-permute-start(bf16[32,2048]{1,0:T(8,128)(2,1)S(1)} %get-tuple-element.72), channel_id=1, source_target_pairs={{0,3},{1,2},{2,1},{3,0},{4,7},{5,6},{6,5},{7,4},{8,11},{9,10},{10,... | collective-permute-start | bytes 393224 | tf_op jit(solution)/shard_map/ppermute | solution.py:513
  94.3 9.5 %collective-permute-start.20 = (bf16[32,2048]{1,0:T(8,128)(2,1)S(1)}, bf16[32,2048]{1,0:T(8,128)(2,1)S(1)}, u32[]{:S(2)}, u32[]{:S(2)}) collective-permute-start(bf16[32,2048]{1,0:T(8,128)(2,1)S(1)} %get-tuple-element.73), channel_id=1, source_target_pairs={{0,4},{1,5},{2,6},{3,7},{4,0},{5,1},{6,2},{7,3},{8,12},{9,13},{10,... | collective-permute-start | bytes 393224 | tf_op jit(solution)/shard_map/ppermute | solution.py:513
  95.2 13.2 %collective-permute-start.21 = (bf16[32,2048]{1,0:T(8,128)(2,1)S(1)}, bf16[32,2048]{1,0:T(8,128)(2,1)S(1)}, u32[]{:S(2)}, u32[]{:S(2)}) collective-permute-start(bf16[32,2048]{1,0:T(8,128)(2,1)S(1)} %get-tuple-element.74), channel_id=1, source_target_pairs={{0,5},{1,4},{2,7},{3,6},{4,1},{5,0},{6,3},{7,2},{8,13},{9,12},{10,... | collective-permute-start | bytes 393224 | tf_op jit(solution)/shard_map/ppermute | solution.py:513
  95.6 12.8 %collective-permute-start.22 = (bf16[32,2048]{1,0:T(8,128)(2,1)S(1)}, bf16[32,2048]{1,0:T(8,128)(2,1)S(1)}, u32[]{:S(2)}, u32[]{:S(2)}) collective-permute-start(bf16[32,2048]{1,0:T(8,128)(2,1)S(1)} %get-tuple-element.75), channel_id=1, source_target_pairs={{0,6},{1,7},{2,4},{3,5},{4,2},{5,3},{6,0},{7,1},{8,14},{9,15},{10,... | collective-permute-start | bytes 393224 | tf_op jit(solution)/shard_map/ppermute | solution.py:513
  97.5 10.9 %collective-permute-start.23 = (bf16[32,2048]{1,0:T(8,128)(2,1)S(1)}, bf16[32,2048]{1,0:T(8,128)(2,1)S(1)}, u32[]{:S(2)}, u32[]{:S(2)}) collective-permute-start(bf16[32,2048]{1,0:T(8,128)(2,1)S(1)} %get-tuple-element.76), channel_id=1, source_target_pairs={{0,7},{1,6},{2,5},{3,4},{4,3},{5,2},{6,1},{7,0},{8,15},{9,14},{10,... | collective-permute-start | bytes 393224 | tf_op jit(solution)/shard_map/ppermute | solution.py:513
  102.5 10.2 %copy-start.15 = (bf16[64,2048]{1,0:T(8,128)(2,1)}, bf16[64,2048]{1,0:T(8,128)(2,1)S(1)}, u32[]{:S(2)}) copy-start(bf16[64,2048]{1,0:T(8,128)(2,1)S(1)} %get-tuple-element.87) | copy-start | bytes 786436
  102.5 10.2 %copy-start.16 = (bf16[64,2048]{1,0:T(8,128)(2,1)}, bf16[64,2048]{1,0:T(8,128)(2,1)S(1)}, u32[]{:S(2)}) copy-start(bf16[64,2048]{1,0:T(8,128)(2,1)S(1)} %get-tuple-element.86) | copy-start | bytes 786436
  102.5 10.2 %copy-start.17 = (bf16[64,2048]{1,0:T(8,128)(2,1)}, bf16[64,2048]{1,0:T(8,128)(2,1)S(1)}, u32[]{:S(2)}) copy-start(bf16[64,2048]{1,0:T(8,128)(2,1)S(1)} %get-tuple-element.85) | copy-start | bytes 786436
  102.5 13.1 %collective-permute-start.1 = (bf16[128,512]{1,0:T(8,128)(2,1)S(1)}, bf16[128,512]{1,0:T(8,128)(2,1)S(1)}, u32[]{:S(2)}, u32[]{:S(2)}) collective-permute-start(bf16[128,512]{1,0:T(8,128)(2,1)S(1)} %pad_maximum_fusion.2), channel_id=1, source_target_pairs={{4,0},{8,4},{12,8},{16,12},{20,16},{24,20},{28,24},{5,1},{9,5},{13... | collective-permute-start | bytes 393224 | tf_op jit(solution)/shard_map/ppermute | solution.py:537
  103.8 17.6 %collective-permute-start = (bf16[128,512]{1,0:T(8,128)(2,1)S(1)}, bf16[128,512]{1,0:T(8,128)(2,1)S(1)}, u32[]{:S(2)}, u32[]{:S(2)}) collective-permute-start(bf16[128,512]{1,0:T(8,128)(2,1)S(1)} %pad_maximum_fusion.1), channel_id=1, source_target_pairs={{0,4},{4,8},{8,12},{12,16},{16,20},{20,24},{24,28},{1,5},{5,9},{9,... | collective-permute-start | bytes 393224 | tf_op jit(solution)/shard_map/ppermute | solution.py:536
  112.7 17.8 %collective-permute-start.33 = (bf16[32,2048]{1,0:T(8,128)(2,1)S(1)}, bf16[32,2048]{1,0:T(8,128)(2,1)S(1)}, u32[]{:S(2)}, u32[]{:S(2)}) collective-permute-start(bf16[32,2048]{1,0:T(8,128)(2,1)S(1)} %get-tuple-element.88), channel_id=1, source_target_pairs={{0,1},{1,0},{2,3},{3,2},{4,5},{5,4},{6,7},{7,6},{8,9},{9,8},{10,11... | collective-permute-start | bytes 393224 | tf_op jit(solution)/shard_map/ppermute | solution.py:513
  114.2 18.8 %collective-permute-start.34 = (bf16[32,2048]{1,0:T(8,128)(2,1)S(1)}, bf16[32,2048]{1,0:T(8,128)(2,1)S(1)}, u32[]{:S(2)}, u32[]{:S(2)}) collective-permute-start(bf16[32,2048]{1,0:T(8,128)(2,1)S(1)} %get-tuple-element.89), channel_id=1, source_target_pairs={{0,2},{1,3},{2,0},{3,1},{4,6},{5,7},{6,4},{7,5},{8,10},{9,11},{10,... | collective-permute-start | bytes 393224 | tf_op jit(solution)/shard_map/ppermute | solution.py:513
  114.8 24.3 %collective-permute-start.35 = (bf16[32,2048]{1,0:T(8,128)(2,1)}, bf16[32,2048]{1,0:T(8,128)(2,1)}, u32[]{:S(2)}, u32[]{:S(2)}) collective-permute-start(bf16[32,2048]{1,0:T(8,128)(2,1)} %get-tuple-element.90), channel_id=1, source_target_pairs={{0,3},{1,2},{2,1},{3,0},{4,7},{5,6},{6,5},{7,4},{8,11},{9,10},{10,... | collective-permute-start | bytes 393224 | tf_op jit(solution)/shard_map/ppermute | solution.py:513
  115.6 25.2 %collective-permute-start.36 = (bf16[32,2048]{1,0:T(8,128)(2,1)}, bf16[32,2048]{1,0:T(8,128)(2,1)}, u32[]{:S(2)}, u32[]{:S(2)}) collective-permute-start(bf16[32,2048]{1,0:T(8,128)(2,1)} %get-tuple-element.91), channel_id=1, source_target_pairs={{0,4},{1,5},{2,6},{3,7},{4,0},{5,1},{6,2},{7,3},{8,12},{9,13},{10,... | collective-permute-start | bytes 393224 | tf_op jit(solution)/shard_map/ppermute | solution.py:513
  121.4 21.1 %collective-permute-start.37 = (bf16[32,2048]{1,0:T(8,128)(2,1)}, bf16[32,2048]{1,0:T(8,128)(2,1)}, u32[]{:S(2)}, u32[]{:S(2)}) collective-permute-start(bf16[32,2048]{1,0:T(8,128)(2,1)} %get-tuple-element.92), channel_id=1, source_target_pairs={{0,5},{1,4},{2,7},{3,6},{4,1},{5,0},{6,3},{7,2},{8,13},{9,12},{10,... | collective-permute-start | bytes 393224 | tf_op jit(solution)/shard_map/ppermute | solution.py:513
  131.2 11.7 %collective-permute-start.38 = (bf16[32,2048]{1,0:T(8,128)(2,1)}, bf16[32,2048]{1,0:T(8,128)(2,1)}, u32[]{:S(2)}, u32[]{:S(2)}) collective-permute-start(bf16[32,2048]{1,0:T(8,128)(2,1)} %get-tuple-element.93), channel_id=1, source_target_pairs={{0,6},{1,7},{2,4},{3,5},{4,2},{5,3},{6,0},{7,1},{8,14},{9,15},{10,... | collective-permute-start | bytes 393224 | tf_op jit(solution)/shard_map/ppermute | solution.py:513
  133.6 9.6 %collective-permute-start.39 = (bf16[32,2048]{1,0:T(8,128)(2,1)S(1)}, bf16[32,2048]{1,0:T(8,128)(2,1)}, u32[]{:S(2)}, u32[]{:S(2)}) collective-permute-start(bf16[32,2048]{1,0:T(8,128)(2,1)S(1)} %get-tuple-element.94), channel_id=1, source_target_pairs={{0,7},{1,6},{2,5},{3,4},{4,3},{5,2},{6,1},{7,0},{8,15},{9,14},{10,... | collective-permute-start | bytes 393224 | tf_op jit(solution)/shard_map/ppermute | solution.py:513
  135.3 64.0 %all-to-all-start = ((bf16[4,256,512]{2,1,0:T(8,128)(2,1)}), bf16[4,256,512]{2,1,0:T(8,128)(2,1)S(1)}, u32[]{:S(2)}, u32[]{:S(2)}) async-start(bf16[4,256,512]{2,1,0:T(8,128)(2,1)} %bitcast.7), calls=%async_computation | async-start | bytes 2097152 | tf_op jit(solution)/shard_map/all_to_all | solution.py:584
  139.1 36.9 %collective-permute-start.27 = (bf16[64,2048]{1,0:T(8,128)(2,1)}, bf16[64,2048]{1,0:T(8,128)(2,1)S(1)}, u32[]{:S(2)}, u32[]{:S(2)}) collective-permute-start(bf16[64,2048]{1,0:T(8,128)(2,1)} %copy-done.14), channel_id=1, source_target_pairs={{0,2},{1,3},{2,0},{3,1},{4,6},{5,7},{6,4},{7,5},{8,10},{9,11},{10,... | collective-permute-start | bytes 786440 | tf_op jit(solution)/shard_map/ppermute | solution.py:513
  140.8 35.3 %collective-permute-start.28 = (bf16[64,2048]{1,0:T(8,128)(2,1)}, bf16[64,2048]{1,0:T(8,128)(2,1)S(1)}, u32[]{:S(2)}, u32[]{:S(2)}) collective-permute-start(bf16[64,2048]{1,0:T(8,128)(2,1)} %copy-done.13), channel_id=1, source_target_pairs={{0,4},{1,5},{2,6},{3,7},{4,0},{5,1},{6,2},{7,3},{8,12},{9,13},{10,... | collective-permute-start | bytes 786440 | tf_op jit(solution)/shard_map/ppermute | solution.py:513
  142.5 27.6 %collective-permute-start.30 = (bf16[64,2048]{1,0:T(8,128)(2,1)}, bf16[64,2048]{1,0:T(8,128)(2,1)S(1)}, u32[]{:S(2)}, u32[]{:S(2)}) collective-permute-start(bf16[64,2048]{1,0:T(8,128)(2,1)} %copy-done.17), channel_id=1, source_target_pairs={{0,2},{1,3},{2,0},{3,1},{4,6},{5,7},{6,4},{7,5},{8,10},{9,11},{10,... | collective-permute-start | bytes 786440 | tf_op jit(solution)/shard_map/ppermute | solution.py:513
  142.9 29.2 %collective-permute-start.31 = (bf16[64,2048]{1,0:T(8,128)(2,1)}, bf16[64,2048]{1,0:T(8,128)(2,1)S(1)}, u32[]{:S(2)}, u32[]{:S(2)}) collective-permute-start(bf16[64,2048]{1,0:T(8,128)(2,1)} %copy-done.16), channel_id=1, source_target_pairs={{0,4},{1,5},{2,6},{3,7},{4,0},{5,1},{6,2},{7,3},{8,12},{9,13},{10,... | collective-permute-start | bytes 786440 | tf_op jit(solution)/shard_map/ppermute | solution.py:513
  143.2 30.9 %copy-start.8 = (bf16[128,2176]{1,0:T(8,128)(2,1)S(1)}, bf16[128,2176]{1,0:T(8,128)(2,1)}, u32[]{:S(2)}) copy-start(bf16[128,2176]{1,0:T(8,128)(2,1)} %copy-done.7) | copy-start | bytes 1671172
  143.2 29.3 %collective-permute-start.32 = (bf16[64,2048]{1,0:T(8,128)(2,1)}, bf16[64,2048]{1,0:T(8,128)(2,1)S(1)}, u32[]{:S(2)}, u32[]{:S(2)}) collective-permute-start(bf16[64,2048]{1,0:T(8,128)(2,1)} %copy-done.15), channel_id=1, source_target_pairs={{0,6},{1,7},{2,4},{3,5},{4,2},{5,3},{6,0},{7,1},{8,14},{9,15},{10,... | collective-permute-start | bytes 786440 | tf_op jit(solution)/shard_map/ppermute | solution.py:513
  148.9 21.2 %copy-start.12 = (bf16[64,2048]{1,0:T(8,128)(2,1)S(1)}, bf16[64,2048]{1,0:T(8,128)(2,1)}, u32[]{:S(2)}) copy-start(bf16[64,2048]{1,0:T(8,128)(2,1)} %copy-done.11) | copy-start | bytes 786436
  170.1 8.6 %collective-permute-start.29 = (bf16[64,2048]{1,0:T(8,128)(2,1)S(1)}, bf16[64,2048]{1,0:T(8,128)(2,1)S(1)}, u32[]{:S(2)}, u32[]{:S(2)}) collective-permute-start(bf16[64,2048]{1,0:T(8,128)(2,1)S(1)} %copy-done.12), channel_id=1, source_target_pairs={{0,6},{1,7},{2,4},{3,5},{4,2},{5,3},{6,0},{7,1},{8,14},{9,15},{10,... | collective-permute-start | bytes 786440 | tf_op jit(solution)/shard_map/ppermute | solution.py:513
  172.1 32.5 %collective-permute-start.48 = (bf16[128,2048]{1,0:T(8,128)(2,1)}, bf16[128,2048]{1,0:T(8,128)(2,1)}, u32[]{:S(2)}, u32[]{:S(2)}) collective-permute-start(bf16[128,2048]{1,0:T(8,128)(2,1)} %combine.4.refs_9_), channel_id=1, source_target_pairs={{0,8},{8,0},{1,9},{9,1},{2,10},{10,2},{3,11},{11,3},{4,12},{12,4},... | collective-permute-start | bytes 1572872 | tf_op jit(solution)/shard_map/ppermute | solution.py:475
  172.5 24.7 %collective-permute-start.50 = (bf16[128,2048]{1,0:T(8,128)(2,1)S(1)}, bf16[128,2048]{1,0:T(8,128)(2,1)S(1)}, u32[]{:S(2)}, u32[]{:S(2)}) collective-permute-start(bf16[128,2048]{1,0:T(8,128)(2,1)S(1)} %combine.5.refs_6_), channel_id=1, source_target_pairs={{0,8},{8,0},{1,9},{9,1},{2,10},{10,2},{3,11},{11,3},{4,12},{12,4},... | collective-permute-start | bytes 1572872 | tf_op jit(solution)/shard_map/ppermute | solution.py:475
  176.0 21.2 %collective-permute-start.49 = (bf16[128,2048]{1,0:T(8,128)(2,1)S(1)}, bf16[128,2048]{1,0:T(8,128)(2,1)S(1)}, u32[]{:S(2)}, u32[]{:S(2)}) collective-permute-start(bf16[128,2048]{1,0:T(8,128)(2,1)S(1)} %get-tuple-element.105), channel_id=1, source_target_pairs={{0,1},{1,0},{2,3},{3,2},{4,5},{5,4},{6,7},{7,6},{8,9},{9,8},{10,11... | collective-permute-start | bytes 1572872 | tf_op jit(solution)/shard_map/ppermute | solution.py:513
  180.6 17.5 %copy-start.22 = (f32[128,2048]{1,0:T(8,128)}, f32[128,2048]{1,0:T(8,128)S(1)}, u32[]{:S(2)}) copy-start(f32[128,2048]{1,0:T(8,128)S(1)} %get-tuple-element.103.refs_0_) | copy-start | bytes 3145732
  180.6 24.0 %collective-permute-start.47 = (bf16[128,2048]{1,0:T(8,128)(2,1)S(1)}, bf16[128,2048]{1,0:T(8,128)(2,1)S(1)}, u32[]{:S(2)}, u32[]{:S(2)}) collective-permute-start(bf16[128,2048]{1,0:T(8,128)(2,1)S(1)} %get-tuple-element.104), channel_id=1, source_target_pairs={{0,1},{1,0},{2,3},{3,2},{4,5},{5,4},{6,7},{7,6},{8,9},{9,8},{10,11... | collective-permute-start | bytes 1572872 | tf_op jit(solution)/shard_map/ppermute | solution.py:513
  198.1 25.0 %collective-permute-start.51 = (bf16[128,2048]{1,0:T(8,128)(2,1)}, bf16[128,2048]{1,0:T(8,128)(2,1)S(1)}, u32[]{:S(2)}, u32[]{:S(2)}) collective-permute-start(bf16[128,2048]{1,0:T(8,128)(2,1)} %add.52), channel_id=1, source_target_pairs={{0,16},{16,0},{1,17},{17,1},{2,18},{18,2},{3,19},{19,3},{4,20},{20... | collective-permute-start | bytes 1572872 | tf_op jit(solution)/shard_map/ppermute | solution.py:475
  199.3 23.8 %copy-start.23 = (f32[128,2048]{1,0:T(8,128)S(1)}, f32[128,2048]{1,0:T(8,128)}, u32[]{:S(2)}) copy-start(f32[128,2048]{1,0:T(8,128)} %copy-done.22) | copy-start | bytes 3145732
  (13 other events, 44.8 us)
